TPU v7x, 32 devices: a whole 2x2x4 slice. The times are simulated.
32 devices in a mesh: ep: 4 (over y, x), tp: 8 (over z, core).
Axes of the slice: x: 2, y: 2, z: 4, core: 2. Of those that a mesh axis runs over, the one named last changes fastest.
Arguments:
- mixer_input: bfloat16 [6144, 1024], P(('ep', 'tp')), may hold values from -6 to 6
- mixer_gain: float32 [1024], replicated, may hold values from 0.1 to 1.9
- group_weight: bfloat16 [4, 256, 256], replicated, may hold values from -0.375 to 0.375
- mixer_scale: float32 [1024], replicated, may hold values from 0.1 to 1.9
- expert_input: bfloat16 [6144, 1024], P(('ep', 'tp')), may hold values from -6 to 6
- expert_gain: float32 [1024], replicated, may hold values from 0.1 to 1.9
- routes: int32 [6144, 2], P(('ep', 'tp')), may hold values from 0 to 3, all different within a row; in each aligned block of 192 rows (0 to 191, 192 to 383, ...) at most 144 rows name the same one
- route_weight: float32 [6144, 2], P(('ep', 'tp')), may hold values from 0.2 to 1
- w_gate: bfloat16 [4, 1024, 4096], P('ep', None, 'tp'), may hold values from -0.1875 to 0.1875
- w_up: bfloat16 [4, 1024, 4096], P('ep', None, 'tp'), may hold values from -0.1875 to 0.1875
- w_down: bfloat16 [4, 4096, 1024], P('ep', 'tp'), may hold values from -0.09375 to 0.09375
Outputs:
- mixer_out: bfloat16 [6144, 1024], P(('ep', 'tp'))
- expert_out: bfloat16 [6144, 1024], P(('ep', 'tp'))
Inputs may be any that keep to these rules, and one draw needn't show every extreme that they name: `routes`: each row names 2 different experts. Among the rows of one device no expert is named by more than 144 rows, and in some device's rows some expert is named exactly 144 times.
All inputs are finite; a program needn't handle non-finite values.
Results may differ from a plain program's by a relative error of at most 0.0076.
Values may be sent and summed in bfloat16 or wider, within the bound.
No kernel may reach another device: no remote copies, remote signals or barrier semaphores. Data moves between devices by JAX's collectives and lax.ppermute only.
A program may use at most 128 MiB of HBM per device.

v0:
```python
import jax
import jax.numpy as jnp
from jax import lax
from jax.sharding import PartitionSpec as P

epsilon = 1e-06


def padded_2(value, sides, width):
    for axis, dim in sides:
        size, length = (lax.axis_size(axis), value.shape[dim])
        up = [(i, (i + 1) % size) for i in range(size - 1)]
        down = [(j, i) for i, j in up]
        last = lax.slice_in_dim(value, length - width, length, axis=dim)
        leading = lax.slice_in_dim(value, 0, width, axis=dim)
        before = lax.ppermute(last, axis, up)
        after = lax.ppermute(leading, axis, down)
        value = jnp.concatenate([before, value, after], axis=dim)
    return value


def normalize(row_values, gain):
    values = row_values.astype(jnp.float32)
    scaled = values * lax.rsqrt(jnp.mean(values * values, axis=-1, keepdims=True) + epsilon)
    return (scaled * gain).astype(jnp.bfloat16)


def pool_groups(padded, start_row, row_count, seq_length):
    group_width = padded.shape[1] // 4
    position = start_row + jnp.arange(row_count, dtype=jnp.int32)
    centre = padded[8 : 8 + row_count]
    pooled_parts = []
    for group_index in range(4):
        window = 2 ** (group_index + 1)
        reach_left = window // 2
        reach_right = window - 1 - reach_left
        group_cols = padded[:, group_index * group_width : (group_index + 1) * group_width]
        window_sum = group_cols[8 - reach_left : 8 - reach_left + row_count]
        for offset in range(1 - reach_left, reach_right + 1):
            window_sum = window_sum + group_cols[8 + offset : 8 + offset + row_count]
        cover = (
            jnp.minimum(position + reach_right + 1, seq_length)
            - jnp.maximum(position - reach_left, 0)
        ).astype(jnp.float32)
        pooled_parts.append(
            window_sum / cover[:, None]
            - centre[:, group_index * group_width : (group_index + 1) * group_width]
        )
    return jnp.stack(pooled_parts, axis=1).astype(jnp.bfloat16)


def mixer(mixer_input, mixer_gain, group_weight, mixer_scale):
    row_count = mixer_input.shape[0]
    normed = normalize(mixer_input, mixer_gain)
    padded = padded_2(normed, ((("ep", "tp"), 0),), 8)
    start_row = lax.axis_index(("ep", "tp")) * row_count
    seq_length = row_count * lax.axis_size(("ep", "tp"))
    pooled = pool_groups(padded.astype(jnp.float32), start_row, row_count, seq_length)
    mixed_groups = jnp.einsum(
        "tgi,gio->tgo", pooled, group_weight, preferred_element_type=jnp.float32
    )
    return (mixed_groups.reshape(row_count, -1) * mixer_scale).astype(jnp.bfloat16)


def swap(value, stride):
    size = lax.axis_size("tp")
    return lax.ppermute(value, "tp", [(i, i ^ stride) for i in range(size)])


def route_table(routes, route_weight, experts, capacity):
    row_count, top_count = routes.shape
    named = routes.T
    member = jnp.zeros((experts, row_count), jnp.float32)
    expert_ids = jnp.arange(experts, dtype=jnp.int32)[:, None]
    for k in range(top_count):
        member = member + (named[k][None, :] == expert_ids)
    earlier = (
        jnp.arange(row_count, dtype=jnp.int32)[:, None]
        < jnp.arange(row_count, dtype=jnp.int32)[None, :]
    )
    place = jnp.dot(
        member.astype(jnp.bfloat16),
        earlier.astype(jnp.bfloat16),
        preferred_element_type=jnp.float32,
    )
    place = place + expert_ids.astype(jnp.float32) * capacity
    slots = [
        jnp.sum(jnp.where(named[k][None, :] == expert_ids, place, 0.0), axis=0)
        for k in range(top_count)
    ]
    return jnp.concatenate([jnp.stack(slots), route_weight.T], axis=0)


def slot_hits(table, top_count, slots):
    ids = lax.broadcasted_iota(jnp.int32, (slots, table.shape[1]), 0).astype(jnp.float32)
    return [table[k][None, :] == ids for k in range(top_count)]


def dispatch(rows, table, top_count, slots):
    hits = slot_hits(table, top_count, slots)
    chosen = hits[0]
    for hit in hits[1:]:
        chosen = chosen | hit
    return jnp.dot(
        chosen.astype(jnp.bfloat16), rows, preferred_element_type=jnp.float32
    ).astype(jnp.bfloat16)


def combine(returned, table, top_count):
    hits = slot_hits(table, top_count, returned.shape[0])
    weight = jnp.zeros(hits[0].shape, jnp.float32)
    for k in range(top_count):
        weight = weight + jnp.where(hits[k], table[top_count + k][None, :], 0.0)
    high = lax.reduce_precision(weight, 8, 7)
    low = weight - high
    dims = (((0,), (0,)), ((), ()))
    parts = [
        lax.dot_general(
            part.astype(jnp.bfloat16), returned, dims, preferred_element_type=jnp.float32
        )
        for part in (high, low)
    ]
    return parts[0] + parts[1]


def over_experts(value):
    return lax.all_to_all(value, "ep", split_axis=0, concat_axis=0, tiled=True)


def on_device(
    mixer_input,
    mixer_gain,
    group_weight,
    mixer_scale,
    expert_input,
    expert_gain,
    routes,
    route_weight,
    w_gate,
    w_up,
    w_down,
):
    row_count, top_count = routes.shape
    experts = lax.axis_size("ep") * w_gate.shape[0]
    capacity = 3 * top_count * row_count // (2 * experts)
    slots = experts * capacity
    half = lax.axis_size("tp") // 2

    normed = normalize(expert_input, expert_gain)
    far_rows = swap(normed, half)

    shards = [(w_gate[0], w_up[0], w_down[0])]
    stride = half // 2
    while stride:
        shards = shards + [tuple(swap(w, stride) for w in shard) for shard in shards]
        stride //= 2

    table = route_table(routes, route_weight, experts, capacity)
    far_table = swap(table, half)
    near = over_experts(dispatch(normed, table, top_count, slots))
    far = over_experts(dispatch(far_rows, far_table, top_count, slots))

    def ffn(arrived):
        total = None
        for gate, up, down in shards:
            gate_part = jnp.dot(arrived, gate, preferred_element_type=jnp.float32)
            up_part = jnp.dot(arrived, up, preferred_element_type=jnp.float32)
            hidden = (jax.nn.silu(gate_part) * up_part).astype(jnp.bfloat16)
            term = jnp.dot(hidden, down, preferred_element_type=jnp.float32)
            total = term if total is None else total + term
        return total.astype(jnp.bfloat16)

    far_back = over_experts(ffn(far))
    far_sum = combine(far_back, far_table, top_count).astype(jnp.bfloat16)
    far_sum = swap(far_sum, half)
    near_back = over_experts(ffn(near))
    near_sum = combine(near_back, table, top_count)
    expert_out = (near_sum + far_sum.astype(jnp.float32)).astype(jnp.bfloat16)

    mixer_out = mixer(mixer_input, mixer_gain, group_weight, mixer_scale)
    return (mixer_out, expert_out)


def solution(mesh):
    placed = (
        P(("ep", "tp"), None),
        P(),
        P(),
        P(),
        P(("ep", "tp"), None),
        P(),
        P(("ep", "tp"), None),
        P(("ep", "tp"), None),
        P("ep", None, "tp"),
        P("ep", None, "tp"),
        P("ep", "tp", None),
    )

    return jax.shard_map(
        on_device,
        mesh=mesh,
        in_specs=placed,
        out_specs=(P(("ep", "tp"), None), P(("ep", "tp"), None)),
        check_vma=False,
    )
```

profile of v0, /device:TPU:0, one launch (start us, length us, event | category | flops | bytes accessed | tf_op | source)
XLA Modules:
  0.0 175.7 jit_solution(17170216909956388449)
XLA Ops:
  0.6 0.0 copy-start
  0.6 3.1 %collective-permute-start.2 = (bf16[1024,512]{1,0:T(8,128)(2,1)}, bf16[1024,512]{1,0:T(8,128)(2,1)}, u32[]{:S(2)}, u32[]{:S(2)}) collective-permute-start(bf16[1024,512]{1,0:T(8,128)(2,1)} %bitcast.132), channel_id=1, source_target_pairs={{0,2},{1,3},{2,0},{3,1},{4,6},{5,7},{6,4},{7,5},{8,10},{9,11},{10,... | collective-permute-start | bytes 3145736 | tf_op jit(solution)/shard_map/ppermute | solution.py:67
  3.8 0.0 collective-permute-start.5
  3.8 0.8 fusion.125
  4.5 0.1 select_reduce_fusion.1
  4.7 0.7 pad_maximum_fusion
  5.4 2.7 %collective-permute-start.11 = (f32[4,192]{1,0:T(4,128)S(1)}, f32[4,192]{1,0:T(4,128)S(1)}, u32[]{:S(2)}, u32[]{:S(2)}) collective-permute-start(f32[4,192]{1,0:T(4,128)S(1)} %pad_maximum_fusion), channel_id=1, source_target_pairs={{0,4},{1,5},{2,6},{3,7},{4,0},{5,1},{6,2},{7,3},{8,12},{9,13},{10,... | collective-permute-start | bytes 9224 | tf_op jit(solution)/shard_map/ppermute | solution.py:67
  8.0 1.2 fusion.18
  9.2 1.2 fusion.20
  10.4 0.4 collective-permute-start.12
  10.8 1.6 convolution_convert_fusion.1
  12.3 3.8 %all-to-all-start = ((bf16[4,144,1024]{2,1,0:T(8,128)(2,1)}), bf16[4,144,1024]{2,1,0:T(8,128)(2,1)S(1)}, u32[]{:S(2)}, u32[]{:S(2)}) async-start(bf16[4,144,1024]{2,1,0:T(8,128)(2,1)} %bitcast.11), calls=%async_computation | async-start | bytes 2359296 | tf_op jit(solution)/shard_map/all_to_all | solution.py:127
  16.2 0.2 fusion.15
  16.4 0.2 fusion.17
  16.5 1.7 collective-permute-start
  18.3 9.3 %collective-permute-done.11 = f32[4,192]{1,0:T(4,128)S(1)} collective-permute-done((f32[4,192]{1,0:T(4,128)S(1)}, f32[4,192]{1,0:T(4,128)S(1)}, u32[]{:S(2)}, u32[]{:S(2)}) %collective-permute-start.11) | collective-permute-done | bytes 3104 | tf_op jit(solution)/shard_map/ppermute | solution.py:67
  27.6 1.3 collective-permute-start.1
  28.9 7.7 %collective-permute-start.3 = (bf16[1024,512]{1,0:T(8,128)(2,1)}, bf16[1024,512]{1,0:T(8,128)(2,1)}, u32[]{:S(2)}, u32[]{:S(2)}) collective-permute-start(bf16[1024,512]{1,0:T(8,128)(2,1)} %bitcast.134), channel_id=1, source_target_pairs={{0,2},{1,3},{2,0},{3,1},{4,6},{5,7},{6,4},{7,5},{8,10},{9,11},{10,... | collective-permute-start | bytes 3145736 | tf_op jit(solution)/shard_map/ppermute | solution.py:67
  36.6 0.0 collective-permute-done.1
  36.6 0.0 collective-permute-start.6
  36.6 0.1 maximum_convert_fusion
  36.7 0.2 fusion.96
  36.9 0.9 fusion.93
  37.9 0.0 collective-permute-done.12
  37.9 2.1 %collective-permute-start.4 = (bf16[512,1024]{1,0:T(8,128)(2,1)}, bf16[512,1024]{1,0:T(8,128)(2,1)}, u32[]{:S(2)}, u32[]{:S(2)}) collective-permute-start(bf16[512,1024]{1,0:T(8,128)(2,1)} %bitcast.15), channel_id=1, source_target_pairs={{0,2},{1,3},{2,0},{3,1},{4,6},{5,7},{6,4},{7,5},{8,10},{9,11},{10,... | collective-permute-start | bytes 3145736 | tf_op jit(solution)/shard_map/ppermute | solution.py:67
  40.0 1.6 convolution_convert_fusion
  41.6 4.1 %all-to-all-start.2 = ((bf16[4,144,1024]{2,1,0:T(8,128)(2,1)}), bf16[4,144,1024]{2,1,0:T(8,128)(2,1)S(1)}, u32[]{:S(2)}, u32[]{:S(2)}) async-start(bf16[4,144,1024]{2,1,0:T(8,128)(2,1)} %bitcast.24), calls=%async_computation.2 | async-start | bytes 2359296 | tf_op jit(solution)/shard_map/all_to_all | solution.py:127
  45.7 3.0 %fusion.108 = f32[576,512]{1,0:T(8,128)} fusion(bf16[576,1024]{1,0:T(8,128)(2,1)S(1)} %bitcast.91, bf16[1,1024,512]{2,1,0:T(8,128)(2,1)} %param.19), kind=kOutput, calls=%fused_computation.176 | convolution fusion | flops 603979776 | bytes 3407872 | tf_op jit(solution)/shard_map/dot_general | solution.py:166
  48.7 4.8 %fusion.4 = f32[576,1024]{1,0:T(8,128)} fusion(bf16[576,1024]{1,0:T(8,128)(2,1)S(1)} %bitcast.92, f32[576,512]{1,0:T(8,128)} %fusion.108, bf16[1,512,1024]{2,1,0:T(8,128)(2,1)} %param.21, bf16[1,1024,512]{2,1,0:T(8,128)(2,1)} %param.20), kind=kOutput, calls=%fused_computation.13 | convolution fusion | flops 1209729024 | bytes 6815744 | tf_op jit(solution)/shard_map/dot_general | solution.py:169
  53.6 0.0 collective-permute-done.2
  53.6 0.0 collective-permute-start.7
  53.6 3.0 %fusion.138 = f32[576,512]{1,0:T(8,128)} fusion(bf16[576,1024]{1,0:T(8,128)(2,1)S(1)} %bitcast.93, bf16[1024,512]{1,0:T(8,128)(2,1)} %collective-permute-done.2), kind=kOutput, calls=%fused_computation.200 | convolution fusion | flops 603979776 | bytes 3407872 | tf_op jit(solution)/shard_map/dot_general | solution.py:166
  56.6 4.3 %collective-permute-done.3 = bf16[1024,512]{1,0:T(8,128)(2,1)} collective-permute-done((bf16[1024,512]{1,0:T(8,128)(2,1)}, bf16[1024,512]{1,0:T(8,128)(2,1)}, u32[]{:S(2)}, u32[]{:S(2)}) %collective-permute-start.3) | collective-permute-done | bytes 1048608 | tf_op jit(solution)/shard_map/ppermute | solution.py:67
  60.9 21.2 %collective-permute-done.4 = bf16[512,1024]{1,0:T(8,128)(2,1)} collective-permute-done((bf16[512,1024]{1,0:T(8,128)(2,1)}, bf16[512,1024]{1,0:T(8,128)(2,1)}, u32[]{:S(2)}, u32[]{:S(2)}) %collective-permute-start.4) | collective-permute-done | bytes 1048608 | tf_op jit(solution)/shard_map/ppermute | solution.py:67
  82.1 4.8 %fusion.25 = f32[576,1024]{1,0:T(8,128)} fusion(bf16[512,1024]{1,0:T(8,128)(2,1)} %collective-permute-done.4, f32[576,512]{1,0:T(8,128)} %fusion.138, bf16[576,1024]{1,0:T(8,128)(2,1)S(1)} %bitcast.94, bf16[1024,512]{1,0:T(8,128)(2,1)} %collective-permute-done.3), kind=kOutput, calls=%fused_computation.57 | convolution fusion | flops 1209729024 | bytes 6815744 | tf_op jit(solution)/shard_map/dot_general | solution.py:169
  87.0 0.5 collective-permute-start.9
  87.5 3.1 %fusion.139 = f32[576,512]{1,0:T(8,128)} fusion(bf16[576,1024]{1,0:T(8,128)(2,1)S(1)} %bitcast.95, bf16[1024,512]{1,0:T(8,128)(2,1)} %collective-permute-done.5), kind=kOutput, calls=%fused_computation.201 | convolution fusion | flops 603979776 | bytes 3407872 | tf_op jit(solution)/shard_map/dot_general | solution.py:166
  90.6 4.8 %fusion.26 = f32[576,1024]{1,0:T(8,128)} fusion(bf16[512,1024]{1,0:T(8,128)(2,1)} %collective-permute-done.7, f32[576,512]{1,0:T(8,128)} %fusion.139, bf16[576,1024]{1,0:T(8,128)(2,1)S(1)} %bitcast.96, bf16[1024,512]{1,0:T(8,128)(2,1)} %collective-permute-done.6), kind=kOutput, calls=%fused_computation.58 | convolution fusion | flops 1209729024 | bytes 6815744 | tf_op jit(solution)/shard_map/dot_general | solution.py:169
  95.5 3.1 %fusion.106 = f32[576,512]{1,0:T(8,128)} fusion(bf16[576,1024]{1,0:T(8,128)(2,1)S(1)} %bitcast.99, bf16[1,1024,512]{2,1,0:T(8,128)(2,1)} %param.19), kind=kOutput, calls=%fused_computation.174 | convolution fusion | flops 603979776 | bytes 3407872 | tf_op jit(solution)/shard_map/dot_general | solution.py:166
  98.5 4.9 %fusion.3 = f32[576,1024]{1,0:T(8,128)} fusion(bf16[576,1024]{1,0:T(8,128)(2,1)S(1)} %bitcast.100, f32[576,512]{1,0:T(8,128)} %fusion.106, bf16[1,512,1024]{2,1,0:T(8,128)(2,1)} %param.21, bf16[1,1024,512]{2,1,0:T(8,128)(2,1)} %param.20), kind=kOutput, calls=%fused_computation.12 | convolution fusion | flops 1209729024 | bytes 6815744 | tf_op jit(solution)/shard_map/dot_general | solution.py:169
  103.4 3.1 %fusion.141 = f32[576,512]{1,0:T(8,128)} fusion(bf16[576,1024]{1,0:T(8,128)(2,1)S(1)} %bitcast.101, bf16[1024,512]{1,0:T(8,128)(2,1)} %collective-permute-done.2), kind=kOutput, calls=%fused_computation.203 | convolution fusion | flops 603979776 | bytes 3407872 | tf_op jit(solution)/shard_map/dot_general | solution.py:166
  106.5 4.8 %fusion.27 = f32[576,1024]{1,0:T(8,128)} fusion(bf16[512,1024]{1,0:T(8,128)(2,1)} %collective-permute-done.4, f32[576,512]{1,0:T(8,128)} %fusion.141, bf16[576,1024]{1,0:T(8,128)(2,1)S(1)} %bitcast.102, bf16[1024,512]{1,0:T(8,128)(2,1)} %collective-permute-done.3), kind=kOutput, calls=%fused_computation.59 | convolution fusion | flops 1209729024 | bytes 6815744 | tf_op jit(solution)/shard_map/dot_general | solution.py:169
  111.3 3.0 %fusion.142 = f32[576,512]{1,0:T(8,128)} fusion(bf16[576,1024]{1,0:T(8,128)(2,1)S(1)} %bitcast.103, bf16[1024,512]{1,0:T(8,128)(2,1)} %collective-permute-done.5), kind=kOutput, calls=%fused_computation.204 | convolution fusion | flops 603979776 | bytes 3407872 | tf_op jit(solution)/shard_map/dot_general | solution.py:166
  114.3 4.8 %fusion.28 = f32[576,1024]{1,0:T(8,128)} fusion(bf16[512,1024]{1,0:T(8,128)(2,1)} %collective-permute-done.7, f32[576,512]{1,0:T(8,128)} %fusion.142, bf16[576,1024]{1,0:T(8,128)(2,1)S(1)} %bitcast.104, bf16[1024,512]{1,0:T(8,128)(2,1)} %collective-permute-done.6), kind=kOutput, calls=%fused_computation.60 | convolution fusion | flops 1209729024 | bytes 6815744 | tf_op jit(solution)/shard_map/dot_general | solution.py:169
  119.1 3.0 %fusion.143 = f32[576,512]{1,0:T(8,128)} fusion(bf16[576,1024]{1,0:T(8,128)(2,1)S(1)} %bitcast.105, bf16[1024,512]{1,0:T(8,128)(2,1)} %collective-permute-done.8), kind=kOutput, calls=%fused_computation.205 | convolution fusion | flops 603979776 | bytes 3407872 | tf_op jit(solution)/shard_map/dot_general | solution.py:166
  122.1 6.6 %add_convert_fusion = bf16[576,1024]{1,0:T(8,128)(2,1)} fusion(f32[576,1024]{1,0:T(8,128)} %fusion.28, f32[576,1024]{1,0:T(8,128)} %fusion.3, f32[576,1024]{1,0:T(8,128)} %fusion.27, bf16[512,1024]{1,0:T(8,128)(2,1)} %collective-permute-done.10, f32[576,512]{1,0:T(8,128)} %fusion.143, bf16[576,1024]{1,0:T(8,128)(2,1)S(1)} %bitcast.106, ...), kind=kOutput, calls=%fused_computation | convolution fusion | flops 1212088320 | bytes 12713984 | tf_op jit(solution)/shard_map/dot_general | solution.py:169
  128.7 3.7 %all-to-all-start.3 = ((bf16[4,144,1024]{2,1,0:T(8,128)(2,1)}), bf16[4,144,1024]{2,1,0:T(8,128)(2,1)S(1)}, u32[]{:S(2)}, u32[]{:S(2)}) async-start(bf16[4,144,1024]{2,1,0:T(8,128)(2,1)} %bitcast.110), calls=%async_computation.3 | async-start | bytes 2359296 | tf_op jit(solution)/shard_map/all_to_all | solution.py:127
  132.5 3.1 %fusion.140 = f32[576,512]{1,0:T(8,128)} fusion(bf16[576,1024]{1,0:T(8,128)(2,1)S(1)} %bitcast.97, bf16[1024,512]{1,0:T(8,128)(2,1)} %collective-permute-done.8), kind=kOutput, calls=%fused_computation.202 | convolution fusion | flops 603979776 | bytes 3407872 | tf_op jit(solution)/shard_map/dot_general | solution.py:166
  135.6 6.7 %add_convert_fusion.1 = bf16[576,1024]{1,0:T(8,128)(2,1)} fusion(f32[576,1024]{1,0:T(8,128)} %fusion.26, f32[576,1024]{1,0:T(8,128)} %fusion.4, f32[576,1024]{1,0:T(8,128)} %fusion.25, bf16[512,1024]{1,0:T(8,128)(2,1)} %collective-permute-done.10, f32[576,512]{1,0:T(8,128)} %fusion.140, bf16[576,1024]{1,0:T(8,128)(2,1)S(1)} %bitcast.98, ...), kind=kOutput, calls=%fused_computation.1 | convolution fusion | flops 1212088320 | bytes 12713984 | tf_op jit(solution)/shard_map/dot_general | solution.py:169
  142.3 5.5 %all-to-all-done.3 = bf16[4,144,1024]{2,1,0:T(8,128)(2,1)S(1)} async-done(((bf16[4,144,1024]{2,1,0:T(8,128)(2,1)}), bf16[4,144,1024]{2,1,0:T(8,128)(2,1)S(1)}, u32[]{:S(2)}, u32[]{:S(2)}) %all-to-all-start.3) | async-done | bytes 1179680 | tf_op jit(solution)/shard_map/all_to_all | solution.py:127
  147.7 4.4 %all-to-all-start.1 = ((bf16[4,144,1024]{2,1,0:T(8,128)(2,1)}), bf16[4,144,1024]{2,1,0:T(8,128)(2,1)}, u32[]{:S(2)}, u32[]{:S(2)}) async-start(bf16[4,144,1024]{2,1,0:T(8,128)(2,1)} %bitcast.109), calls=%async_computation.1 | async-start | bytes 2359296 | tf_op jit(solution)/shard_map/all_to_all | solution.py:127
  152.2 0.3 convolution_bitcast_fusion
  152.4 0.0 copy-start.6
  152.4 0.1 copy.14
  152.5 0.6 copy-done.6
  153.1 0.8 multiply_convert_fusion.6
  153.9 0.7 fusion.47
  154.6 0.7 fusion.2
  155.3 2.6 %collective-permute-start.13 = (bf16[192,1024]{1,0:T(8,128)(2,1)S(1)}, bf16[192,1024]{1,0:T(8,128)(2,1)S(1)}, u32[]{:S(2)}, u32[]{:S(2)}) collective-permute-start(bf16[192,1024]{1,0:T(8,128)(2,1)S(1)} %fusion.2), channel_id=1, source_target_pairs={{0,4},{1,5},{2,6},{3,7},{4,0},{5,1},{6,2},{7,3},{8,12},{9,13},{10,... | collective-permute-start | bytes 1179656 | tf_op jit(solution)/shard_map/ppermute | solution.py:67
  157.9 8.9 %all-to-all-done.1 = bf16[4,144,1024]{2,1,0:T(8,128)(2,1)} async-done(((bf16[4,144,1024]{2,1,0:T(8,128)(2,1)}), bf16[4,144,1024]{2,1,0:T(8,128)(2,1)}, u32[]{:S(2)}, u32[]{:S(2)}) %all-to-all-start.1) | async-done | bytes 1179680 | tf_op jit(solution)/shard_map/all_to_all | solution.py:127
  166.8 1.9 %fusion.46 = f32[192,1024]{1,0:T(8,128)S(1)} fusion(bf16[576,1024]{1,0:T(8,128)(2,1)} %bitcast.17, f32[192]{0:T(256)S(1)} %bitcast.124, f32[192]{0:T(256)S(1)} %get-tuple-element.3, f32[192]{0:T(256)S(1)} %bitcast.122, f32[192]{0:T(256)S(1)} %get-tuple-element.2, f32[576]{0:T(1024)S(1)} %iota_convert_fusion), kind=kOutput, calls=%fused_computation.77 | convolution fusion | flops 227266560 | bytes 1971456 | tf_op jit(solution)/shard_map/dot_general | solution.py:118
  168.7 2.0 %convolution_add_fusion.1 = f32[192,1024]{1,0:T(8,128)S(1)} fusion(f32[192,1024]{1,0:T(8,128)S(1)} %fusion.46, bf16[576,1024]{1,0:T(8,128)(2,1)} %bitcast.17, f32[192]{0:T(256)S(1)} %bitcast.125, f32[192]{0:T(256)S(1)} %get-tuple-element.3, f32[192]{0:T(256)S(1)} %bitcast.123, f32[192]{0:T(256)S(1)} %get-tuple-element.2, f32[576]{0:T(1024)S(1)} %iota_convert_fusion), kind=kOutput, calls=%fused_computation.10 | convolution fusion | flops 227573760 | bytes 2757888 | tf_op jit(solution)/shard_map/dot_general | solution.py:118
  170.7 4.1 %collective-permute-done.13 = bf16[192,1024]{1,0:T(8,128)(2,1)S(1)} collective-permute-done((bf16[192,1024]{1,0:T(8,128)(2,1)S(1)}, bf16[192,1024]{1,0:T(8,128)(2,1)S(1)}, u32[]{:S(2)}, u32[]{:S(2)}) %collective-permute-start.13) | collective-permute-done | bytes 393248 | tf_op jit(solution)/shard_map/ppermute | solution.py:67
  174.8 0.8 add_convert_fusion.2
  (31 shorter events, 0.1 us)
Async XLA Ops:
  0.6 151.5 %copy-start = (bf16[4,256,256]{2,1,0:T(8,128)(2,1)S(1)}, bf16[4,256,256]{2,1,0:T(8,128)(2,1)}, u32[]{:S(2)}) copy-start(bf16[4,256,256]{2,1,0:T(8,128)(2,1)} %param.13) | copy-start | bytes 1572868
  0.6 52.9 %collective-permute-start.2 = (bf16[1024,512]{1,0:T(8,128)(2,1)}, bf16[1024,512]{1,0:T(8,128)(2,1)}, u32[]{:S(2)}, u32[]{:S(2)}) collective-permute-start(bf16[1024,512]{1,0:T(8,128)(2,1)} %bitcast.132), channel_id=1, source_target_pairs={{0,2},{1,3},{2,0},{3,1},{4,6},{5,7},{6,4},{7,5},{8,10},{9,11},{10,... | collective-permute-start | bytes 3145736 | tf_op jit(solution)/shard_map/ppermute | solution.py:67
  3.8 83.2 %collective-permute-start.5 = (bf16[1024,512]{1,0:T(8,128)(2,1)}, bf16[1024,512]{1,0:T(8,128)(2,1)}, u32[]{:S(2)}, u32[]{:S(2)}) collective-permute-start(bf16[1024,512]{1,0:T(8,128)(2,1)} %bitcast.133), channel_id=1, source_target_pairs={{0,1},{1,0},{2,3},{3,2},{4,5},{5,4},{6,7},{7,6},{8,9},{9,8},{10,11... | collective-permute-start | bytes 3145736 | tf_op jit(solution)/shard_map/ppermute | solution.py:67
  5.4 22.2 %collective-permute-start.11 = (f32[4,192]{1,0:T(4,128)S(1)}, f32[4,192]{1,0:T(4,128)S(1)}, u32[]{:S(2)}, u32[]{:S(2)}) collective-permute-start(f32[4,192]{1,0:T(4,128)S(1)} %pad_maximum_fusion), channel_id=1, source_target_pairs={{0,4},{1,5},{2,6},{3,7},{4,0},{5,1},{6,2},{7,3},{8,12},{9,13},{10,... | collective-permute-start | bytes 9224 | tf_op jit(solution)/shard_map/ppermute | solution.py:67
  10.4 27.5 %collective-permute-start.12 = (bf16[192,1024]{1,0:T(8,128)(2,1)S(1)}, bf16[192,1024]{1,0:T(8,128)(2,1)S(1)}, u32[]{:S(2)}, u32[]{:S(2)}) collective-permute-start(bf16[192,1024]{1,0:T(8,128)(2,1)S(1)} %fusion.20), channel_id=1, source_target_pairs={{0,4},{1,5},{2,6},{3,7},{4,0},{5,1},{6,2},{7,3},{8,12},{9,13},{10,... | collective-permute-start | bytes 1179656 | tf_op jit(solution)/shard_map/ppermute | solution.py:67
  12.3 3.9 %copy-start.1 = (bf16[192,1024]{1,0:T(8,128)(2,1)S(1)}, bf16[192,1024]{1,0:T(8,128)(2,1)}, u32[]{:S(2)}) copy-start(bf16[192,1024]{1,0:T(8,128)(2,1)} %param.11) | copy-start | bytes 1179652
  12.3 4.0 %copy-start.5 = (f32[1024]{0:T(1024)S(1)}, f32[1024]{0:T(1024)}, u32[]{:S(2)}) copy-start(f32[1024]{0:T(1024)} %param.12) | copy-start | bytes 12292
  12.3 29.2 %all-to-all-start = ((bf16[4,144,1024]{2,1,0:T(8,128)(2,1)}), bf16[4,144,1024]{2,1,0:T(8,128)(2,1)S(1)}, u32[]{:S(2)}, u32[]{:S(2)}) async-start(bf16[4,144,1024]{2,1,0:T(8,128)(2,1)} %bitcast.11), calls=%async_computation | async-start | bytes 2359296 | tf_op jit(solution)/shard_map/all_to_all | solution.py:127
  16.2 2.1 %copy-start.4 = (f32[192,2]{0,1:T(2,128)S(1)}, f32[192,2]{0,1:T(2,128)}, u32[]{:S(2)}) copy-start(f32[192,2]{0,1:T(2,128)} %param.18) | copy-start | bytes 4612
  16.5 12.4 %collective-permute-start = (bf16[8,1024]{1,0:T(8,128)(2,1)S(1)}, bf16[8,1024]{1,0:T(8,128)(2,1)S(1)}, u32[]{:S(2)}, u32[]{:S(2)}) collective-permute-start(bf16[8,1024]{1,0:T(8,128)(2,1)S(1)} %get-tuple-element.7), channel_id=1, source_target_pairs={{0,1},{1,2},{2,3},{3,4},{4,5},{5,6},{6,7},{7,8},{8,9},{9,10},{10,1... | collective-permute-start | bytes 49160 | tf_op jit(solution)/shard_map/ppermute | solution.py:16
  27.6 9.0 %collective-permute-start.1 = (bf16[8,1024]{1,0:T(8,128)(2,1)S(1)}, bf16[8,1024]{1,0:T(8,128)(2,1)S(1)}, u32[]{:S(2)}, u32[]{:S(2)}) collective-permute-start(bf16[8,1024]{1,0:T(8,128)(2,1)S(1)} %get-tuple-element.8), channel_id=1, source_target_pairs={{1,0},{2,1},{3,2},{4,3},{5,4},{6,5},{7,6},{8,7},{9,8},{10,9},{11,1... | collective-permute-start | bytes 49160 | tf_op jit(solution)/shard_map/ppermute | solution.py:17
  28.9 32.0 %collective-permute-start.3 = (bf16[1024,512]{1,0:T(8,128)(2,1)}, bf16[1024,512]{1,0:T(8,128)(2,1)}, u32[]{:S(2)}, u32[]{:S(2)}) collective-permute-start(bf16[1024,512]{1,0:T(8,128)(2,1)} %bitcast.134), channel_id=1, source_target_pairs={{0,2},{1,3},{2,0},{3,1},{4,6},{5,7},{6,4},{7,5},{8,10},{9,11},{10,... | collective-permute-start | bytes 3145736 | tf_op jit(solution)/shard_map/ppermute | solution.py:67
  36.6 54.0 %collective-permute-start.6 = (bf16[1024,512]{1,0:T(8,128)(2,1)}, bf16[1024,512]{1,0:T(8,128)(2,1)}, u32[]{:S(2)}, u32[]{:S(2)}) collective-permute-start(bf16[1024,512]{1,0:T(8,128)(2,1)} %bitcast.135), channel_id=1, source_target_pairs={{0,1},{1,0},{2,3},{3,2},{4,5},{5,4},{6,7},{7,6},{8,9},{9,8},{10,11... | collective-permute-start | bytes 3145736 | tf_op jit(solution)/shard_map/ppermute | solution.py:67
  37.9 44.3 %collective-permute-start.4 = (bf16[512,1024]{1,0:T(8,128)(2,1)}, bf16[512,1024]{1,0:T(8,128)(2,1)}, u32[]{:S(2)}, u32[]{:S(2)}) collective-permute-start(bf16[512,1024]{1,0:T(8,128)(2,1)} %bitcast.15), channel_id=1, source_target_pairs={{0,2},{1,3},{2,0},{3,1},{4,6},{5,7},{6,4},{7,5},{8,10},{9,11},{10,... | collective-permute-start | bytes 3145736 | tf_op jit(solution)/shard_map/ppermute | solution.py:67
  41.6 53.9 %all-to-all-start.2 = ((bf16[4,144,1024]{2,1,0:T(8,128)(2,1)}), bf16[4,144,1024]{2,1,0:T(8,128)(2,1)S(1)}, u32[]{:S(2)}, u32[]{:S(2)}) async-start(bf16[4,144,1024]{2,1,0:T(8,128)(2,1)} %bitcast.24), calls=%async_computation.2 | async-start | bytes 2359296 | tf_op jit(solution)/shard_map/all_to_all | solution.py:127
  53.6 37.1 %collective-permute-start.7 = (bf16[512,1024]{1,0:T(8,128)(2,1)}, bf16[512,1024]{1,0:T(8,128)(2,1)}, u32[]{:S(2)}, u32[]{:S(2)}) collective-permute-start(bf16[512,1024]{1,0:T(8,128)(2,1)} %bitcast.15), channel_id=1, source_target_pairs={{0,1},{1,0},{2,3},{3,2},{4,5},{5,4},{6,7},{7,6},{8,9},{9,8},{10,11... | collective-permute-start | bytes 3145736 | tf_op jit(solution)/shard_map/ppermute | solution.py:67
  60.9 58.2 %collective-permute-start.8 = (bf16[1024,512]{1,0:T(8,128)(2,1)}, bf16[1024,512]{1,0:T(8,128)(2,1)}, u32[]{:S(2)}, u32[]{:S(2)}) collective-permute-start(bf16[1024,512]{1,0:T(8,128)(2,1)} %collective-permute-done.2), channel_id=1, source_target_pairs={{0,1},{1,0},{2,3},{3,2},{4,5},{5,4},{6,7},{7,6},{8,9},{9,8},{10,11... | collective-permute-start | bytes 3145736 | tf_op jit(solution)/shard_map/ppermute | solution.py:67
  82.1 40.0 %collective-permute-start.10 = (bf16[512,1024]{1,0:T(8,128)(2,1)}, bf16[512,1024]{1,0:T(8,128)(2,1)}, u32[]{:S(2)}, u32[]{:S(2)}) collective-permute-start(bf16[512,1024]{1,0:T(8,128)(2,1)} %collective-permute-done.4), channel_id=1, source_target_pairs={{0,1},{1,0},{2,3},{3,2},{4,5},{5,4},{6,7},{7,6},{8,9},{9,8},{10,11... | collective-permute-start | bytes 3145736 | tf_op jit(solution)/shard_map/ppermute | solution.py:67
  87.0 35.1 %collective-permute-start.9 = (bf16[1024,512]{1,0:T(8,128)(2,1)}, bf16[1024,512]{1,0:T(8,128)(2,1)}, u32[]{:S(2)}, u32[]{:S(2)}) collective-permute-start(bf16[1024,512]{1,0:T(8,128)(2,1)} %collective-permute-done.3), channel_id=1, source_target_pairs={{0,1},{1,0},{2,3},{3,2},{4,5},{5,4},{6,7},{7,6},{8,9},{9,8},{10,11... | collective-permute-start | bytes 3145736 | tf_op jit(solution)/shard_map/ppermute | solution.py:67
  128.7 19.0 %all-to-all-start.3 = ((bf16[4,144,1024]{2,1,0:T(8,128)(2,1)}), bf16[4,144,1024]{2,1,0:T(8,128)(2,1)S(1)}, u32[]{:S(2)}, u32[]{:S(2)}) async-start(bf16[4,144,1024]{2,1,0:T(8,128)(2,1)} %bitcast.110), calls=%async_computation.3 | async-start | bytes 2359296 | tf_op jit(solution)/shard_map/all_to_all | solution.py:127
  147.7 4.4 %copy-start.2 = (bf16[192,1,256]{2,0,1:T(8,128)(2,1)S(1)}, bf16[192,1,256]{2,0,1:T(8,128)(2,1)}, u32[]{:S(2)}) copy-start(bf16[192,1,256]{2,0,1:T(8,128)(2,1)} %get-tuple-element.5) | copy-start | bytes 294916
  147.7 4.4 %copy-start.3 = (bf16[192,1,256]{2,0,1:T(8,128)(2,1)S(1)}, bf16[192,1,256]{2,0,1:T(8,128)(2,1)}, u32[]{:S(2)}) copy-start(bf16[192,1,256]{2,0,1:T(8,128)(2,1)} %get-tuple-element.6) | copy-start | bytes 294916
  147.7 19.0 %all-to-all-start.1 = ((bf16[4,144,1024]{2,1,0:T(8,128)(2,1)}), bf16[4,144,1024]{2,1,0:T(8,128)(2,1)}, u32[]{:S(2)}, u32[]{:S(2)}) async-start(bf16[4,144,1024]{2,1,0:T(8,128)(2,1)} %bitcast.109), calls=%async_computation.1 | async-start | bytes 2359296 | tf_op jit(solution)/shard_map/all_to_all | solution.py:127
  152.4 0.7 copy-start.6
  155.3 19.5 %collective-permute-start.13 = (bf16[192,1024]{1,0:T(8,128)(2,1)S(1)}, bf16[192,1024]{1,0:T(8,128)(2,1)S(1)}, u32[]{:S(2)}, u32[]{:S(2)}) collective-permute-start(bf16[192,1024]{1,0:T(8,128)(2,1)S(1)} %fusion.2), channel_id=1, source_target_pairs={{0,4},{1,5},{2,6},{3,7},{4,0},{5,1},{6,2},{7,3},{8,12},{9,13},{10,... | collective-permute-start | bytes 1179656 | tf_op jit(solution)/shard_map/ppermute | solution.py:67
where the time goes:
time: 177 us; the launch traced here: 176 us
  matrix products  75.5 us (43%)
  waiting for transfers between devices  53.3 us (30%)
  starting transfers between devices  38.2 us (22%)
  other arithmetic  6.29 us (4%)
    dot_general x8, matrix products, ffn(): term = jnp.dot(hidden, down, preferred_element_type=jnp.float32)  42.2 us
    ppermute x12, waiting for transfers between devices, swap(): return lax.ppermute(value, 'tp', [(i, i ^ stride) for i in range(size)])  39 us
    dot_general x8, matrix products, ffn(): gate_part = jnp.dot(arrived, gate, preferred_element_type=jnp.float32)  24.5 us
    ppermute x12, starting transfers between devices, swap(): return lax.ppermute(value, 'tp', [(i, i ^ stride) for i in range(size)])  19.1 us
    all_to_all x4, starting transfers between devices, over_experts(): return lax.all_to_all(value, 'ep', split_axis=0, concat_axis=0, tiled=True)  16.1 us
    all_to_all x4, waiting for transfers between devices, over_experts(): return lax.all_to_all(value, 'ep', split_axis=0, concat_axis=0, tiled=True)  14.3 us
    dot_general x4, matrix products, combine(): lax.dot_general(part.astype(jnp.bfloat16), returned, dims, preferred_elem...  5.26 us
  transfers between devices with their start and end apart: 18, of which 6 were waited for; matrix products, arithmetic and copies ran while one was open for 43% of the time, Pallas kernels for 0%

commit v1 on v0

--- a/solution.py
+++ b/solution.py
@@ -1,6 +1,8 @@
 import jax
 import jax.numpy as jnp
 from jax import lax
+from jax.experimental import pallas as pl
+from jax.experimental.pallas import tpu as pltpu
 from jax.sharding import PartitionSpec as P
 
 epsilon = 1e-06
@@ -62,14 +64,42 @@
     return (mixed_groups.reshape(row_count, -1) * mixer_scale).astype(jnp.bfloat16)
 
 
-def swap(value, stride):
+CORES = 2
+
+
+def ring(value):
     size = lax.axis_size("tp")
-    return lax.ppermute(value, "tp", [(i, i ^ stride) for i in range(size)])
+    return lax.ppermute(value, "tp", [(i, (i + CORES) % size) for i in range(size)])
+
+
+def core_swap(value):
+    size = lax.axis_size("tp")
+    return lax.ppermute(value, "tp", [(i, i ^ 1) for i in range(size)])
+
+
+def is_direct(experts):
+    return experts <= 4
+
+
+def exchange(pieces):
+    count = len(pieces)
+    if is_direct(count):
+        received = {
+            m: lax.ppermute(pieces[m], "ep", [(i, i ^ m) for i in range(count)])
+            for m in reversed(range(1, count))
+        }
+        return [pieces[0]] + [received[m] for m in range(1, count)]
+    joined = lax.all_to_all(
+        jnp.stack(pieces), "ep", split_axis=0, concat_axis=0, tiled=True
+    )
+    return [joined[m] for m in range(count)]
 
 
 def route_table(routes, route_weight, experts, capacity):
     row_count, top_count = routes.shape
     named = routes.T
+    if is_direct(experts):
+        named = named ^ lax.axis_index("ep")
     member = jnp.zeros((experts, row_count), jnp.float32)
     expert_ids = jnp.arange(experts, dtype=jnp.int32)[:, None]
     for k in range(top_count):
@@ -91,40 +121,142 @@
     return jnp.concatenate([jnp.stack(slots), route_weight.T], axis=0)
 
 
-def slot_hits(table, top_count, slots):
-    ids = lax.broadcasted_iota(jnp.int32, (slots, table.shape[1]), 0).astype(jnp.float32)
-    return [table[k][None, :] == ids for k in range(top_count)]
-
-
-def dispatch(rows, table, top_count, slots):
-    hits = slot_hits(table, top_count, slots)
-    chosen = hits[0]
-    for hit in hits[1:]:
-        chosen = chosen | hit
-    return jnp.dot(
-        chosen.astype(jnp.bfloat16), rows, preferred_element_type=jnp.float32
-    ).astype(jnp.bfloat16)
-
-
-def combine(returned, table, top_count):
-    hits = slot_hits(table, top_count, returned.shape[0])
-    weight = jnp.zeros(hits[0].shape, jnp.float32)
-    for k in range(top_count):
-        weight = weight + jnp.where(hits[k], table[top_count + k][None, :], 0.0)
-    high = lax.reduce_precision(weight, 8, 7)
-    low = weight - high
-    dims = (((0,), (0,)), ((), ()))
-    parts = [
-        lax.dot_general(
-            part.astype(jnp.bfloat16), returned, dims, preferred_element_type=jnp.float32
-        )
-        for part in (high, low)
-    ]
-    return parts[0] + parts[1]
-
-
-def over_experts(value):
-    return lax.all_to_all(value, "ep", split_axis=0, concat_axis=0, tiled=True)
+def slot_hits(table_ref, top_count, first, capacity):
+    row_count = table_ref.shape[1]
+    ids = lax.broadcasted_iota(jnp.int32, (capacity, row_count), 0) + first
+    ids = ids.astype(jnp.float32)
+    return [table_ref[k : k + 1, :] == ids for k in range(top_count)]
+
+
+def dispatch(rows, table, experts, capacity):
+    top_count = table.shape[0] // 2
+
+    def kernel(rows_ref, table_ref, *out_refs):
+        for m, out_ref in enumerate(out_refs):
+            hits = slot_hits(table_ref, top_count, m * capacity, capacity)
+            chosen = jnp.zeros(hits[0].shape, jnp.float32)
+            for hit in hits:
+                chosen = chosen + jnp.where(hit, 1.0, 0.0)
+            out_ref[...] = jnp.dot(
+                chosen.astype(jnp.bfloat16),
+                rows_ref[...],
+                preferred_element_type=jnp.float32,
+            ).astype(jnp.bfloat16)
+
+    shape = jax.ShapeDtypeStruct((capacity, rows.shape[1]), jnp.bfloat16)
+    work = experts * capacity * rows.shape[0] * rows.shape[1]
+    return pl.pallas_call(
+        kernel,
+        out_shape=[shape] * experts,
+        cost_estimate=pl.CostEstimate(
+            flops=2 * work, transcendentals=0, bytes_accessed=2 * rows.size + 2 * experts * shape.size
+        ),
+        name="dispatch",
+    )(rows, table)
+
+
+def combine(pieces, table, incoming):
+    top_count = table.shape[0] // 2
+    capacity, width = pieces[0].shape
+    row_count = table.shape[1]
+    extra = [] if incoming is None else [incoming]
+
+    def kernel(table_ref, *refs):
+        out_ref = refs[-1]
+        total = jnp.zeros((row_count, width), jnp.float32)
+        if extra:
+            total = refs[-2][...].astype(jnp.float32)
+        for m in range(len(pieces)):
+            hits = slot_hits(table_ref, top_count, m * capacity, capacity)
+            weight = jnp.zeros(hits[0].shape, jnp.float32)
+            for k, hit in enumerate(hits):
+                weight = weight + jnp.where(hit, table_ref[top_count + k : top_count + k + 1, :], 0.0)
+            high = weight.astype(jnp.bfloat16)
+            low = (weight - high.astype(jnp.float32)).astype(jnp.bfloat16)
+            for part in (high, low):
+                total = total + lax.dot_general(
+                    part,
+                    refs[m][...],
+                    (((0,), (0,)), ((), ())),
+                    preferred_element_type=jnp.float32,
+                )
+        out_ref[...] = total.astype(jnp.bfloat16)
+
+    work = len(pieces) * capacity * row_count * width
+    return pl.pallas_call(
+        kernel,
+        out_shape=jax.ShapeDtypeStruct((row_count, width), jnp.bfloat16),
+        cost_estimate=pl.CostEstimate(
+            flops=4 * work, transcendentals=0, bytes_accessed=2 * (len(pieces) * capacity + 2 * row_count) * width
+        ),
+        name="combine",
+    )(table, *pieces, *extra)
+
+
+def ffn(pieces, shards):
+    count = len(pieces)
+    capacity, width = pieces[0].shape
+    rows = count * capacity
+    hidden_width = shards[0][0].shape[1]
+    tile = min(256, hidden_width)
+    steps = hidden_width // tile
+    n_shards = len(shards)
+
+    def kernel(*refs):
+        piece_refs = refs[:count]
+        weight_refs = refs[count : count + 3 * n_shards]
+        out_refs = refs[count + 3 * n_shards : 2 * count + 3 * n_shards]
+        rows_ref, sum_ref = refs[-2:]
+        step = pl.program_id(0)
+
+        @pl.when(step == 0)
+        def _():
+            for m in range(count):
+                rows_ref[m * capacity : (m + 1) * capacity, :] = piece_refs[m][...]
+
+        values = rows_ref[...]
+        term = None
+        for n in range(n_shards):
+            gate_ref, up_ref, down_ref = weight_refs[3 * n : 3 * n + 3]
+            gate = jnp.dot(values, gate_ref[...], preferred_element_type=jnp.float32)
+            up = jnp.dot(values, up_ref[...], preferred_element_type=jnp.float32)
+            hidden = (gate / (1.0 + jnp.exp(-gate)) * up).astype(jnp.bfloat16)
+            part = jnp.dot(hidden, down_ref[...], preferred_element_type=jnp.float32)
+            term = part if term is None else term + part
+
+        @pl.when(step == 0)
+        def _():
+            sum_ref[...] = term
+
+        @pl.when(step > 0)
+        def _():
+            sum_ref[...] += term
+
+        @pl.when(step == steps - 1)
+        def _():
+            for m in range(count):
+                out_refs[m][...] = sum_ref[m * capacity : (m + 1) * capacity, :].astype(jnp.bfloat16)
+
+    whole = pl.BlockSpec((capacity, width), lambda j: (0, 0))
+    across = pl.BlockSpec((width, tile), lambda j: (0, j))
+    along = pl.BlockSpec((tile, width), lambda j: (j, 0))
+    work = rows * width * hidden_width * n_shards
+    return pl.pallas_call(
+        kernel,
+        grid=(steps,),
+        in_specs=[whole] * count + [across, across, along] * n_shards,
+        out_specs=[whole] * count,
+        out_shape=[jax.ShapeDtypeStruct((capacity, width), jnp.bfloat16)] * count,
+        scratch_shapes=[
+            pltpu.VMEM((rows, width), jnp.bfloat16),
+            pltpu.VMEM((rows, width), jnp.float32),
+        ],
+        cost_estimate=pl.CostEstimate(
+            flops=6 * work, transcendentals=rows * hidden_width * n_shards,
+            bytes_accessed=4 * rows * width + 6 * width * hidden_width * n_shards,
+        ),
+        name="ffn",
+    )(*pieces, *(w for shard in shards for w in shard))
 
 
 def on_device(
@@ -143,42 +275,33 @@
     row_count, top_count = routes.shape
     experts = lax.axis_size("ep") * w_gate.shape[0]
     capacity = 3 * top_count * row_count // (2 * experts)
-    slots = experts * capacity
-    half = lax.axis_size("tp") // 2
+    capacity = -(-capacity // 16) * 16
+    chips = lax.axis_size("tp") // CORES
 
     normed = normalize(expert_input, expert_gain)
-    far_rows = swap(normed, half)
-
-    shards = [(w_gate[0], w_up[0], w_down[0])]
-    stride = half // 2
-    while stride:
-        shards = shards + [tuple(swap(w, stride) for w in shard) for shard in shards]
-        stride //= 2
+    shard = (w_gate[0], w_up[0], w_down[0])
+    shards = [shard, tuple(core_swap(w) for w in shard)]
 
     table = route_table(routes, route_weight, experts, capacity)
-    far_table = swap(table, half)
-    near = over_experts(dispatch(normed, table, top_count, slots))
-    far = over_experts(dispatch(far_rows, far_table, top_count, slots))
-
-    def ffn(arrived):
-        total = None
-        for gate, up, down in shards:
-            gate_part = jnp.dot(arrived, gate, preferred_element_type=jnp.float32)
-            up_part = jnp.dot(arrived, up, preferred_element_type=jnp.float32)
-            hidden = (jax.nn.silu(gate_part) * up_part).astype(jnp.bfloat16)
-            term = jnp.dot(hidden, down, preferred_element_type=jnp.float32)
-            total = term if total is None else total + term
-        return total.astype(jnp.bfloat16)
-
-    far_back = over_experts(ffn(far))
-    far_sum = combine(far_back, far_table, top_count).astype(jnp.bfloat16)
-    far_sum = swap(far_sum, half)
-    near_back = over_experts(ffn(near))
-    near_sum = combine(near_back, table, top_count)
-    expert_out = (near_sum + far_sum.astype(jnp.float32)).astype(jnp.bfloat16)
+    blocks, tables = [normed], [table]
+    for _ in range(1, chips):
+        blocks.append(ring(blocks[-1]))
+        tables.append(ring(tables[-1]))
+
+    back = []
+    for n in range(chips):
+        arrived = exchange(dispatch(blocks[n], tables[n], experts, capacity))
+        served = ffn(arrived, shards)
+        back.append(exchange(served))
+
+    total = None
+    for n in list(range(1, chips)) + [0]:
+        total = combine(back[n], tables[n], total)
+        if n:
+            total = ring(total)
 
     mixer_out = mixer(mixer_input, mixer_gain, group_weight, mixer_scale)
-    return (mixer_out, expert_out)
+    return (mixer_out, total)
 
 
 def solution(mesh):

time: 177 us -> 165 us (0.932)
  matrix products: 75.5 us -> 0.4 us
  Pallas kernels: 0 us -> 54.4 us
  starting transfers between devices: 38.2 us -> 63.1 us
  waiting for transfers between devices: 53.3 us -> 35.4 us
  local copies, waits for them, and re-layouts: 1.48 us -> 4.5 us
    dot_general x22 -> x0, matrix products: 75.1 us -> none  [the longest x8 42.2 us: ffn(): term = jnp.dot(hidden, down, preferred_element_type=jnp.float32)]
    pallas_call x0 -> x12, Pallas kernels: none -> 54.4 us  [the longest x4 32.7 us: ffn(): pl.pallas_call(kernel, grid=(steps,), in_specs=[whole] * count + [across,...]
    ppermute x12 -> x36, starting transfers between devices: 19.1 us -> 60.6 us  [the longest x24 49.5 us: exchange(): lax.ppermute(pieces[m], 'ep', [(i, i ^ m) for i in range(count)])]
    all_to_all x4 -> x0, starting transfers between devices: 16.1 us -> none  [over_experts(): return lax.all_to_all(value, 'ep', split_axis=0, concat_axis=0, tiled=True)]
    all_to_all x4 -> x0, waiting for transfers between devices: 14.3 us -> none  [over_experts(): return lax.all_to_all(value, 'ep', split_axis=0, concat_axis=0, tiled=True)]
    ppermute x12 -> x36, waiting for transfers between devices: 39 us -> 31.8 us  [the longest x24 20.2 us: exchange(): lax.ppermute(pieces[m], 'ep', [(i, i ^ m) for i in range(count)])]
    unnamed x14 -> x76, local copies, waits for them, and re-layouts: 0.62 us -> 4.41 us
    ppermute x1, waiting for transfers between devices: 0.01 us -> 2.77 us  [padded_2(): after = lax.ppermute(leading, axis, down)]
  transfers between devices with their start and end apart: 18 -> 38, of which waited for: 6 -> 10; matrix products, arithmetic and copies ran while one was open for 43% -> 2% of each run, Pallas kernels for 0% -> 31%
where the time goes in v1:
time: 165 us; the launch traced here: 163 us
  starting transfers between devices  63.1 us (38%)
  Pallas kernels  54.4 us (33%)
  waiting for transfers between devices  35.4 us (21%)
  other arithmetic  4.57 us (3%)
  local copies, waits for them, and re-layouts  4.5 us (3%)
    ppermute x24, starting transfers between devices, exchange(): lax.ppermute(pieces[m], 'ep', [(i, i ^ m) for i in range(count)])  49.5 us
    pallas_call x4, Pallas kernels, ffn(): pl.pallas_call(kernel, grid=(steps,), in_specs=[whole] * count + [across,...  32.7 us
    ppermute x24, waiting for transfers between devices, exchange(): lax.ppermute(pieces[m], 'ep', [(i, i ^ m) for i in range(count)])  20.2 us
    pallas_call x4, Pallas kernels, combine(): pl.pallas_call(kernel, out_shape=jax.ShapeDtypeStruct((row_count, width),...  12.5 us
    ppermute x9, waiting for transfers between devices, ring(): lax.ppermute(value, 'tp', [(i, (i + CORES) % size) for i in range(size)])  11.6 us
    ppermute x9, starting transfers between devices, ring(): lax.ppermute(value, 'tp', [(i, (i + CORES) % size) for i in range(size)])  10.6 us
    pallas_call x4, Pallas kernels, dispatch(): pl.pallas_call(kernel, out_shape=[shape] * experts, cost_estimate=pl.Cost...  9.16 us
    unnamed x76, local copies, waits for them, and re-layouts  4.41 us
  transfers between devices with their start and end apart: 38, of which 10 were waited for; matrix products, arithmetic and copies ran while one was open for 2% of the time, Pallas kernels for 31%

profile of v1, /device:TPU:0, one launch (start us, length us, event | category | flops | bytes accessed | tf_op | source)
XLA Modules:
  0.0 163.5 jit_solution(5724004003699944471)
XLA Ops:
  0.7 0.8 xor_bitcast_fusion
  1.6 0.7 pad_maximum_fusion.table_ref
  2.3 3.1 %collective-permute-start.11 = (f32[4,192]{1,0:T(4,128)S(1)}, f32[4,192]{1,0:T(4,128)S(1)}, u32[]{:S(2)}, u32[]{:S(2)}) collective-permute-start(f32[4,192]{1,0:T(4,128)S(1)} %pad_maximum_fusion.table_ref), channel_id=1, source_target_pairs={{0,2},{1,3},{2,4},{3,5},{4,6},{5,7},{6,0},{7,1},{8,10},{9,11},{10,... | collective-permute-start | bytes 9224 | tf_op jit(solution)/shard_map/ppermute | solution.py:72
  5.4 1.2 fusion.3
  6.6 0.2 fusion.5.rows_ref
  6.8 1.6 collective-permute-start.14
  8.4 0.5 collective-permute-start.6
  9.1 0.5 copy-done.18
  9.8 1.6 collective-permute-start.12
  11.5 7.8 %collective-permute-done.14.rows_ref = bf16[192,1024]{1,0:T(8,128)(2,1)S(1)} collective-permute-done((bf16[192,1024]{1,0:T(8,128)(2,1)S(1)}, bf16[192,1024]{1,0:T(8,128)(2,1)S(1)}, u32[]{:S(2)}, u32[]{:S(2)}) %collective-permute-start.14) | collective-permute-done | bytes 393248 | tf_op jit(solution)/shard_map/ppermute | solution.py:72
  19.3 1.3 collective-permute-start
  20.6 0.8 collective-permute-done
  21.4 1.3 collective-permute-start.1
  22.7 2.2 %dispatch.7 = (bf16[144,1024]{1,0:T(8,128)(2,1)}, bf16[144,1024]{1,0:T(8,128)(2,1)}, bf16[144,1024]{1,0:T(8,128)(2,1)}, bf16[144,1024]{1,0:T(8,128)(2,1)}) custom-call(bf16[192,1024]{1,0:T(8,128)(2,1)} %copy-done.25, f32[4,192]{1,0:T(4,128)} %copy-done.37), custom_call_target="tpu_custom_call" | custom-call | flops 226492416 | bytes 1572864 | tf_op jit(solution)/shard_map/dispatch/pallas_call | solution.py:148
  25.0 2.8 %collective-permute-done.1 = bf16[8,1024]{1,0:T(8,128)(2,1)S(1)} collective-permute-done((bf16[8,1024]{1,0:T(8,128)(2,1)S(1)}, bf16[8,1024]{1,0:T(8,128)(2,1)S(1)}, u32[]{:S(2)}, u32[]{:S(2)}) %collective-permute-start.1) | collective-permute-done | bytes 16416 | tf_op jit(solution)/shard_map/ppermute | solution.py:19
  27.8 6.7 %collective-permute-start.29 = (bf16[144,1024]{1,0:T(8,128)(2,1)}, bf16[144,1024]{1,0:T(8,128)(2,1)S(1)}, u32[]{:S(2)}, u32[]{:S(2)}) collective-permute-start(bf16[144,1024]{1,0:T(8,128)(2,1)} %get-tuple-element.59), channel_id=1, source_target_pairs={{0,8},{8,0},{16,24},{24,16},{1,9},{9,1},{17,25},{25,17},{2,10},{10... | collective-permute-start | bytes 884744 | tf_op jit(solution)/shard_map/ppermute | solution.py:88
  34.5 7.9 %collective-permute-done.29.refs_1_ = bf16[144,1024]{1,0:T(8,128)(2,1)S(1)} collective-permute-done((bf16[144,1024]{1,0:T(8,128)(2,1)}, bf16[144,1024]{1,0:T(8,128)(2,1)S(1)}, u32[]{:S(2)}, u32[]{:S(2)}) %collective-permute-start.29) | collective-permute-done | bytes 294944 | tf_op jit(solution)/shard_map/ppermute | solution.py:88
  42.4 2.7 %collective-permute-start.30 = (bf16[144,1024]{1,0:T(8,128)(2,1)}, bf16[144,1024]{1,0:T(8,128)(2,1)S(1)}, u32[]{:S(2)}, u32[]{:S(2)}) collective-permute-start(bf16[144,1024]{1,0:T(8,128)(2,1)} %get-tuple-element.60), channel_id=1, source_target_pairs={{0,16},{8,24},{16,0},{24,8},{1,17},{9,25},{17,1},{25,9},{2,18},{10... | collective-permute-start | bytes 884744 | tf_op jit(solution)/shard_map/ppermute | solution.py:88
  45.0 0.5 collective-permute-start.31
  45.6 2.3 %dispatch.4 = (bf16[144,1024]{1,0:T(8,128)(2,1)}, bf16[144,1024]{1,0:T(8,128)(2,1)}, bf16[144,1024]{1,0:T(8,128)(2,1)}, bf16[144,1024]{1,0:T(8,128)(2,1)}) custom-call(bf16[192,1024]{1,0:T(8,128)(2,1)} %copy-done.3, f32[4,192]{1,0:T(4,128)} %copy-done.16), custom_call_target="tpu_custom_call" | custom-call | flops 226492416 | bytes 1572864 | tf_op jit(solution)/shard_map/dispatch/pallas_call | solution.py:148
  48.0 2.3 %dispatch.6 = (bf16[144,1024]{1,0:T(8,128)(2,1)}, bf16[144,1024]{1,0:T(8,128)(2,1)}, bf16[144,1024]{1,0:T(8,128)(2,1)}, bf16[144,1024]{1,0:T(8,128)(2,1)}) custom-call(bf16[192,1024]{1,0:T(8,128)(2,1)} %copy-done.23, f32[4,192]{1,0:T(4,128)} %copy-done.21), custom_call_target="tpu_custom_call" | custom-call | flops 226492416 | bytes 1572864 | tf_op jit(solution)/shard_map/dispatch/pallas_call | solution.py:148
  50.3 8.0 %collective-permute-done.30.refs_2_ = bf16[144,1024]{1,0:T(8,128)(2,1)S(1)} collective-permute-done((bf16[144,1024]{1,0:T(8,128)(2,1)}, bf16[144,1024]{1,0:T(8,128)(2,1)S(1)}, u32[]{:S(2)}, u32[]{:S(2)}) %collective-permute-start.30) | collective-permute-done | bytes 294944 | tf_op jit(solution)/shard_map/ppermute | solution.py:88
  58.4 0.9 collective-permute-start.23
  59.3 1.5 collective-permute-start.24
  60.8 1.1 collective-permute-start.25
  62.0 8.2 %ffn.7 = (bf16[144,1024]{1,0:T(8,128)(2,1)}, bf16[144,1024]{1,0:T(8,128)(2,1)}, bf16[144,1024]{1,0:T(8,128)(2,1)}, bf16[144,1024]{1,0:T(8,128)(2,1)}) custom-call(bf16[144,1024]{1,0:T(8,128)(2,1)} %get-tuple-element.58.refs_0_, bf16[144,1024]{1,0:T(8,128)(2,1)} %copy-done.28, bf16[144,1024]{1,0:T(8,128)(2,1)} %copy-done.29, bf16[144,1024]{1,0:T(8,128)(2,1)} %copy-done.30, ...), custom_call_target="tpu_custom_call" | custom-call | flops 3623878656 | bytes 8650752 | tf_op jit(solution)/shard_map/ffn/pallas_call | solution.py:244
  70.2 0.9 collective-permute-start.32
  71.2 2.9 %collective-permute-start.33 = (bf16[144,1024]{1,0:T(8,128)(2,1)}, bf16[144,1024]{1,0:T(8,128)(2,1)S(1)}, u32[]{:S(2)}, u32[]{:S(2)}) collective-permute-start(bf16[144,1024]{1,0:T(8,128)(2,1)} %get-tuple-element.64), channel_id=1, source_target_pairs={{0,16},{8,24},{16,0},{24,8},{1,17},{9,25},{17,1},{25,9},{2,18},{10... | collective-permute-start | bytes 884744 | tf_op jit(solution)/shard_map/ppermute | solution.py:88
  74.1 1.7 %collective-permute-done.25.refs_3_ = bf16[144,1024]{1,0:T(8,128)(2,1)S(1)} collective-permute-done((bf16[144,1024]{1,0:T(8,128)(2,1)}, bf16[144,1024]{1,0:T(8,128)(2,1)S(1)}, u32[]{:S(2)}, u32[]{:S(2)}) %collective-permute-start.25) | collective-permute-done | bytes 294944 | tf_op jit(solution)/shard_map/ppermute | solution.py:88
  75.8 0.8 collective-permute-start.34
  76.6 8.2 %ffn.6 = (bf16[144,1024]{1,0:T(8,128)(2,1)}, bf16[144,1024]{1,0:T(8,128)(2,1)}, bf16[144,1024]{1,0:T(8,128)(2,1)}, bf16[144,1024]{1,0:T(8,128)(2,1)}) custom-call(bf16[144,1024]{1,0:T(8,128)(2,1)} %get-tuple-element.50.refs_0_, bf16[144,1024]{1,0:T(8,128)(2,1)} %copy-done.31, bf16[144,1024]{1,0:T(8,128)(2,1)} %copy-done.33, bf16[144,1024]{1,0:T(8,128)(2,1)} %copy-done.35, ...), custom_call_target="tpu_custom_call" | custom-call | flops 3623878656 | bytes 8650752 | tf_op jit(solution)/shard_map/ffn/pallas_call | solution.py:244
  84.8 1.3 collective-permute-start.26
  86.1 1.4 collective-permute-start.27
  87.6 1.0 collective-permute-done.34.refs_3_
  88.5 4.4 %collective-permute-start.28 = (bf16[144,1024]{1,0:T(8,128)(2,1)}, bf16[144,1024]{1,0:T(8,128)(2,1)S(1)}, u32[]{:S(2)}, u32[]{:S(2)}) collective-permute-start(bf16[144,1024]{1,0:T(8,128)(2,1)} %get-tuple-element.57), channel_id=1, source_target_pairs={{0,24},{8,16},{16,8},{24,0},{1,25},{9,17},{17,9},{25,1},{2,26},{10... | collective-permute-start | bytes 884744 | tf_op jit(solution)/shard_map/ppermute | solution.py:88
  93.0 3.0 %combine.4 = bf16[192,1024]{1,0:T(8,128)(2,1)} custom-call(f32[4,192]{1,0:T(4,128)} %copy-done.37, bf16[144,1024]{1,0:T(8,128)(2,1)} %get-tuple-element.62.refs_0_, bf16[144,1024]{1,0:T(8,128)(2,1)} %copy-done.34, bf16[144,1024]{1,0:T(8,128)(2,1)} %copy-done.36, bf16[144,1024]{1,0:T(8,128)(2,1)} %collective-permute-done.34.refs_3_), custom_call_target="tpu_custom_call" | custom-call | flops 452984832 | bytes 1966080 | tf_op jit(solution)/shard_map/combine/pallas_call | solution.py:186
  96.0 0.2 fusion.31
  96.3 0.3 copy-done.20
  96.6 2.3 %dispatch.5 = (bf16[144,1024]{1,0:T(8,128)(2,1)}, bf16[144,1024]{1,0:T(8,128)(2,1)}, bf16[144,1024]{1,0:T(8,128)(2,1)}, bf16[144,1024]{1,0:T(8,128)(2,1)}) custom-call(bf16[192,1024]{1,0:T(8,128)(2,1)} %collective-permute-done.16.rows_ref, f32[4,192]{1,0:T(4,128)} %copy-done.20), custom_call_target="tpu_custom_call" | custom-call | flops 226492416 | bytes 1572864 | tf_op jit(solution)/shard_map/dispatch/pallas_call | solution.py:148
  98.9 1.4 collective-permute-start.18
  100.3 7.3 %collective-permute-start.19 = (bf16[144,1024]{1,0:T(8,128)(2,1)}, bf16[144,1024]{1,0:T(8,128)(2,1)}, u32[]{:S(2)}, u32[]{:S(2)}) collective-permute-start(bf16[144,1024]{1,0:T(8,128)(2,1)} %get-tuple-element.45), channel_id=1, source_target_pairs={{0,24},{8,16},{16,8},{24,0},{1,25},{9,17},{17,9},{25,1},{2,26},{10... | collective-permute-start | bytes 884744 | tf_op jit(solution)/shard_map/ppermute | solution.py:88
  107.6 0.3 fusion.28
  108.0 0.5 copy-done.27
  108.6 0.4 collective-permute-start.3
  109.0 3.2 %combine.5 = bf16[192,1024]{1,0:T(8,128)(2,1)} custom-call(f32[4,192]{1,0:T(4,128)} %copy-done.21, bf16[144,1024]{1,0:T(8,128)(2,1)} %get-tuple-element.54.refs_0_, bf16[144,1024]{1,0:T(8,128)(2,1)} %copy-done.7, bf16[144,1024]{1,0:T(8,128)(2,1)} %copy-done.8, bf16[144,1024]{1,0:T(8,128)(2,1)} %copy-done.9, bf16[192,1024]{1,0:T(8,128)(2,1)} %copy-done.5), custom_call_target="tpu_custom_call" | custom-call | flops 452984832 | bytes 1966080 | tf_op jit(solution)/shard_map/combine/pallas_call | solution.py:186
  112.2 2.6 %collective-permute-start.4 = (bf16[144,1024]{1,0:T(8,128)(2,1)S(1)}, bf16[144,1024]{1,0:T(8,128)(2,1)S(1)}, u32[]{:S(2)}, u32[]{:S(2)}) collective-permute-start(bf16[144,1024]{1,0:T(8,128)(2,1)S(1)} %copy-done.26), channel_id=1, source_target_pairs={{0,24},{8,16},{16,8},{24,0},{1,25},{9,17},{17,9},{25,1},{2,26},{10... | collective-permute-start | bytes 884744 | tf_op jit(solution)/shard_map/ppermute | solution.py:88
  114.8 1.4 collective-permute-done.19.refs_3_
  116.2 8.2 %ffn.5 = (bf16[144,1024]{1,0:T(8,128)(2,1)}, bf16[144,1024]{1,0:T(8,128)(2,1)}, bf16[144,1024]{1,0:T(8,128)(2,1)}, bf16[144,1024]{1,0:T(8,128)(2,1)}) custom-call(bf16[144,1024]{1,0:T(8,128)(2,1)} %get-tuple-element.42.refs_0_, bf16[144,1024]{1,0:T(8,128)(2,1)} %collective-permute-done.17.refs_1_, bf16[144,1024]{1,0:T(8,128)(2,1)} %collective-permute-done.18.refs_2_, ...), custom_call_target="tpu_custom_call" | custom-call | flops 3623878656 | bytes 8650752 | tf_op jit(solution)/shard_map/ffn/pallas_call | solution.py:244
  124.4 3.6 %collective-permute-start.20 = (bf16[144,1024]{1,0:T(8,128)(2,1)}, bf16[144,1024]{1,0:T(8,128)(2,1)S(1)}, u32[]{:S(2)}, u32[]{:S(2)}) collective-permute-start(bf16[144,1024]{1,0:T(8,128)(2,1)} %get-tuple-element.47), channel_id=1, source_target_pairs={{0,8},{8,0},{16,24},{24,16},{1,9},{9,1},{17,25},{25,17},{2,10},{10... | collective-permute-start | bytes 884744 | tf_op jit(solution)/shard_map/ppermute | solution.py:88
  128.1 1.4 collective-permute-start.21
  129.5 3.9 %collective-permute-start.22 = (bf16[144,1024]{1,0:T(8,128)(2,1)}, bf16[144,1024]{1,0:T(8,128)(2,1)S(1)}, u32[]{:S(2)}, u32[]{:S(2)}) collective-permute-start(bf16[144,1024]{1,0:T(8,128)(2,1)} %get-tuple-element.49), channel_id=1, source_target_pairs={{0,24},{8,16},{16,8},{24,0},{1,25},{9,17},{17,9},{25,1},{2,26},{10... | collective-permute-start | bytes 884744 | tf_op jit(solution)/shard_map/ppermute | solution.py:88
  133.4 0.7 copy-done.32
  134.1 8.2 %ffn.4 = (bf16[144,1024]{1,0:T(8,128)(2,1)}, bf16[144,1024]{1,0:T(8,128)(2,1)}, bf16[144,1024]{1,0:T(8,128)(2,1)}, bf16[144,1024]{1,0:T(8,128)(2,1)}) custom-call(bf16[144,1024]{1,0:T(8,128)(2,1)} %get-tuple-element.34.refs_0_, bf16[144,1024]{1,0:T(8,128)(2,1)} %collective-permute-done.2.refs_1_, bf16[144,1024]{1,0:T(8,128)(2,1)} %collective-permute-done.3.refs_2_, ...), custom_call_target="tpu_custom_call" | custom-call | flops 3623878656 | bytes 8650752 | tf_op jit(solution)/shard_map/ffn/pallas_call | solution.py:244
  142.3 2.5 %collective-permute-start.8 = (bf16[144,1024]{1,0:T(8,128)(2,1)}, bf16[144,1024]{1,0:T(8,128)(2,1)S(1)}, u32[]{:S(2)}, u32[]{:S(2)}) collective-permute-start(bf16[144,1024]{1,0:T(8,128)(2,1)} %get-tuple-element.39), channel_id=1, source_target_pairs={{0,8},{8,0},{16,24},{24,16},{1,9},{9,1},{17,25},{25,17},{2,10},{10... | collective-permute-start | bytes 884744 | tf_op jit(solution)/shard_map/ppermute | solution.py:88
  144.8 0.9 collective-permute-start.9
  145.8 0.7 copy-done.14
  146.6 3.2 %combine.6 = bf16[192,1024]{1,0:T(8,128)(2,1)} custom-call(f32[4,192]{1,0:T(4,128)} %copy-done.20, bf16[144,1024]{1,0:T(8,128)(2,1)} %get-tuple-element.46.refs_0_, bf16[144,1024]{1,0:T(8,128)(2,1)} %copy-done.10, bf16[144,1024]{1,0:T(8,128)(2,1)} %copy-done.12, bf16[144,1024]{1,0:T(8,128)(2,1)} %copy-done.14, bf16[192,1024]{1,0:T(8,128)(2,1)} %copy-done.4), custom_call_target="tpu_custom_call" | custom-call | flops 452984832 | bytes 1966080 | tf_op jit(solution)/shard_map/combine/pallas_call | solution.py:186
  149.8 4.2 %collective-permute-start.37 = (bf16[192,1024]{1,0:T(8,128)(2,1)}, bf16[192,1024]{1,0:T(8,128)(2,1)S(1)}, u32[]{:S(2)}, u32[]{:S(2)}) collective-permute-start(bf16[192,1024]{1,0:T(8,128)(2,1)} %combine.6), channel_id=1, source_target_pairs={{0,2},{1,3},{2,4},{3,5},{4,6},{5,7},{6,0},{7,1},{8,10},{9,11},{10,... | collective-permute-start | bytes 1179656 | tf_op jit(solution)/shard_map/ppermute | solution.py:72
  154.0 0.3 convolution_bitcast_fusion
  154.3 0.6 copy-done.19
  154.9 0.8 multiply_convert_fusion
  155.8 3.8 %collective-permute-done.37.refs_4_ = bf16[192,1024]{1,0:T(8,128)(2,1)S(1)} collective-permute-done((bf16[192,1024]{1,0:T(8,128)(2,1)}, bf16[192,1024]{1,0:T(8,128)(2,1)S(1)}, u32[]{:S(2)}, u32[]{:S(2)}) %collective-permute-start.37) | collective-permute-done | bytes 393248 | tf_op jit(solution)/shard_map/ppermute | solution.py:72
  159.6 0.7 copy-done.6
  160.3 3.1 %combine.7 = bf16[192,1024]{1,0:T(8,128)(2,1)} custom-call(f32[4,192]{1,0:T(4,128)} %copy-done.16, bf16[144,1024]{1,0:T(8,128)(2,1)} %get-tuple-element.38.refs_0_, bf16[144,1024]{1,0:T(8,128)(2,1)} %copy-done.13, bf16[144,1024]{1,0:T(8,128)(2,1)} %copy-done.15, bf16[144,1024]{1,0:T(8,128)(2,1)} %copy-done.11, bf16[192,1024]{1,0:T(8,128)(2,1)} %copy-done.6), custom_call_target="tpu_custom_call" | custom-call | flops 452984832 | bytes 1966080 | tf_op jit(solution)/shard_map/combine/pallas_call | solution.py:186
  (120 shorter events, 1.2 us)
Async XLA Ops:
  0.6 153.3 %copy-start = (bf16[4,256,256]{2,1,0:T(8,128)(2,1)S(1)}, bf16[4,256,256]{2,1,0:T(8,128)(2,1)}, u32[]{:S(2)}) copy-start(bf16[4,256,256]{2,1,0:T(8,128)(2,1)} %param.13) | copy-start | bytes 1572868
  0.6 6.0 %copy-start.1 = (bf16[192,1024]{1,0:T(8,128)(2,1)S(1)}, bf16[192,1024]{1,0:T(8,128)(2,1)}, u32[]{:S(2)}) copy-start(bf16[192,1024]{1,0:T(8,128)(2,1)} %param.15) | copy-start | bytes 1179652
  2.3 4.3 %copy-start.16 = (f32[4,192]{1,0:T(4,128)}, f32[4,192]{1,0:T(4,128)S(1)}, u32[]{:S(2)}) copy-start(f32[4,192]{1,0:T(4,128)S(1)} %pad_maximum_fusion.table_ref) | copy-start | bytes 9220
  2.3 7.5 %collective-permute-start.11 = (f32[4,192]{1,0:T(4,128)S(1)}, f32[4,192]{1,0:T(4,128)S(1)}, u32[]{:S(2)}, u32[]{:S(2)}) collective-permute-start(f32[4,192]{1,0:T(4,128)S(1)} %pad_maximum_fusion.table_ref), channel_id=1, source_target_pairs={{0,2},{1,3},{2,4},{3,5},{4,6},{5,7},{6,0},{7,1},{8,10},{9,11},{10,... | collective-permute-start | bytes 9224 | tf_op jit(solution)/shard_map/ppermute | solution.py:72
  5.4 1.2 copy-start.17
  6.6 2.3 %copy-start.2 = (bf16[192,1024]{1,0:T(8,128)(2,1)S(1)}, bf16[192,1024]{1,0:T(8,128)(2,1)}, u32[]{:S(2)}) copy-start(bf16[192,1024]{1,0:T(8,128)(2,1)} %param.11) | copy-start | bytes 1179652
  6.8 3.0 %copy-start.3 = (bf16[192,1024]{1,0:T(8,128)(2,1)}, bf16[192,1024]{1,0:T(8,128)(2,1)S(1)}, u32[]{:S(2)}) copy-start(bf16[192,1024]{1,0:T(8,128)(2,1)S(1)} %fusion.5.rows_ref) | copy-start | bytes 1179652
  6.8 12.5 %collective-permute-start.14 = (bf16[192,1024]{1,0:T(8,128)(2,1)S(1)}, bf16[192,1024]{1,0:T(8,128)(2,1)S(1)}, u32[]{:S(2)}, u32[]{:S(2)}) collective-permute-start(bf16[192,1024]{1,0:T(8,128)(2,1)S(1)} %fusion.5.rows_ref), channel_id=1, source_target_pairs={{0,2},{1,3},{2,4},{3,5},{4,6},{5,7},{6,0},{7,1},{8,10},{9,11},{10,... | collective-permute-start | bytes 1179656 | tf_op jit(solution)/shard_map/ppermute | solution.py:72
  8.4 50.9 %collective-permute-start.5 = (bf16[1024,512]{1,0:T(8,128)(2,1)}, bf16[1024,512]{1,0:T(8,128)(2,1)}, u32[]{:S(2)}, u32[]{:S(2)}) collective-permute-start(bf16[1024,512]{1,0:T(8,128)(2,1)} %bitcast.29), channel_id=1, source_target_pairs={{0,1},{1,0},{2,3},{3,2},{4,5},{5,4},{6,7},{7,6},{8,9},{9,8},{10,11... | collective-permute-start | bytes 3145736 | tf_op jit(solution)/shard_map/ppermute | solution.py:77
  8.4 52.4 %collective-permute-start.6 = (bf16[1024,512]{1,0:T(8,128)(2,1)}, bf16[1024,512]{1,0:T(8,128)(2,1)}, u32[]{:S(2)}, u32[]{:S(2)}) collective-permute-start(bf16[1024,512]{1,0:T(8,128)(2,1)} %bitcast.34), channel_id=1, source_target_pairs={{0,1},{1,0},{2,3},{3,2},{4,5},{5,4},{6,7},{7,6},{8,9},{9,8},{10,11... | collective-permute-start | bytes 3145736 | tf_op jit(solution)/shard_map/ppermute | solution.py:77
  8.9 53.0 %collective-permute-start.7 = (bf16[512,1024]{1,0:T(8,128)(2,1)}, bf16[512,1024]{1,0:T(8,128)(2,1)}, u32[]{:S(2)}, u32[]{:S(2)}) collective-permute-start(bf16[512,1024]{1,0:T(8,128)(2,1)} %bitcast.39), channel_id=1, source_target_pairs={{0,1},{1,0},{2,3},{3,2},{4,5},{5,4},{6,7},{7,6},{8,9},{9,8},{10,11... | collective-permute-start | bytes 3145736 | tf_op jit(solution)/shard_map/ppermute | solution.py:77
  9.8 9.5 %copy-start.37 = (f32[4,192]{1,0:T(4,128)}, f32[4,192]{1,0:T(4,128)S(1)}, u32[]{:S(2)}) copy-start(f32[4,192]{1,0:T(4,128)S(1)} %collective-permute-done.11.table_ref) | copy-start | bytes 9220
  9.8 9.5 %collective-permute-start.12 = (f32[4,192]{1,0:T(4,128)S(1)}, f32[4,192]{1,0:T(4,128)S(1)}, u32[]{:S(2)}, u32[]{:S(2)}) collective-permute-start(f32[4,192]{1,0:T(4,128)S(1)} %collective-permute-done.11.table_ref), channel_id=1, source_target_pairs={{0,2},{1,3},{2,4},{3,5},{4,6},{5,7},{6,0},{7,1},{8,10},{9,11},{10,... | collective-permute-start | bytes 9224 | tf_op jit(solution)/shard_map/ppermute | solution.py:72
  19.3 3.5 %copy-start.25 = (bf16[192,1024]{1,0:T(8,128)(2,1)}, bf16[192,1024]{1,0:T(8,128)(2,1)S(1)}, u32[]{:S(2)}) copy-start(bf16[192,1024]{1,0:T(8,128)(2,1)S(1)} %collective-permute-done.14.rows_ref) | copy-start | bytes 1179652
  19.3 25.8 %collective-permute-start.15 = (bf16[192,1024]{1,0:T(8,128)(2,1)S(1)}, bf16[192,1024]{1,0:T(8,128)(2,1)S(1)}, u32[]{:S(2)}, u32[]{:S(2)}) collective-permute-start(bf16[192,1024]{1,0:T(8,128)(2,1)S(1)} %collective-permute-done.14.rows_ref), channel_id=1, source_target_pairs={{0,2},{1,3},{2,4},{3,5},{4,6},{5,7},{6,0},{7,1},{8,10},{9,11},{10,... | collective-permute-start | bytes 1179656 | tf_op jit(solution)/shard_map/ppermute | solution.py:72
  19.3 5.7 %copy-start.21 = (f32[4,192]{1,0:T(4,128)}, f32[4,192]{1,0:T(4,128)S(1)}, u32[]{:S(2)}) copy-start(f32[4,192]{1,0:T(4,128)S(1)} %collective-permute-done.12.table_ref) | copy-start | bytes 9220
  19.3 2.1 %collective-permute-start = (bf16[8,1024]{1,0:T(8,128)(2,1)S(1)}, bf16[8,1024]{1,0:T(8,128)(2,1)S(1)}, u32[]{:S(2)}, u32[]{:S(2)}) collective-permute-start(bf16[8,1024]{1,0:T(8,128)(2,1)S(1)} %get-tuple-element.71), channel_id=1, source_target_pairs={{0,1},{1,2},{2,3},{3,4},{4,5},{5,6},{6,7},{7,8},{8,9},{9,10},{10,1... | collective-permute-start | bytes 49160 | tf_op jit(solution)/shard_map/ppermute | solution.py:18
  21.4 6.3 %collective-permute-start.1 = (bf16[8,1024]{1,0:T(8,128)(2,1)S(1)}, bf16[8,1024]{1,0:T(8,128)(2,1)S(1)}, u32[]{:S(2)}, u32[]{:S(2)}) collective-permute-start(bf16[8,1024]{1,0:T(8,128)(2,1)S(1)} %get-tuple-element.72), channel_id=1, source_target_pairs={{1,0},{2,1},{3,2},{4,3},{5,4},{6,5},{7,6},{8,7},{9,8},{10,9},{11,1... | collective-permute-start | bytes 49160 | tf_op jit(solution)/shard_map/ppermute | solution.py:19
  27.8 14.6 %collective-permute-start.29 = (bf16[144,1024]{1,0:T(8,128)(2,1)}, bf16[144,1024]{1,0:T(8,128)(2,1)S(1)}, u32[]{:S(2)}, u32[]{:S(2)}) collective-permute-start(bf16[144,1024]{1,0:T(8,128)(2,1)} %get-tuple-element.59), channel_id=1, source_target_pairs={{0,8},{8,0},{16,24},{24,16},{1,9},{9,1},{17,25},{25,17},{2,10},{10... | collective-permute-start | bytes 884744 | tf_op jit(solution)/shard_map/ppermute | solution.py:88
  42.4 5.5 %copy-start.28 = (bf16[144,1024]{1,0:T(8,128)(2,1)}, bf16[144,1024]{1,0:T(8,128)(2,1)S(1)}, u32[]{:S(2)}) copy-start(bf16[144,1024]{1,0:T(8,128)(2,1)S(1)} %collective-permute-done.29.refs_1_) | copy-start | bytes 884740
  42.4 16.0 %collective-permute-start.30 = (bf16[144,1024]{1,0:T(8,128)(2,1)}, bf16[144,1024]{1,0:T(8,128)(2,1)S(1)}, u32[]{:S(2)}, u32[]{:S(2)}) collective-permute-start(bf16[144,1024]{1,0:T(8,128)(2,1)} %get-tuple-element.60), channel_id=1, source_target_pairs={{0,16},{8,24},{16,0},{24,8},{1,17},{9,25},{17,1},{25,9},{2,18},{10... | collective-permute-start | bytes 884744 | tf_op jit(solution)/shard_map/ppermute | solution.py:88
  45.0 2.9 %copy-start.23 = (bf16[192,1024]{1,0:T(8,128)(2,1)}, bf16[192,1024]{1,0:T(8,128)(2,1)S(1)}, u32[]{:S(2)}) copy-start(bf16[192,1024]{1,0:T(8,128)(2,1)S(1)} %collective-permute-done.15.rows_ref) | copy-start | bytes 1179652
  45.0 13.3 %collective-permute-start.31 = (bf16[144,1024]{1,0:T(8,128)(2,1)}, bf16[144,1024]{1,0:T(8,128)(2,1)S(1)}, u32[]{:S(2)}, u32[]{:S(2)}) collective-permute-start(bf16[144,1024]{1,0:T(8,128)(2,1)} %get-tuple-element.61), channel_id=1, source_target_pairs={{0,24},{8,16},{16,8},{24,0},{1,25},{9,17},{17,9},{25,1},{2,26},{10... | collective-permute-start | bytes 884744 | tf_op jit(solution)/shard_map/ppermute | solution.py:88
  48.0 10.4 %copy-start.22 = (f32[4,192]{1,0:T(4,128)S(1)}, f32[4,192]{1,0:T(4,128)}, u32[]{:S(2)}) copy-start(f32[4,192]{1,0:T(4,128)} %copy-done.21) | copy-start | bytes 9220
  48.0 13.9 %copy-start.24 = (bf16[192,1024]{1,0:T(8,128)(2,1)S(1)}, bf16[192,1024]{1,0:T(8,128)(2,1)}, u32[]{:S(2)}) copy-start(bf16[192,1024]{1,0:T(8,128)(2,1)} %copy-done.23) | copy-start | bytes 1179652
  58.4 3.6 %copy-start.29 = (bf16[144,1024]{1,0:T(8,128)(2,1)}, bf16[144,1024]{1,0:T(8,128)(2,1)S(1)}, u32[]{:S(2)}) copy-start(bf16[144,1024]{1,0:T(8,128)(2,1)S(1)} %collective-permute-done.30.refs_2_) | copy-start | bytes 884740
  58.4 37.6 %collective-permute-start.13 = (f32[4,192]{1,0:T(4,128)S(1)}, f32[4,192]{1,0:T(4,128)S(1)}, u32[]{:S(2)}, u32[]{:S(2)}) collective-permute-start(f32[4,192]{1,0:T(4,128)S(1)} %copy-done.22), channel_id=1, source_target_pairs={{0,2},{1,3},{2,4},{3,5},{4,6},{5,7},{6,0},{7,1},{8,10},{9,11},{10,... | collective-permute-start | bytes 9224 | tf_op jit(solution)/shard_map/ppermute | solution.py:72
  58.4 3.6 %copy-start.30 = (bf16[144,1024]{1,0:T(8,128)(2,1)}, bf16[144,1024]{1,0:T(8,128)(2,1)S(1)}, u32[]{:S(2)}) copy-start(bf16[144,1024]{1,0:T(8,128)(2,1)S(1)} %collective-permute-done.31.refs_3_) | copy-start | bytes 884740
  58.4 11.8 %collective-permute-start.23 = (bf16[144,1024]{1,0:T(8,128)(2,1)}, bf16[144,1024]{1,0:T(8,128)(2,1)S(1)}, u32[]{:S(2)}, u32[]{:S(2)}) collective-permute-start(bf16[144,1024]{1,0:T(8,128)(2,1)} %get-tuple-element.51), channel_id=1, source_target_pairs={{0,8},{8,0},{16,24},{24,16},{1,9},{9,1},{17,25},{25,17},{2,10},{10... | collective-permute-start | bytes 884744 | tf_op jit(solution)/shard_map/ppermute | solution.py:88
  59.3 11.9 %collective-permute-start.24 = (bf16[144,1024]{1,0:T(8,128)(2,1)}, bf16[144,1024]{1,0:T(8,128)(2,1)S(1)}, u32[]{:S(2)}, u32[]{:S(2)}) collective-permute-start(bf16[144,1024]{1,0:T(8,128)(2,1)} %get-tuple-element.52), channel_id=1, source_target_pairs={{0,16},{8,24},{16,0},{24,8},{1,17},{9,25},{17,1},{25,9},{2,18},{10... | collective-permute-start | bytes 884744 | tf_op jit(solution)/shard_map/ppermute | solution.py:88
  60.8 14.9 %collective-permute-start.25 = (bf16[144,1024]{1,0:T(8,128)(2,1)}, bf16[144,1024]{1,0:T(8,128)(2,1)S(1)}, u32[]{:S(2)}, u32[]{:S(2)}) collective-permute-start(bf16[144,1024]{1,0:T(8,128)(2,1)} %get-tuple-element.53), channel_id=1, source_target_pairs={{0,24},{8,16},{16,8},{24,0},{1,25},{9,17},{17,9},{25,1},{2,26},{10... | collective-permute-start | bytes 884744 | tf_op jit(solution)/shard_map/ppermute | solution.py:88
  62.0 34.6 %collective-permute-start.16 = (bf16[192,1024]{1,0:T(8,128)(2,1)S(1)}, bf16[192,1024]{1,0:T(8,128)(2,1)}, u32[]{:S(2)}, u32[]{:S(2)}) collective-permute-start(bf16[192,1024]{1,0:T(8,128)(2,1)S(1)} %copy-done.24), channel_id=1, source_target_pairs={{0,2},{1,3},{2,4},{3,5},{4,6},{5,7},{6,0},{7,1},{8,10},{9,11},{10,... | collective-permute-start | bytes 1179656 | tf_op jit(solution)/shard_map/ppermute | solution.py:72
  70.2 6.4 %copy-start.31 = (bf16[144,1024]{1,0:T(8,128)(2,1)}, bf16[144,1024]{1,0:T(8,128)(2,1)S(1)}, u32[]{:S(2)}) copy-start(bf16[144,1024]{1,0:T(8,128)(2,1)S(1)} %collective-permute-done.23.refs_1_) | copy-start | bytes 884740
  70.2 14.6 %collective-permute-start.32 = (bf16[144,1024]{1,0:T(8,128)(2,1)}, bf16[144,1024]{1,0:T(8,128)(2,1)S(1)}, u32[]{:S(2)}, u32[]{:S(2)}) collective-permute-start(bf16[144,1024]{1,0:T(8,128)(2,1)} %get-tuple-element.63), channel_id=1, source_target_pairs={{0,8},{8,0},{16,24},{24,16},{1,9},{9,1},{17,25},{25,17},{2,10},{10... | collective-permute-start | bytes 884744 | tf_op jit(solution)/shard_map/ppermute | solution.py:88
  71.2 5.4 %copy-start.33 = (bf16[144,1024]{1,0:T(8,128)(2,1)}, bf16[144,1024]{1,0:T(8,128)(2,1)S(1)}, u32[]{:S(2)}) copy-start(bf16[144,1024]{1,0:T(8,128)(2,1)S(1)} %collective-permute-done.24.refs_2_) | copy-start | bytes 884740
  71.2 14.8 %collective-permute-start.33 = (bf16[144,1024]{1,0:T(8,128)(2,1)}, bf16[144,1024]{1,0:T(8,128)(2,1)S(1)}, u32[]{:S(2)}, u32[]{:S(2)}) collective-permute-start(bf16[144,1024]{1,0:T(8,128)(2,1)} %get-tuple-element.64), channel_id=1, source_target_pairs={{0,16},{8,24},{16,0},{24,8},{1,17},{9,25},{17,1},{25,9},{2,18},{10... | collective-permute-start | bytes 884744 | tf_op jit(solution)/shard_map/ppermute | solution.py:88
  75.8 12.7 %collective-permute-start.34 = (bf16[144,1024]{1,0:T(8,128)(2,1)}, bf16[144,1024]{1,0:T(8,128)(2,1)}, u32[]{:S(2)}, u32[]{:S(2)}) collective-permute-start(bf16[144,1024]{1,0:T(8,128)(2,1)} %get-tuple-element.65), channel_id=1, source_target_pairs={{0,24},{8,16},{16,8},{24,0},{1,25},{9,17},{17,9},{25,1},{2,26},{10... | collective-permute-start | bytes 884744 | tf_op jit(solution)/shard_map/ppermute | solution.py:88
  84.8 8.2 %copy-start.34 = (bf16[144,1024]{1,0:T(8,128)(2,1)}, bf16[144,1024]{1,0:T(8,128)(2,1)S(1)}, u32[]{:S(2)}) copy-start(bf16[144,1024]{1,0:T(8,128)(2,1)S(1)} %collective-permute-done.32.refs_1_) | copy-start | bytes 884740
  84.8 14.1 %collective-permute-start.26 = (bf16[144,1024]{1,0:T(8,128)(2,1)}, bf16[144,1024]{1,0:T(8,128)(2,1)S(1)}, u32[]{:S(2)}, u32[]{:S(2)}) collective-permute-start(bf16[144,1024]{1,0:T(8,128)(2,1)} %get-tuple-element.55), channel_id=1, source_target_pairs={{0,8},{8,0},{16,24},{24,16},{1,9},{9,1},{17,25},{25,17},{2,10},{10... | collective-permute-start | bytes 884744 | tf_op jit(solution)/shard_map/ppermute | solution.py:88
  86.1 2.4 %copy-start.36 = (bf16[144,1024]{1,0:T(8,128)(2,1)}, bf16[144,1024]{1,0:T(8,128)(2,1)S(1)}, u32[]{:S(2)}) copy-start(bf16[144,1024]{1,0:T(8,128)(2,1)S(1)} %collective-permute-done.33.refs_2_) | copy-start | bytes 884740
  86.1 14.2 %collective-permute-start.27 = (bf16[144,1024]{1,0:T(8,128)(2,1)}, bf16[144,1024]{1,0:T(8,128)(2,1)S(1)}, u32[]{:S(2)}, u32[]{:S(2)}) collective-permute-start(bf16[144,1024]{1,0:T(8,128)(2,1)} %get-tuple-element.56), channel_id=1, source_target_pairs={{0,16},{8,24},{16,0},{24,8},{1,17},{9,25},{17,1},{25,9},{2,18},{10... | collective-permute-start | bytes 884744 | tf_op jit(solution)/shard_map/ppermute | solution.py:88
  88.5 19.4 %collective-permute-start.28 = (bf16[144,1024]{1,0:T(8,128)(2,1)}, bf16[144,1024]{1,0:T(8,128)(2,1)S(1)}, u32[]{:S(2)}, u32[]{:S(2)}) collective-permute-start(bf16[144,1024]{1,0:T(8,128)(2,1)} %get-tuple-element.57), channel_id=1, source_target_pairs={{0,24},{8,16},{16,8},{24,0},{1,25},{9,17},{17,9},{25,1},{2,26},{10... | collective-permute-start | bytes 884744 | tf_op jit(solution)/shard_map/ppermute | solution.py:88
  96.0 12.0 %collective-permute-start.35 = (bf16[192,1024]{1,0:T(8,128)(2,1)}, bf16[192,1024]{1,0:T(8,128)(2,1)S(1)}, u32[]{:S(2)}, u32[]{:S(2)}) collective-permute-start(bf16[192,1024]{1,0:T(8,128)(2,1)} %combine.4), channel_id=1, source_target_pairs={{0,2},{1,3},{2,4},{3,5},{4,6},{5,7},{6,0},{7,1},{8,10},{9,11},{10,... | collective-permute-start | bytes 1179656 | tf_op jit(solution)/shard_map/ppermute | solution.py:72
  98.9 13.3 %collective-permute-start.17 = (bf16[144,1024]{1,0:T(8,128)(2,1)}, bf16[144,1024]{1,0:T(8,128)(2,1)}, u32[]{:S(2)}, u32[]{:S(2)}) collective-permute-start(bf16[144,1024]{1,0:T(8,128)(2,1)} %get-tuple-element.43), channel_id=1, source_target_pairs={{0,8},{8,0},{16,24},{24,16},{1,9},{9,1},{17,25},{25,17},{2,10},{10... | collective-permute-start | bytes 884744 | tf_op jit(solution)/shard_map/ppermute | solution.py:88
  98.9 9.0 %copy-start.7 = (bf16[144,1024]{1,0:T(8,128)(2,1)}, bf16[144,1024]{1,0:T(8,128)(2,1)S(1)}, u32[]{:S(2)}) copy-start(bf16[144,1024]{1,0:T(8,128)(2,1)S(1)} %collective-permute-done.26.refs_1_) | copy-start | bytes 884740
  98.9 15.9 %collective-permute-start.18 = (bf16[144,1024]{1,0:T(8,128)(2,1)}, bf16[144,1024]{1,0:T(8,128)(2,1)}, u32[]{:S(2)}, u32[]{:S(2)}) collective-permute-start(bf16[144,1024]{1,0:T(8,128)(2,1)} %get-tuple-element.44), channel_id=1, source_target_pairs={{0,16},{8,24},{16,0},{24,8},{1,17},{9,25},{17,1},{25,9},{2,18},{10... | collective-permute-start | bytes 884744 | tf_op jit(solution)/shard_map/ppermute | solution.py:88
  100.3 7.6 %copy-start.8 = (bf16[144,1024]{1,0:T(8,128)(2,1)}, bf16[144,1024]{1,0:T(8,128)(2,1)S(1)}, u32[]{:S(2)}) copy-start(bf16[144,1024]{1,0:T(8,128)(2,1)S(1)} %collective-permute-done.27.refs_2_) | copy-start | bytes 884740
  100.3 16.0 %collective-permute-start.19 = (bf16[144,1024]{1,0:T(8,128)(2,1)}, bf16[144,1024]{1,0:T(8,128)(2,1)}, u32[]{:S(2)}, u32[]{:S(2)}) collective-permute-start(bf16[144,1024]{1,0:T(8,128)(2,1)} %get-tuple-element.45), channel_id=1, source_target_pairs={{0,24},{8,16},{16,8},{24,0},{1,25},{9,17},{17,9},{25,1},{2,26},{10... | collective-permute-start | bytes 884744 | tf_op jit(solution)/shard_map/ppermute | solution.py:88
  107.9 20.1 %collective-permute-start.2 = (bf16[144,1024]{1,0:T(8,128)(2,1)}, bf16[144,1024]{1,0:T(8,128)(2,1)}, u32[]{:S(2)}, u32[]{:S(2)}) collective-permute-start(bf16[144,1024]{1,0:T(8,128)(2,1)} %get-tuple-element.35), channel_id=1, source_target_pairs={{0,8},{8,0},{16,24},{24,16},{1,9},{9,1},{17,25},{25,17},{2,10},{10... | collective-permute-start | bytes 884744 | tf_op jit(solution)/shard_map/ppermute | solution.py:88
  108.6 20.9 %collective-permute-start.3 = (bf16[144,1024]{1,0:T(8,128)(2,1)S(1)}, bf16[144,1024]{1,0:T(8,128)(2,1)}, u32[]{:S(2)}, u32[]{:S(2)}) collective-permute-start(bf16[144,1024]{1,0:T(8,128)(2,1)S(1)} %copy-done.27), channel_id=1, source_target_pairs={{0,16},{8,24},{16,0},{24,8},{1,17},{9,25},{17,1},{25,9},{2,18},{10... | collective-permute-start | bytes 884744 | tf_op jit(solution)/shard_map/ppermute | solution.py:88
  109.0 3.2 %copy-start.26 = (bf16[144,1024]{1,0:T(8,128)(2,1)S(1)}, bf16[144,1024]{1,0:T(8,128)(2,1)}, u32[]{:S(2)}) copy-start(bf16[144,1024]{1,0:T(8,128)(2,1)} %get-tuple-element.37) | copy-start | bytes 884740
  112.2 21.2 %collective-permute-start.4 = (bf16[144,1024]{1,0:T(8,128)(2,1)S(1)}, bf16[144,1024]{1,0:T(8,128)(2,1)S(1)}, u32[]{:S(2)}, u32[]{:S(2)}) collective-permute-start(bf16[144,1024]{1,0:T(8,128)(2,1)S(1)} %copy-done.26), channel_id=1, source_target_pairs={{0,24},{8,16},{16,8},{24,0},{1,25},{9,17},{17,9},{25,1},{2,26},{10... | collective-permute-start | bytes 884744 | tf_op jit(solution)/shard_map/ppermute | solution.py:88
  114.8 30.9 %collective-permute-start.36 = (bf16[192,1024]{1,0:T(8,128)(2,1)}, bf16[192,1024]{1,0:T(8,128)(2,1)S(1)}, u32[]{:S(2)}, u32[]{:S(2)}) collective-permute-start(bf16[192,1024]{1,0:T(8,128)(2,1)} %combine.5), channel_id=1, source_target_pairs={{0,2},{1,3},{2,4},{3,5},{4,6},{5,7},{6,0},{7,1},{8,10},{9,11},{10,... | collective-permute-start | bytes 1179656 | tf_op jit(solution)/shard_map/ppermute | solution.py:72
  124.4 17.9 %collective-permute-start.20 = (bf16[144,1024]{1,0:T(8,128)(2,1)}, bf16[144,1024]{1,0:T(8,128)(2,1)S(1)}, u32[]{:S(2)}, u32[]{:S(2)}) collective-permute-start(bf16[144,1024]{1,0:T(8,128)(2,1)} %get-tuple-element.47), channel_id=1, source_target_pairs={{0,8},{8,0},{16,24},{24,16},{1,9},{9,1},{17,25},{25,17},{2,10},{10... | collective-permute-start | bytes 884744 | tf_op jit(solution)/shard_map/ppermute | solution.py:88
  128.1 16.8 %collective-permute-start.21 = (bf16[144,1024]{1,0:T(8,128)(2,1)}, bf16[144,1024]{1,0:T(8,128)(2,1)S(1)}, u32[]{:S(2)}, u32[]{:S(2)}) collective-permute-start(bf16[144,1024]{1,0:T(8,128)(2,1)} %get-tuple-element.48), channel_id=1, source_target_pairs={{0,16},{8,24},{16,0},{24,8},{1,17},{9,25},{17,1},{25,9},{2,18},{10... | collective-permute-start | bytes 884744 | tf_op jit(solution)/shard_map/ppermute | solution.py:88
  129.5 16.3 %collective-permute-start.22 = (bf16[144,1024]{1,0:T(8,128)(2,1)}, bf16[144,1024]{1,0:T(8,128)(2,1)S(1)}, u32[]{:S(2)}, u32[]{:S(2)}) collective-permute-start(bf16[144,1024]{1,0:T(8,128)(2,1)} %get-tuple-element.49), channel_id=1, source_target_pairs={{0,24},{8,16},{16,8},{24,0},{1,25},{9,17},{17,9},{25,1},{2,26},{10... | collective-permute-start | bytes 884744 | tf_op jit(solution)/shard_map/ppermute | solution.py:88
  142.3 13.5 %collective-permute-start.10 = (bf16[144,1024]{1,0:T(8,128)(2,1)}, bf16[144,1024]{1,0:T(8,128)(2,1)S(1)}, u32[]{:S(2)}, u32[]{:S(2)}) collective-permute-start(bf16[144,1024]{1,0:T(8,128)(2,1)} %get-tuple-element.41), channel_id=1, source_target_pairs={{0,24},{8,16},{16,8},{24,0},{1,25},{9,17},{17,9},{25,1},{2,26},{10... | collective-permute-start | bytes 884744 | tf_op jit(solution)/shard_map/ppermute | solution.py:88
  142.3 3.5 %copy-start.10 = (bf16[144,1024]{1,0:T(8,128)(2,1)}, bf16[144,1024]{1,0:T(8,128)(2,1)S(1)}, u32[]{:S(2)}) copy-start(bf16[144,1024]{1,0:T(8,128)(2,1)S(1)} %collective-permute-done.20.refs_1_) | copy-start | bytes 884740
  142.3 13.5 %collective-permute-start.8 = (bf16[144,1024]{1,0:T(8,128)(2,1)}, bf16[144,1024]{1,0:T(8,128)(2,1)S(1)}, u32[]{:S(2)}, u32[]{:S(2)}) collective-permute-start(bf16[144,1024]{1,0:T(8,128)(2,1)} %get-tuple-element.39), channel_id=1, source_target_pairs={{0,8},{8,0},{16,24},{24,16},{1,9},{9,1},{17,25},{25,17},{2,10},{10... | collective-permute-start | bytes 884744 | tf_op jit(solution)/shard_map/ppermute | solution.py:88
  144.8 11.0 %collective-permute-start.9 = (bf16[144,1024]{1,0:T(8,128)(2,1)}, bf16[144,1024]{1,0:T(8,128)(2,1)S(1)}, u32[]{:S(2)}, u32[]{:S(2)}) collective-permute-start(bf16[144,1024]{1,0:T(8,128)(2,1)} %get-tuple-element.40), channel_id=1, source_target_pairs={{0,16},{8,24},{16,0},{24,8},{1,17},{9,25},{17,1},{25,9},{2,18},{10... | collective-permute-start | bytes 884744 | tf_op jit(solution)/shard_map/ppermute | solution.py:88
  149.8 9.8 %collective-permute-start.37 = (bf16[192,1024]{1,0:T(8,128)(2,1)}, bf16[192,1024]{1,0:T(8,128)(2,1)S(1)}, u32[]{:S(2)}, u32[]{:S(2)}) collective-permute-start(bf16[192,1024]{1,0:T(8,128)(2,1)} %combine.6), channel_id=1, source_target_pairs={{0,2},{1,3},{2,4},{3,5},{4,6},{5,7},{6,0},{7,1},{8,10},{9,11},{10,... | collective-permute-start | bytes 1179656 | tf_op jit(solution)/shard_map/ppermute | solution.py:72
  155.8 3.8 %copy-start.11 = (bf16[144,1024]{1,0:T(8,128)(2,1)}, bf16[144,1024]{1,0:T(8,128)(2,1)S(1)}, u32[]{:S(2)}) copy-start(bf16[144,1024]{1,0:T(8,128)(2,1)S(1)} %collective-permute-done.10.refs_3_) | copy-start | bytes 884740
  155.8 3.8 %copy-start.13 = (bf16[144,1024]{1,0:T(8,128)(2,1)}, bf16[144,1024]{1,0:T(8,128)(2,1)S(1)}, u32[]{:S(2)}) copy-start(bf16[144,1024]{1,0:T(8,128)(2,1)S(1)} %collective-permute-done.8.refs_1_) | copy-start | bytes 884740
  155.8 3.8 %copy-start.15 = (bf16[144,1024]{1,0:T(8,128)(2,1)}, bf16[144,1024]{1,0:T(8,128)(2,1)S(1)}, u32[]{:S(2)}) copy-start(bf16[144,1024]{1,0:T(8,128)(2,1)S(1)} %collective-permute-done.9.refs_2_) | copy-start | bytes 884740
  (12 other events, 9.8 us)

commit v2 on v1

--- a/solution.py
+++ b/solution.py
@@ -67,9 +67,9 @@
 CORES = 2
 
 
-def ring(value):
+def ring(value, steps=1):
     size = lax.axis_size("tp")
-    return lax.ppermute(value, "tp", [(i, (i + CORES) % size) for i in range(size)])
+    return lax.ppermute(value, "tp", [(i, (i + steps * CORES) % size) for i in range(size)])
 
 
 def core_swap(value):
@@ -155,17 +155,14 @@
     )(rows, table)
 
 
-def combine(pieces, table, incoming):
+def combine(pieces, table):
     top_count = table.shape[0] // 2
     capacity, width = pieces[0].shape
     row_count = table.shape[1]
-    extra = [] if incoming is None else [incoming]
 
     def kernel(table_ref, *refs):
         out_ref = refs[-1]
         total = jnp.zeros((row_count, width), jnp.float32)
-        if extra:
-            total = refs[-2][...].astype(jnp.float32)
         for m in range(len(pieces)):
             hits = slot_hits(table_ref, top_count, m * capacity, capacity)
             weight = jnp.zeros(hits[0].shape, jnp.float32)
@@ -180,17 +177,17 @@
                     (((0,), (0,)), ((), ())),
                     preferred_element_type=jnp.float32,
                 )
-        out_ref[...] = total.astype(jnp.bfloat16)
+        out_ref[...] = total
 
     work = len(pieces) * capacity * row_count * width
     return pl.pallas_call(
         kernel,
-        out_shape=jax.ShapeDtypeStruct((row_count, width), jnp.bfloat16),
+        out_shape=jax.ShapeDtypeStruct((row_count, width), jnp.float32),
         cost_estimate=pl.CostEstimate(
             flops=4 * work, transcendentals=0, bytes_accessed=2 * (len(pieces) * capacity + 2 * row_count) * width
         ),
         name="combine",
-    )(table, *pieces, *extra)
+    )(table, *pieces)
 
 
 def ffn(pieces, shards):
@@ -220,7 +217,9 @@
             gate_ref, up_ref, down_ref = weight_refs[3 * n : 3 * n + 3]
             gate = jnp.dot(values, gate_ref[...], preferred_element_type=jnp.float32)
             up = jnp.dot(values, up_ref[...], preferred_element_type=jnp.float32)
-            hidden = (gate / (1.0 + jnp.exp(-gate)) * up).astype(jnp.bfloat16)
+            half_gate = 0.5 * gate
+            silu = half_gate + half_gate * jnp.tanh(half_gate)
+            hidden = (silu * up).astype(jnp.bfloat16)
             part = jnp.dot(hidden, down_ref[...], preferred_element_type=jnp.float32)
             term = part if term is None else term + part
 
@@ -283,20 +282,28 @@
     shards = [shard, tuple(core_swap(w) for w in shard)]
 
     table = route_table(routes, route_weight, experts, capacity)
-    blocks, tables = [normed], [table]
+    blocks = [normed]
     for _ in range(1, chips):
         blocks.append(ring(blocks[-1]))
-        tables.append(ring(tables[-1]))
-
-    back = []
+    tables = [table] + [ring(table, n) for n in range(1, chips)]
+
+    arrived = []
     for n in range(chips):
-        arrived = exchange(dispatch(blocks[n], tables[n], experts, capacity))
-        served = ffn(arrived, shards)
-        back.append(exchange(served))
+        arrived.append(exchange(dispatch(blocks[n], tables[n], experts, capacity)))
+
+    order = list(range(1, chips)) + [0]
+    back = {}
+    for first in range(0, chips, 2):
+        group = order[first : first + 2]
+        served = ffn([piece for n in group for piece in arrived[n]], shards)
+        for place, n in enumerate(group):
+            back[n] = exchange(served[place * experts : (place + 1) * experts])
 
     total = None
-    for n in list(range(1, chips)) + [0]:
-        total = combine(back[n], tables[n], total)
+    for n in order:
+        term = combine(back[n], tables[n])
+        total = term if total is None else term + total.astype(jnp.float32)
+        total = total.astype(jnp.bfloat16)
         if n:
             total = ring(total)
 
@@ -319,6 +326,7 @@
         P("ep", "tp", None),
     )
 
+
     return jax.shard_map(
         on_device,
         mesh=mesh,

time: 165 us -> 189 us (1.15)
  waiting for transfers between devices: 35.4 us -> 69 us
  starting transfers between devices: 63.1 us -> 54.3 us
  other arithmetic: 4.57 us -> 10.8 us
  Pallas kernels: 54.4 us -> 48.3 us
    ppermute x24, waiting for transfers between devices: 20.2 us -> 42.8 us  [exchange(): lax.ppermute(pieces[m], 'ep', [(i, i ^ m) for i in range(count)])]
    ppermute x9, waiting for transfers between devices: 11.6 us -> 26.2 us  [ring(): lax.ppermute(value, 'tp', [(i, (i + steps * CORES) % size) for i in range...]
    ppermute x24, starting transfers between devices: 49.5 us -> 42.3 us  [exchange(): lax.ppermute(pieces[m], 'ep', [(i, i ^ m) for i in range(count)])]
    pallas_call x4 -> x2, Pallas kernels: 32.7 us -> 26.5 us  [ffn(): pl.pallas_call(kernel, grid=(steps,), in_specs=[whole] * count + [across,...]
    convert_element_type x0 -> x4, other arithmetic: none -> 4.49 us  [on_device(): total = total.astype(jnp.bfloat16)]
    ppermute x1, waiting for transfers between devices: 2.77 us -> 0.01 us  [padded_2(): after = lax.ppermute(leading, axis, down)]
    unnamed x76 -> x72, local copies, waits for them, and re-layouts: 4.41 us -> 4.02 us
  transfers between devices with their start and end apart: 38 -> 38, of which waited for: 10 -> 16; matrix products, arithmetic and copies ran while one was open for 2% -> 4% of each run, Pallas kernels for 31% -> 26%
where the time goes in v2:
time: 189 us; the launch traced here: 188 us
  waiting for transfers between devices  69 us (37%)
  starting transfers between devices  54.3 us (29%)
  Pallas kernels  48.3 us (26%)
  other arithmetic  10.8 us (6%)
  local copies, waits for them, and re-layouts  4.1 us (2%)
    ppermute x24, waiting for transfers between devices, exchange(): lax.ppermute(pieces[m], 'ep', [(i, i ^ m) for i in range(count)])  42.8 us
    ppermute x24, starting transfers between devices, exchange(): lax.ppermute(pieces[m], 'ep', [(i, i ^ m) for i in range(count)])  42.3 us
    pallas_call x2, Pallas kernels, ffn(): pl.pallas_call(kernel, grid=(steps,), in_specs=[whole] * count + [across,...  26.5 us
    ppermute x9, waiting for transfers between devices, ring(): lax.ppermute(value, 'tp', [(i, (i + steps * CORES) % size) for i in range...  26.2 us
    pallas_call x4, Pallas kernels, combine(): pl.pallas_call(kernel, out_shape=jax.ShapeDtypeStruct((row_count, width),...  12.7 us
    pallas_call x4, Pallas kernels, dispatch(): pl.pallas_call(kernel, out_shape=[shape] * experts, cost_estimate=pl.Cost...  9.07 us
    ppermute x9, starting transfers between devices, ring(): lax.ppermute(value, 'tp', [(i, (i + steps * CORES) % size) for i in range...  8.94 us
    convert_element_type x4, other arithmetic, on_device(): total = total.astype(jnp.bfloat16)  4.49 us
  transfers between devices with their start and end apart: 38, of which 16 were waited for; matrix products, arithmetic and copies ran while one was open for 4% of the time, Pallas kernels for 26%

profile of v2, /device:TPU:0, one launch (start us, length us, event | category | flops | bytes accessed | tf_op | source)
XLA Modules:
  0.0 187.9 jit_solution(13490433045649623125)
XLA Ops:
  0.7 1.2 fusion.3
  1.9 0.8 fusion.5.rows_ref
  2.8 3.1 %collective-permute-start.2 = (bf16[192,1024]{1,0:T(8,128)(2,1)S(1)}, bf16[192,1024]{1,0:T(8,128)(2,1)}, u32[]{:S(2)}, u32[]{:S(2)}) collective-permute-start(bf16[192,1024]{1,0:T(8,128)(2,1)S(1)} %fusion.5.rows_ref), channel_id=1, source_target_pairs={{0,2},{1,3},{2,4},{3,5},{4,6},{5,7},{6,0},{7,1},{8,10},{9,11},{10,... | collective-permute-start | bytes 1179656 | tf_op jit(solution)/shard_map/ppermute | solution.py:72
  6.4 0.7 copy-done.28
  7.2 9.9 %collective-permute-done.2.rows_ref = bf16[192,1024]{1,0:T(8,128)(2,1)} collective-permute-done((bf16[192,1024]{1,0:T(8,128)(2,1)S(1)}, bf16[192,1024]{1,0:T(8,128)(2,1)}, u32[]{:S(2)}, u32[]{:S(2)}) %collective-permute-start.2) | collective-permute-done | bytes 393248 | tf_op jit(solution)/shard_map/ppermute | solution.py:72
  17.1 0.7 copy-done.29
  17.8 1.3 collective-permute-start.22
  19.2 10.4 %collective-permute-done.22.table_ref = f32[4,192]{1,0:T(4,128)S(1)} collective-permute-done((f32[4,192]{1,0:T(4,128)S(1)}, f32[4,192]{1,0:T(4,128)S(1)}, u32[]{:S(2)}, u32[]{:S(2)}) %collective-permute-start.22) | collective-permute-done | bytes 3104 | tf_op jit(solution)/shard_map/ppermute | solution.py:72
  30.2 2.3 %dispatch.6 = (bf16[144,1024]{1,0:T(8,128)(2,1)}, bf16[144,1024]{1,0:T(8,128)(2,1)}, bf16[144,1024]{1,0:T(8,128)(2,1)}, bf16[144,1024]{1,0:T(8,128)(2,1)}) custom-call(bf16[192,1024]{1,0:T(8,128)(2,1)} %collective-permute-done.2.rows_ref, f32[4,192]{1,0:T(4,128)} %copy-done.26), custom_call_target="tpu_custom_call" | custom-call | flops 226492416 | bytes 1572864 | tf_op jit(solution)/shard_map/dispatch/pallas_call | solution.py:148
  32.4 1.6 collective-permute-done.21.table_ref
  34.1 1.3 collective-permute-start.23
  35.3 5.7 %collective-permute-done.23.refs_1_ = bf16[144,1024]{1,0:T(8,128)(2,1)S(1)} collective-permute-done((bf16[144,1024]{1,0:T(8,128)(2,1)}, bf16[144,1024]{1,0:T(8,128)(2,1)S(1)}, u32[]{:S(2)}, u32[]{:S(2)}) %collective-permute-start.23) | collective-permute-done | bytes 294944 | tf_op jit(solution)/shard_map/ppermute | solution.py:88
  41.0 1.3 collective-permute-start.24
  42.3 1.7 collective-permute-start.25
  44.0 2.3 %dispatch.7 = (bf16[144,1024]{1,0:T(8,128)(2,1)}, bf16[144,1024]{1,0:T(8,128)(2,1)}, bf16[144,1024]{1,0:T(8,128)(2,1)}, bf16[144,1024]{1,0:T(8,128)(2,1)}) custom-call(bf16[192,1024]{1,0:T(8,128)(2,1)} %collective-permute-done.3.rows_ref, f32[4,192]{1,0:T(4,128)} %copy-done.25), custom_call_target="tpu_custom_call" | custom-call | flops 226492416 | bytes 1572864 | tf_op jit(solution)/shard_map/dispatch/pallas_call | solution.py:148
  46.3 6.3 %collective-permute-done.24.refs_2_ = bf16[144,1024]{1,0:T(8,128)(2,1)S(1)} collective-permute-done((bf16[144,1024]{1,0:T(8,128)(2,1)}, bf16[144,1024]{1,0:T(8,128)(2,1)S(1)}, u32[]{:S(2)}, u32[]{:S(2)}) %collective-permute-start.24) | collective-permute-done | bytes 294944 | tf_op jit(solution)/shard_map/ppermute | solution.py:88
  52.6 1.1 collective-permute-start.26
  53.7 1.5 collective-permute-start.27
  55.2 1.0 collective-permute-start.28
  56.3 2.3 %dispatch.5 = (bf16[144,1024]{1,0:T(8,128)(2,1)}, bf16[144,1024]{1,0:T(8,128)(2,1)}, bf16[144,1024]{1,0:T(8,128)(2,1)}, bf16[144,1024]{1,0:T(8,128)(2,1)}) custom-call(bf16[192,1024]{1,0:T(8,128)(2,1)} %copy-done.4, f32[4,192]{1,0:T(4,128)} %copy-done.17), custom_call_target="tpu_custom_call" | custom-call | flops 226492416 | bytes 1572864 | tf_op jit(solution)/shard_map/dispatch/pallas_call | solution.py:148
  58.7 1.1 collective-permute-start.10
  59.8 3.0 %collective-permute-done.26.refs_5_ = bf16[144,1024]{1,0:T(8,128)(2,1)} collective-permute-done((bf16[144,1024]{1,0:T(8,128)(2,1)}, bf16[144,1024]{1,0:T(8,128)(2,1)}, u32[]{:S(2)}, u32[]{:S(2)}) %collective-permute-start.26) | collective-permute-done | bytes 294944 | tf_op jit(solution)/shard_map/ppermute | solution.py:88
  62.8 6.5 %collective-permute-done.27.refs_6_ = bf16[144,1024]{1,0:T(8,128)(2,1)} collective-permute-done((bf16[144,1024]{1,0:T(8,128)(2,1)}, bf16[144,1024]{1,0:T(8,128)(2,1)}, u32[]{:S(2)}, u32[]{:S(2)}) %collective-permute-start.27) | collective-permute-done | bytes 294944 | tf_op jit(solution)/shard_map/ppermute | solution.py:88
  69.3 13.2 %ffn.3 = (bf16[144,1024]{1,0:T(8,128)(2,1)}, bf16[144,1024]{1,0:T(8,128)(2,1)}, bf16[144,1024]{1,0:T(8,128)(2,1)}, bf16[144,1024]{1,0:T(8,128)(2,1)}, bf16[144,1...) custom-call(bf16[144,1024]{1,0:T(8,128)(2,1)} %get-tuple-element.50.refs_0_,, ...), custom_call_target="tpu_custom_call" | custom-call | flops 7247757312 | bytes 11010048 | tf_op jit(solution)/shard_map/ffn/pallas_call | solution.py:243
  82.5 1.1 collective-permute-start.32
  83.9 1.3 collective-permute-start
  85.2 1.3 collective-permute-start.1
  86.5 7.9 %collective-permute-start.33 = (bf16[144,1024]{1,0:T(8,128)(2,1)}, bf16[144,1024]{1,0:T(8,128)(2,1)S(1)}, u32[]{:S(2)}, u32[]{:S(2)}) collective-permute-start(bf16[144,1024]{1,0:T(8,128)(2,1)} %get-tuple-element.64), channel_id=1, source_target_pairs={{0,16},{8,24},{16,0},{24,8},{1,17},{9,25},{17,1},{25,9},{2,18},{10... | collective-permute-start | bytes 884744 | tf_op jit(solution)/shard_map/ppermute | solution.py:88
  94.4 1.9 collective-permute-start.34
  96.3 0.9 collective-permute-start.29
  97.2 0.7 collective-permute-start.30
  97.9 1.9 collective-permute-start.31
  100.3 2.3 %dispatch.4 = (bf16[144,1024]{1,0:T(8,128)(2,1)}, bf16[144,1024]{1,0:T(8,128)(2,1)}, bf16[144,1024]{1,0:T(8,128)(2,1)}, bf16[144,1024]{1,0:T(8,128)(2,1)}) custom-call(bf16[192,1024]{1,0:T(8,128)(2,1)} %collective-permute-done.4.rows_ref, f32[4,192]{1,0:T(4,128)} %copy-done.24), custom_call_target="tpu_custom_call" | custom-call | flops 226492416 | bytes 1572864 | tf_op jit(solution)/shard_map/dispatch/pallas_call | solution.py:148
  102.6 10.6 %collective-permute-done.33.refs_2_ = bf16[144,1024]{1,0:T(8,128)(2,1)S(1)} collective-permute-done((bf16[144,1024]{1,0:T(8,128)(2,1)}, bf16[144,1024]{1,0:T(8,128)(2,1)S(1)}, u32[]{:S(2)}, u32[]{:S(2)}) %collective-permute-start.33) | collective-permute-done | bytes 294944 | tf_op jit(solution)/shard_map/ppermute | solution.py:88
  113.2 3.4 %collective-permute-start.11 = (bf16[144,1024]{1,0:T(8,128)(2,1)}, bf16[144,1024]{1,0:T(8,128)(2,1)S(1)}, u32[]{:S(2)}, u32[]{:S(2)}) collective-permute-start(bf16[144,1024]{1,0:T(8,128)(2,1)} %get-tuple-element.41), channel_id=1, source_target_pairs={{0,24},{8,16},{16,8},{24,0},{1,25},{9,17},{17,9},{25,1},{2,26},{10... | collective-permute-start | bytes 884744 | tf_op jit(solution)/shard_map/ppermute | solution.py:88
  116.6 2.0 %collective-permute-start.6 = (bf16[144,1024]{1,0:T(8,128)(2,1)}, bf16[144,1024]{1,0:T(8,128)(2,1)}, u32[]{:S(2)}, u32[]{:S(2)}) collective-permute-start(bf16[144,1024]{1,0:T(8,128)(2,1)} %get-tuple-element.35), channel_id=1, source_target_pairs={{0,8},{8,0},{16,24},{24,16},{1,9},{9,1},{17,25},{25,17},{2,10},{10... | collective-permute-start | bytes 884744 | tf_op jit(solution)/shard_map/ppermute | solution.py:88
  118.6 2.9 %collective-permute-done.30.refs_2_ = bf16[144,1024]{1,0:T(8,128)(2,1)S(1)} collective-permute-done((bf16[144,1024]{1,0:T(8,128)(2,1)}, bf16[144,1024]{1,0:T(8,128)(2,1)S(1)}, u32[]{:S(2)}, u32[]{:S(2)}) %collective-permute-start.30) | collective-permute-done | bytes 294944 | tf_op jit(solution)/shard_map/ppermute | solution.py:88
  121.5 2.9 %collective-permute-start.7 = (bf16[144,1024]{1,0:T(8,128)(2,1)}, bf16[144,1024]{1,0:T(8,128)(2,1)}, u32[]{:S(2)}, u32[]{:S(2)}) collective-permute-start(bf16[144,1024]{1,0:T(8,128)(2,1)} %get-tuple-element.36), channel_id=1, source_target_pairs={{0,16},{8,24},{16,0},{24,8},{1,17},{9,25},{17,1},{25,9},{2,18},{10... | collective-permute-start | bytes 884744 | tf_op jit(solution)/shard_map/ppermute | solution.py:88
  124.4 0.6 subtract_convert_fusion.2
  125.0 0.8 maximum_convert_fusion
  125.8 3.1 %combine.7 = f32[192,1024]{1,0:T(8,128)} custom-call(f32[4,192]{1,0:T(4,128)} %copy-done.26, bf16[144,1024]{1,0:T(8,128)(2,1)} %get-tuple-element.62.refs_0_, bf16[144,1024]{1,0:T(8,128)(2,1)} %copy-done.5, bf16[144,1024]{1,0:T(8,128)(2,1)} %copy-done.6, bf16[144,1024]{1,0:T(8,128)(2,1)} %copy-done.7), custom_call_target="tpu_custom_call" | custom-call | flops 452984832 | bytes 1966080 | tf_op jit(solution)/shard_map/combine/pallas_call | solution.py:183
  129.0 1.2 convert_element_type.100
  130.1 3.1 %combine.6 = f32[192,1024]{1,0:T(8,128)} custom-call(f32[4,192]{1,0:T(4,128)} %copy-done.25, bf16[144,1024]{1,0:T(8,128)(2,1)} %get-tuple-element.58.refs_0_, bf16[144,1024]{1,0:T(8,128)(2,1)} %copy-done.8, bf16[144,1024]{1,0:T(8,128)(2,1)} %copy-done.9, bf16[144,1024]{1,0:T(8,128)(2,1)} %copy-done.10), custom_call_target="tpu_custom_call" | custom-call | flops 452984832 | bytes 1966080 | tf_op jit(solution)/shard_map/combine/pallas_call | solution.py:183
  133.3 1.3 collective-permute-done.6.refs_1_
  134.6 3.2 %collective-permute-done.8.refs_3_ = bf16[144,1024]{1,0:T(8,128)(2,1)} collective-permute-done((bf16[144,1024]{1,0:T(8,128)(2,1)}, bf16[144,1024]{1,0:T(8,128)(2,1)}, u32[]{:S(2)}, u32[]{:S(2)}) %collective-permute-start.8) | collective-permute-done | bytes 294944 | tf_op jit(solution)/shard_map/ppermute | solution.py:88
  137.8 13.3 %ffn.2 = (bf16[144,1024]{1,0:T(8,128)(2,1)}, bf16[144,1024]{1,0:T(8,128)(2,1)}, bf16[144,1024]{1,0:T(8,128)(2,1)}, bf16[144,1024]{1,0:T(8,128)(2,1)}, bf16[144,1...) custom-call(bf16[144,1024]{1,0:T(8,128)(2,1)} %get-tuple-element.34.refs_0_,, ...), custom_call_target="tpu_custom_call" | custom-call | flops 7247757312 | bytes 11010048 | tf_op jit(solution)/shard_map/ffn/pallas_call | solution.py:243
  151.1 1.6 collective-permute-start.18
  152.8 1.6 collective-permute-start.19
  154.8 1.4 collective-permute-start.36
  157.0 0.9 fusion.28
  158.0 0.8 collective-permute-start.15
  158.8 1.7 collective-permute-done.18.refs_1_
  160.5 1.7 collective-permute-start.16
  162.1 0.9 collective-permute-done.19.refs_2_
  163.0 4.6 %collective-permute-start.17 = (bf16[144,1024]{1,0:T(8,128)(2,1)}, bf16[144,1024]{1,0:T(8,128)(2,1)}, u32[]{:S(2)}, u32[]{:S(2)}) collective-permute-start(bf16[144,1024]{1,0:T(8,128)(2,1)} %get-tuple-element.45), channel_id=1, source_target_pairs={{0,24},{8,16},{16,8},{24,0},{1,25},{9,17},{17,9},{25,1},{2,26},{10... | collective-permute-start | bytes 884744 | tf_op jit(solution)/shard_map/ppermute | solution.py:88
  167.9 3.2 %combine.5 = f32[192,1024]{1,0:T(8,128)} custom-call(f32[4,192]{1,0:T(4,128)} %copy-done.24, bf16[144,1024]{1,0:T(8,128)(2,1)} %get-tuple-element.46.refs_0_, bf16[144,1024]{1,0:T(8,128)(2,1)} %copy-done.12, bf16[144,1024]{1,0:T(8,128)(2,1)} %copy-done.14, bf16[144,1024]{1,0:T(8,128)(2,1)} %collective-permute-done.20.refs_3_), custom_call_target="tpu_custom_call" | custom-call | flops 452984832 | bytes 1966080 | tf_op jit(solution)/shard_map/combine/pallas_call | solution.py:183
  171.1 1.3 add_convert_fusion.1
  172.3 3.0 %collective-permute-start.37 = (bf16[192,1024]{1,0:T(8,128)(2,1)S(1)}, bf16[192,1024]{1,0:T(8,128)(2,1)S(1)}, u32[]{:S(2)}, u32[]{:S(2)}) collective-permute-start(bf16[192,1024]{1,0:T(8,128)(2,1)S(1)} %add_convert_fusion.1), channel_id=1, source_target_pairs={{0,2},{1,3},{2,4},{3,5},{4,6},{5,7},{6,0},{7,1},{8,10},{9,11},{10,... | collective-permute-start | bytes 1179656 | tf_op jit(solution)/shard_map/ppermute | solution.py:72
  176.3 0.8 multiply_convert_fusion
  177.2 0.6 collective-permute-done.16.refs_2_
  177.9 0.6 copy-done.13
  178.5 3.2 %combine.4 = f32[192,1024]{1,0:T(8,128)} custom-call(f32[4,192]{1,0:T(4,128)} %copy-done.17, bf16[144,1024]{1,0:T(8,128)(2,1)} %get-tuple-element.42.refs_0_, bf16[144,1024]{1,0:T(8,128)(2,1)} %copy-done.11, bf16[144,1024]{1,0:T(8,128)(2,1)} %copy-done.13, bf16[144,1024]{1,0:T(8,128)(2,1)} %collective-permute-done.17.refs_3_), custom_call_target="tpu_custom_call" | custom-call | flops 452984832 | bytes 1966080 | tf_op jit(solution)/shard_map/combine/pallas_call | solution.py:183
  181.7 4.3 %collective-permute-done.37 = bf16[192,1024]{1,0:T(8,128)(2,1)S(1)} collective-permute-done((bf16[192,1024]{1,0:T(8,128)(2,1)S(1)}, bf16[192,1024]{1,0:T(8,128)(2,1)S(1)}, u32[]{:S(2)}, u32[]{:S(2)}) %collective-permute-start.37) | collective-permute-done | bytes 393248 | tf_op jit(solution)/shard_map/ppermute | solution.py:72
  186.0 2.0 %add_convert_fusion = bf16[192,1024]{1,0:T(8,128)(2,1)} fusion(f32[192,1024]{1,0:T(8,128)} %combine.4, bf16[192,1024]{1,0:T(8,128)(2,1)S(1)} %collective-permute-done.37), kind=kLoop, calls=%fused_computation.12 | loop fusion | flops 589824 | bytes 1572864 | tf_op jit(solution)/shard_map/convert_element_type | solution.py:306
  (118 shorter events, 4.9 us)
Async XLA Ops:
  0.6 174.7 %copy-start = (bf16[4,256,256]{2,1,0:T(8,128)(2,1)S(1)}, bf16[4,256,256]{2,1,0:T(8,128)(2,1)}, u32[]{:S(2)}) copy-start(bf16[4,256,256]{2,1,0:T(8,128)(2,1)} %param.13) | copy-start | bytes 1572868
  2.8 29.7 %copy-start.4 = (bf16[192,1024]{1,0:T(8,128)(2,1)}, bf16[192,1024]{1,0:T(8,128)(2,1)S(1)}, u32[]{:S(2)}) copy-start(bf16[192,1024]{1,0:T(8,128)(2,1)S(1)} %fusion.5.rows_ref) | copy-start | bytes 1179652
  2.8 14.4 %collective-permute-start.2 = (bf16[192,1024]{1,0:T(8,128)(2,1)S(1)}, bf16[192,1024]{1,0:T(8,128)(2,1)}, u32[]{:S(2)}, u32[]{:S(2)}) collective-permute-start(bf16[192,1024]{1,0:T(8,128)(2,1)S(1)} %fusion.5.rows_ref), channel_id=1, source_target_pairs={{0,2},{1,3},{2,4},{3,5},{4,6},{5,7},{6,0},{7,1},{8,10},{9,11},{10,... | collective-permute-start | bytes 1179656 | tf_op jit(solution)/shard_map/ppermute | solution.py:72
  5.9 49.3 %collective-permute-start.12 = (bf16[1024,512]{1,0:T(8,128)(2,1)}, bf16[1024,512]{1,0:T(8,128)(2,1)S(1)}, u32[]{:S(2)}, u32[]{:S(2)}) collective-permute-start(bf16[1024,512]{1,0:T(8,128)(2,1)} %bitcast.29), channel_id=1, source_target_pairs={{0,1},{1,0},{2,3},{3,2},{4,5},{5,4},{6,7},{7,6},{8,9},{9,8},{10,11... | collective-permute-start | bytes 3145736 | tf_op jit(solution)/shard_map/ppermute | solution.py:77
  5.9 52.7 %collective-permute-start.13 = (bf16[1024,512]{1,0:T(8,128)(2,1)}, bf16[1024,512]{1,0:T(8,128)(2,1)S(1)}, u32[]{:S(2)}, u32[]{:S(2)}) collective-permute-start(bf16[1024,512]{1,0:T(8,128)(2,1)} %bitcast.32), channel_id=1, source_target_pairs={{0,1},{1,0},{2,3},{3,2},{4,5},{5,4},{6,7},{7,6},{8,9},{9,8},{10,11... | collective-permute-start | bytes 3145736 | tf_op jit(solution)/shard_map/ppermute | solution.py:77
  6.4 52.3 %collective-permute-start.14 = (bf16[512,1024]{1,0:T(8,128)(2,1)}, bf16[512,1024]{1,0:T(8,128)(2,1)}, u32[]{:S(2)}, u32[]{:S(2)}) collective-permute-start(bf16[512,1024]{1,0:T(8,128)(2,1)} %bitcast.35), channel_id=1, source_target_pairs={{0,1},{1,0},{2,3},{3,2},{4,5},{5,4},{6,7},{7,6},{8,9},{9,8},{10,11... | collective-permute-start | bytes 3145736 | tf_op jit(solution)/shard_map/ppermute | solution.py:77
  17.1 25.2 %collective-permute-start.3 = (bf16[192,1024]{1,0:T(8,128)(2,1)}, bf16[192,1024]{1,0:T(8,128)(2,1)}, u32[]{:S(2)}, u32[]{:S(2)}) collective-permute-start(bf16[192,1024]{1,0:T(8,128)(2,1)} %collective-permute-done.2.rows_ref), channel_id=1, source_target_pairs={{0,2},{1,3},{2,4},{3,5},{4,6},{5,7},{6,0},{7,1},{8,10},{9,11},{10,... | collective-permute-start | bytes 1179656 | tf_op jit(solution)/shard_map/ppermute | solution.py:72
  17.8 14.6 %copy-start.17 = (f32[4,192]{1,0:T(4,128)}, f32[4,192]{1,0:T(4,128)S(1)}, u32[]{:S(2)}) copy-start(f32[4,192]{1,0:T(4,128)S(1)} %pad_maximum_fusion.table_ref) | copy-start | bytes 9220
  17.8 11.7 %collective-permute-start.22 = (f32[4,192]{1,0:T(4,128)S(1)}, f32[4,192]{1,0:T(4,128)S(1)}, u32[]{:S(2)}, u32[]{:S(2)}) collective-permute-start(f32[4,192]{1,0:T(4,128)S(1)} %pad_maximum_fusion.table_ref), channel_id=1, source_target_pairs={{0,2},{1,3},{2,4},{3,5},{4,6},{5,7},{6,0},{7,1},{8,10},{9,11},{10,... | collective-permute-start | bytes 9224 | tf_op jit(solution)/shard_map/ppermute | solution.py:72
  29.6 4.5 %collective-permute-start.21 = (f32[4,192]{1,0:T(4,128)S(1)}, f32[4,192]{1,0:T(4,128)S(1)}, u32[]{:S(2)}, u32[]{:S(2)}) collective-permute-start(f32[4,192]{1,0:T(4,128)S(1)} %pad_maximum_fusion.table_ref), channel_id=1, source_target_pairs={{0,4},{1,5},{2,6},{3,7},{4,0},{5,1},{6,2},{7,3},{8,12},{9,13},{10,... | collective-permute-start | bytes 9224 | tf_op jit(solution)/shard_map/ppermute | solution.py:72
  34.1 9.9 %copy-start.25 = (f32[4,192]{1,0:T(4,128)}, f32[4,192]{1,0:T(4,128)S(1)}, u32[]{:S(2)}) copy-start(f32[4,192]{1,0:T(4,128)S(1)} %collective-permute-done.21.table_ref) | copy-start | bytes 9220
  34.1 6.9 %collective-permute-start.23 = (bf16[144,1024]{1,0:T(8,128)(2,1)}, bf16[144,1024]{1,0:T(8,128)(2,1)S(1)}, u32[]{:S(2)}, u32[]{:S(2)}) collective-permute-start(bf16[144,1024]{1,0:T(8,128)(2,1)} %get-tuple-element.51), channel_id=1, source_target_pairs={{0,8},{8,0},{16,24},{24,16},{1,9},{9,1},{17,25},{25,17},{2,10},{10... | collective-permute-start | bytes 884744 | tf_op jit(solution)/shard_map/ppermute | solution.py:88
  41.0 1.3 copy-start.34
  41.0 11.6 %collective-permute-start.24 = (bf16[144,1024]{1,0:T(8,128)(2,1)}, bf16[144,1024]{1,0:T(8,128)(2,1)S(1)}, u32[]{:S(2)}, u32[]{:S(2)}) collective-permute-start(bf16[144,1024]{1,0:T(8,128)(2,1)} %get-tuple-element.52), channel_id=1, source_target_pairs={{0,16},{8,24},{16,0},{24,8},{1,17},{9,25},{17,1},{25,9},{2,18},{10... | collective-permute-start | bytes 884744 | tf_op jit(solution)/shard_map/ppermute | solution.py:88
  42.3 13.8 %copy-start.3 = (bf16[192,1024]{1,0:T(8,128)(2,1)S(1)}, bf16[192,1024]{1,0:T(8,128)(2,1)}, u32[]{:S(2)}) copy-start(bf16[192,1024]{1,0:T(8,128)(2,1)} %param.11) | copy-start | bytes 1179652
  42.3 11.3 %collective-permute-start.25 = (bf16[144,1024]{1,0:T(8,128)(2,1)}, bf16[144,1024]{1,0:T(8,128)(2,1)}, u32[]{:S(2)}, u32[]{:S(2)}) collective-permute-start(bf16[144,1024]{1,0:T(8,128)(2,1)} %get-tuple-element.53), channel_id=1, source_target_pairs={{0,24},{8,16},{16,8},{24,0},{1,25},{9,17},{17,9},{25,1},{2,26},{10... | collective-permute-start | bytes 884744 | tf_op jit(solution)/shard_map/ppermute | solution.py:88
  52.6 2.6 %copy-start.35 = (bf16[144,1024]{1,0:T(8,128)(2,1)}, bf16[144,1024]{1,0:T(8,128)(2,1)S(1)}, u32[]{:S(2)}) copy-start(bf16[144,1024]{1,0:T(8,128)(2,1)S(1)} %collective-permute-done.24.refs_2_) | copy-start | bytes 884740
  52.6 10.2 %collective-permute-start.26 = (bf16[144,1024]{1,0:T(8,128)(2,1)}, bf16[144,1024]{1,0:T(8,128)(2,1)}, u32[]{:S(2)}, u32[]{:S(2)}) collective-permute-start(bf16[144,1024]{1,0:T(8,128)(2,1)} %get-tuple-element.55), channel_id=1, source_target_pairs={{0,8},{8,0},{16,24},{24,16},{1,9},{9,1},{17,25},{25,17},{2,10},{10... | collective-permute-start | bytes 884744 | tf_op jit(solution)/shard_map/ppermute | solution.py:88
  53.7 15.6 %collective-permute-start.27 = (bf16[144,1024]{1,0:T(8,128)(2,1)}, bf16[144,1024]{1,0:T(8,128)(2,1)}, u32[]{:S(2)}, u32[]{:S(2)}) collective-permute-start(bf16[144,1024]{1,0:T(8,128)(2,1)} %get-tuple-element.56), channel_id=1, source_target_pairs={{0,16},{8,24},{16,0},{24,8},{1,17},{9,25},{17,1},{25,9},{2,18},{10... | collective-permute-start | bytes 884744 | tf_op jit(solution)/shard_map/ppermute | solution.py:88
  55.2 14.1 %copy-start.30 = (bf16[1024,512]{1,0:T(8,128)(2,1)}, bf16[1024,512]{1,0:T(8,128)(2,1)S(1)}, u32[]{:S(2)}) copy-start(bf16[1024,512]{1,0:T(8,128)(2,1)S(1)} %collective-permute-done.12.refs_11_) | copy-start | bytes 3145732
  55.2 14.1 %collective-permute-start.28 = (bf16[144,1024]{1,0:T(8,128)(2,1)}, bf16[144,1024]{1,0:T(8,128)(2,1)}, u32[]{:S(2)}, u32[]{:S(2)}) collective-permute-start(bf16[144,1024]{1,0:T(8,128)(2,1)} %get-tuple-element.57), channel_id=1, source_target_pairs={{0,24},{8,16},{16,8},{24,0},{1,25},{9,17},{17,9},{25,1},{2,26},{10... | collective-permute-start | bytes 884744 | tf_op jit(solution)/shard_map/ppermute | solution.py:88
  56.3 2.3 %copy-start.18 = (f32[4,192]{1,0:T(4,128)S(1)}, f32[4,192]{1,0:T(4,128)}, u32[]{:S(2)}) copy-start(f32[4,192]{1,0:T(4,128)} %copy-done.17) | copy-start | bytes 9220
  58.6 10.7 %copy-start.31 = (bf16[1024,512]{1,0:T(8,128)(2,1)}, bf16[1024,512]{1,0:T(8,128)(2,1)S(1)}, u32[]{:S(2)}) copy-start(bf16[1024,512]{1,0:T(8,128)(2,1)S(1)} %collective-permute-done.13.refs_12_) | copy-start | bytes 3145732
  58.6 26.5 %collective-permute-start.5 = (f32[4,192]{1,0:T(4,128)S(1)}, f32[4,192]{1,0:T(4,128)S(1)}, u32[]{:S(2)}, u32[]{:S(2)}) collective-permute-start(f32[4,192]{1,0:T(4,128)S(1)} %copy-done.18), channel_id=1, source_target_pairs={{0,6},{1,7},{2,0},{3,1},{4,2},{5,3},{6,4},{7,5},{8,14},{9,15},{10,... | collective-permute-start | bytes 9224 | tf_op jit(solution)/shard_map/ppermute | solution.py:72
  58.7 37.6 %collective-permute-start.10 = (bf16[144,1024]{1,0:T(8,128)(2,1)}, bf16[144,1024]{1,0:T(8,128)(2,1)S(1)}, u32[]{:S(2)}, u32[]{:S(2)}) collective-permute-start(bf16[144,1024]{1,0:T(8,128)(2,1)} %get-tuple-element.40), channel_id=1, source_target_pairs={{0,16},{8,24},{16,0},{24,8},{1,17},{9,25},{17,1},{25,9},{2,18},{10... | collective-permute-start | bytes 884744 | tf_op jit(solution)/shard_map/ppermute | solution.py:88
  62.8 34.4 %collective-permute-start.4 = (bf16[192,1024]{1,0:T(8,128)(2,1)}, bf16[192,1024]{1,0:T(8,128)(2,1)}, u32[]{:S(2)}, u32[]{:S(2)}) collective-permute-start(bf16[192,1024]{1,0:T(8,128)(2,1)} %collective-permute-done.3.rows_ref), channel_id=1, source_target_pairs={{0,2},{1,3},{2,4},{3,5},{4,6},{5,7},{6,0},{7,1},{8,10},{9,11},{10,... | collective-permute-start | bytes 1179656 | tf_op jit(solution)/shard_map/ppermute | solution.py:72
  69.3 14.4 %copy-start.22 = (f32[1024]{0:T(1024)S(1)}, f32[1024]{0:T(1024)}, u32[]{:S(2)}) copy-start(f32[1024]{0:T(1024)} %param.12) | copy-start | bytes 12292
  82.5 15.3 %collective-permute-start.32 = (bf16[144,1024]{1,0:T(8,128)(2,1)}, bf16[144,1024]{1,0:T(8,128)(2,1)S(1)}, u32[]{:S(2)}, u32[]{:S(2)}) collective-permute-start(bf16[144,1024]{1,0:T(8,128)(2,1)} %get-tuple-element.63), channel_id=1, source_target_pairs={{0,8},{8,0},{16,24},{24,16},{1,9},{9,1},{17,25},{25,17},{2,10},{10... | collective-permute-start | bytes 884744 | tf_op jit(solution)/shard_map/ppermute | solution.py:88
  83.9 2.6 %collective-permute-start = (bf16[8,1024]{1,0:T(8,128)(2,1)S(1)}, bf16[8,1024]{1,0:T(8,128)(2,1)S(1)}, u32[]{:S(2)}, u32[]{:S(2)}) collective-permute-start(bf16[8,1024]{1,0:T(8,128)(2,1)S(1)} %get-tuple-element.71), channel_id=1, source_target_pairs={{0,1},{1,2},{2,3},{3,4},{4,5},{5,6},{6,7},{7,8},{8,9},{9,10},{10,1... | collective-permute-start | bytes 49160 | tf_op jit(solution)/shard_map/ppermute | solution.py:18
  85.2 12.0 %copy-start.24 = (f32[4,192]{1,0:T(4,128)}, f32[4,192]{1,0:T(4,128)S(1)}, u32[]{:S(2)}) copy-start(f32[4,192]{1,0:T(4,128)S(1)} %collective-permute-done.5.table_ref) | copy-start | bytes 9220
  85.2 9.2 %collective-permute-start.1 = (bf16[8,1024]{1,0:T(8,128)(2,1)S(1)}, bf16[8,1024]{1,0:T(8,128)(2,1)}, u32[]{:S(2)}, u32[]{:S(2)}) collective-permute-start(bf16[8,1024]{1,0:T(8,128)(2,1)S(1)} %get-tuple-element.72), channel_id=1, source_target_pairs={{1,0},{2,1},{3,2},{4,3},{5,4},{6,5},{7,6},{8,7},{9,8},{10,9},{11,1... | collective-permute-start | bytes 49160 | tf_op jit(solution)/shard_map/ppermute | solution.py:19
  86.5 26.7 %collective-permute-start.33 = (bf16[144,1024]{1,0:T(8,128)(2,1)}, bf16[144,1024]{1,0:T(8,128)(2,1)S(1)}, u32[]{:S(2)}, u32[]{:S(2)}) collective-permute-start(bf16[144,1024]{1,0:T(8,128)(2,1)} %get-tuple-element.64), channel_id=1, source_target_pairs={{0,16},{8,24},{16,0},{24,8},{1,17},{9,25},{17,1},{25,9},{2,18},{10... | collective-permute-start | bytes 884744 | tf_op jit(solution)/shard_map/ppermute | solution.py:88
  94.4 22.2 %collective-permute-start.34 = (bf16[144,1024]{1,0:T(8,128)(2,1)}, bf16[144,1024]{1,0:T(8,128)(2,1)S(1)}, u32[]{:S(2)}, u32[]{:S(2)}) collective-permute-start(bf16[144,1024]{1,0:T(8,128)(2,1)} %get-tuple-element.65), channel_id=1, source_target_pairs={{0,24},{8,16},{16,8},{24,0},{1,25},{9,17},{17,9},{25,1},{2,26},{10... | collective-permute-start | bytes 884744 | tf_op jit(solution)/shard_map/ppermute | solution.py:88
  96.3 6.3 %copy-start.32 = (bf16[144,1024]{1,0:T(8,128)(2,1)}, bf16[144,1024]{1,0:T(8,128)(2,1)S(1)}, u32[]{:S(2)}) copy-start(bf16[144,1024]{1,0:T(8,128)(2,1)S(1)} %collective-permute-done.10.refs_6_) | copy-start | bytes 884740
  96.3 20.3 %collective-permute-start.29 = (bf16[144,1024]{1,0:T(8,128)(2,1)}, bf16[144,1024]{1,0:T(8,128)(2,1)S(1)}, u32[]{:S(2)}, u32[]{:S(2)}) collective-permute-start(bf16[144,1024]{1,0:T(8,128)(2,1)} %get-tuple-element.59), channel_id=1, source_target_pairs={{0,8},{8,0},{16,24},{24,16},{1,9},{9,1},{17,25},{25,17},{2,10},{10... | collective-permute-start | bytes 884744 | tf_op jit(solution)/shard_map/ppermute | solution.py:88
  97.2 24.3 %collective-permute-start.30 = (bf16[144,1024]{1,0:T(8,128)(2,1)}, bf16[144,1024]{1,0:T(8,128)(2,1)S(1)}, u32[]{:S(2)}, u32[]{:S(2)}) collective-permute-start(bf16[144,1024]{1,0:T(8,128)(2,1)} %get-tuple-element.60), channel_id=1, source_target_pairs={{0,16},{8,24},{16,0},{24,8},{1,17},{9,25},{17,1},{25,9},{2,18},{10... | collective-permute-start | bytes 884744 | tf_op jit(solution)/shard_map/ppermute | solution.py:88
  97.9 4.7 %copy-start.5 = (bf16[144,1024]{1,0:T(8,128)(2,1)}, bf16[144,1024]{1,0:T(8,128)(2,1)S(1)}, u32[]{:S(2)}) copy-start(bf16[144,1024]{1,0:T(8,128)(2,1)S(1)} %collective-permute-done.32.refs_1_) | copy-start | bytes 884740
  97.9 26.5 %collective-permute-start.31 = (bf16[144,1024]{1,0:T(8,128)(2,1)}, bf16[144,1024]{1,0:T(8,128)(2,1)S(1)}, u32[]{:S(2)}, u32[]{:S(2)}) collective-permute-start(bf16[144,1024]{1,0:T(8,128)(2,1)} %get-tuple-element.61), channel_id=1, source_target_pairs={{0,24},{8,16},{16,8},{24,0},{1,25},{9,17},{17,9},{25,1},{2,26},{10... | collective-permute-start | bytes 884744 | tf_op jit(solution)/shard_map/ppermute | solution.py:88
  113.2 12.6 %copy-start.6 = (bf16[144,1024]{1,0:T(8,128)(2,1)}, bf16[144,1024]{1,0:T(8,128)(2,1)S(1)}, u32[]{:S(2)}) copy-start(bf16[144,1024]{1,0:T(8,128)(2,1)S(1)} %collective-permute-done.33.refs_2_) | copy-start | bytes 884740
  113.2 20.1 %collective-permute-start.11 = (bf16[144,1024]{1,0:T(8,128)(2,1)}, bf16[144,1024]{1,0:T(8,128)(2,1)S(1)}, u32[]{:S(2)}, u32[]{:S(2)}) collective-permute-start(bf16[144,1024]{1,0:T(8,128)(2,1)} %get-tuple-element.41), channel_id=1, source_target_pairs={{0,24},{8,16},{16,8},{24,0},{1,25},{9,17},{17,9},{25,1},{2,26},{10... | collective-permute-start | bytes 884744 | tf_op jit(solution)/shard_map/ppermute | solution.py:88
  116.6 9.2 %copy-start.7 = (bf16[144,1024]{1,0:T(8,128)(2,1)}, bf16[144,1024]{1,0:T(8,128)(2,1)S(1)}, u32[]{:S(2)}) copy-start(bf16[144,1024]{1,0:T(8,128)(2,1)S(1)} %collective-permute-done.34.refs_3_) | copy-start | bytes 884740
  116.6 16.7 %collective-permute-start.9 = (bf16[144,1024]{1,0:T(8,128)(2,1)}, bf16[144,1024]{1,0:T(8,128)(2,1)}, u32[]{:S(2)}, u32[]{:S(2)}) collective-permute-start(bf16[144,1024]{1,0:T(8,128)(2,1)} %get-tuple-element.39), channel_id=1, source_target_pairs={{0,8},{8,0},{16,24},{24,16},{1,9},{9,1},{17,25},{25,17},{2,10},{10... | collective-permute-start | bytes 884744 | tf_op jit(solution)/shard_map/ppermute | solution.py:88
  116.6 9.2 %copy-start.8 = (bf16[144,1024]{1,0:T(8,128)(2,1)}, bf16[144,1024]{1,0:T(8,128)(2,1)S(1)}, u32[]{:S(2)}) copy-start(bf16[144,1024]{1,0:T(8,128)(2,1)S(1)} %collective-permute-done.29.refs_1_) | copy-start | bytes 884740
  116.6 18.0 %collective-permute-start.6 = (bf16[144,1024]{1,0:T(8,128)(2,1)}, bf16[144,1024]{1,0:T(8,128)(2,1)}, u32[]{:S(2)}, u32[]{:S(2)}) collective-permute-start(bf16[144,1024]{1,0:T(8,128)(2,1)} %get-tuple-element.35), channel_id=1, source_target_pairs={{0,8},{8,0},{16,24},{24,16},{1,9},{9,1},{17,25},{25,17},{2,10},{10... | collective-permute-start | bytes 884744 | tf_op jit(solution)/shard_map/ppermute | solution.py:88
  121.5 4.3 %copy-start.9 = (bf16[144,1024]{1,0:T(8,128)(2,1)}, bf16[144,1024]{1,0:T(8,128)(2,1)S(1)}, u32[]{:S(2)}) copy-start(bf16[144,1024]{1,0:T(8,128)(2,1)S(1)} %collective-permute-done.30.refs_2_) | copy-start | bytes 884740
  121.5 13.1 %collective-permute-start.7 = (bf16[144,1024]{1,0:T(8,128)(2,1)}, bf16[144,1024]{1,0:T(8,128)(2,1)}, u32[]{:S(2)}, u32[]{:S(2)}) collective-permute-start(bf16[144,1024]{1,0:T(8,128)(2,1)} %get-tuple-element.36), channel_id=1, source_target_pairs={{0,16},{8,24},{16,0},{24,8},{1,17},{9,25},{17,1},{25,9},{2,18},{10... | collective-permute-start | bytes 884744 | tf_op jit(solution)/shard_map/ppermute | solution.py:88
  124.4 4.6 %copy-start.10 = (bf16[144,1024]{1,0:T(8,128)(2,1)}, bf16[144,1024]{1,0:T(8,128)(2,1)S(1)}, u32[]{:S(2)}) copy-start(bf16[144,1024]{1,0:T(8,128)(2,1)S(1)} %collective-permute-done.31.refs_3_) | copy-start | bytes 884740
  124.4 13.5 %collective-permute-start.8 = (bf16[144,1024]{1,0:T(8,128)(2,1)}, bf16[144,1024]{1,0:T(8,128)(2,1)}, u32[]{:S(2)}, u32[]{:S(2)}) collective-permute-start(bf16[144,1024]{1,0:T(8,128)(2,1)} %get-tuple-element.37), channel_id=1, source_target_pairs={{0,24},{8,16},{16,8},{24,0},{1,25},{9,17},{17,9},{25,1},{2,26},{10... | collective-permute-start | bytes 884744 | tf_op jit(solution)/shard_map/ppermute | solution.py:88
  133.3 4.5 %copy-start.33 = (bf16[144,1024]{1,0:T(8,128)(2,1)}, bf16[144,1024]{1,0:T(8,128)(2,1)S(1)}, u32[]{:S(2)}) copy-start(bf16[144,1024]{1,0:T(8,128)(2,1)S(1)} %collective-permute-done.11.refs_7_) | copy-start | bytes 884740
  133.3 21.4 %collective-permute-start.35 = (bf16[192,1024]{1,0:T(8,128)(2,1)S(1)}, bf16[192,1024]{1,0:T(8,128)(2,1)S(1)}, u32[]{:S(2)}, u32[]{:S(2)}) collective-permute-start(bf16[192,1024]{1,0:T(8,128)(2,1)S(1)} %convert_element_type.100), channel_id=1, source_target_pairs={{0,2},{1,3},{2,4},{3,5},{4,6},{5,7},{6,0},{7,1},{8,10},{9,11},{10,... | collective-permute-start | bytes 1179656 | tf_op jit(solution)/shard_map/ppermute | solution.py:72
  137.8 16.8 %copy-start.1 = (f32[192,1024]{1,0:T(8,128)S(1)}, f32[192,1024]{1,0:T(8,128)}, u32[]{:S(2)}) copy-start(f32[192,1024]{1,0:T(8,128)} %combine.6) | copy-start | bytes 2359300
  151.1 9.4 %collective-permute-start.18 = (bf16[144,1024]{1,0:T(8,128)(2,1)}, bf16[144,1024]{1,0:T(8,128)(2,1)S(1)}, u32[]{:S(2)}, u32[]{:S(2)}) collective-permute-start(bf16[144,1024]{1,0:T(8,128)(2,1)} %get-tuple-element.47), channel_id=1, source_target_pairs={{0,8},{8,0},{16,24},{24,16},{1,9},{9,1},{17,25},{25,17},{2,10},{10... | collective-permute-start | bytes 884744 | tf_op jit(solution)/shard_map/ppermute | solution.py:88
  152.8 10.2 %collective-permute-start.19 = (bf16[144,1024]{1,0:T(8,128)(2,1)}, bf16[144,1024]{1,0:T(8,128)(2,1)S(1)}, u32[]{:S(2)}, u32[]{:S(2)}) collective-permute-start(bf16[144,1024]{1,0:T(8,128)(2,1)} %get-tuple-element.48), channel_id=1, source_target_pairs={{0,16},{8,24},{16,0},{24,8},{1,17},{9,25},{17,1},{25,9},{2,18},{10... | collective-permute-start | bytes 884744 | tf_op jit(solution)/shard_map/ppermute | solution.py:88
  154.4 13.5 %collective-permute-start.20 = (bf16[144,1024]{1,0:T(8,128)(2,1)}, bf16[144,1024]{1,0:T(8,128)(2,1)}, u32[]{:S(2)}, u32[]{:S(2)}) collective-permute-start(bf16[144,1024]{1,0:T(8,128)(2,1)} %get-tuple-element.49), channel_id=1, source_target_pairs={{0,24},{8,16},{16,8},{24,0},{1,25},{9,17},{17,9},{25,1},{2,26},{10... | collective-permute-start | bytes 884744 | tf_op jit(solution)/shard_map/ppermute | solution.py:88
  154.8 1.4 copy-start.27
  154.8 16.3 %collective-permute-start.36 = (bf16[192,1024]{1,0:T(8,128)(2,1)S(1)}, bf16[192,1024]{1,0:T(8,128)(2,1)S(1)}, u32[]{:S(2)}, u32[]{:S(2)}) collective-permute-start(bf16[192,1024]{1,0:T(8,128)(2,1)S(1)} %add_convert_fusion.2), channel_id=1, source_target_pairs={{0,2},{1,3},{2,4},{3,5},{4,6},{5,7},{6,0},{7,1},{8,10},{9,11},{10,... | collective-permute-start | bytes 1179656 | tf_op jit(solution)/shard_map/ppermute | solution.py:72
  158.0 19.2 %collective-permute-start.15 = (bf16[144,1024]{1,0:T(8,128)(2,1)}, bf16[144,1024]{1,0:T(8,128)(2,1)S(1)}, u32[]{:S(2)}, u32[]{:S(2)}) collective-permute-start(bf16[144,1024]{1,0:T(8,128)(2,1)} %get-tuple-element.43), channel_id=1, source_target_pairs={{0,8},{8,0},{16,24},{24,16},{1,9},{9,1},{17,25},{25,17},{2,10},{10... | collective-permute-start | bytes 884744 | tf_op jit(solution)/shard_map/ppermute | solution.py:88
  160.5 7.4 %copy-start.12 = (bf16[144,1024]{1,0:T(8,128)(2,1)}, bf16[144,1024]{1,0:T(8,128)(2,1)S(1)}, u32[]{:S(2)}) copy-start(bf16[144,1024]{1,0:T(8,128)(2,1)S(1)} %collective-permute-done.18.refs_1_) | copy-start | bytes 884740
  160.5 17.3 %collective-permute-start.16 = (bf16[144,1024]{1,0:T(8,128)(2,1)}, bf16[144,1024]{1,0:T(8,128)(2,1)S(1)}, u32[]{:S(2)}, u32[]{:S(2)}) collective-permute-start(bf16[144,1024]{1,0:T(8,128)(2,1)} %get-tuple-element.44), channel_id=1, source_target_pairs={{0,16},{8,24},{16,0},{24,8},{1,17},{9,25},{17,1},{25,9},{2,18},{10... | collective-permute-start | bytes 884744 | tf_op jit(solution)/shard_map/ppermute | solution.py:88
  163.0 4.9 %copy-start.14 = (bf16[144,1024]{1,0:T(8,128)(2,1)}, bf16[144,1024]{1,0:T(8,128)(2,1)S(1)}, u32[]{:S(2)}) copy-start(bf16[144,1024]{1,0:T(8,128)(2,1)S(1)} %collective-permute-done.19.refs_2_) | copy-start | bytes 884740
  163.0 14.8 %collective-permute-start.17 = (bf16[144,1024]{1,0:T(8,128)(2,1)}, bf16[144,1024]{1,0:T(8,128)(2,1)}, u32[]{:S(2)}, u32[]{:S(2)}) collective-permute-start(bf16[144,1024]{1,0:T(8,128)(2,1)} %get-tuple-element.45), channel_id=1, source_target_pairs={{0,24},{8,16},{16,8},{24,0},{1,25},{9,17},{17,9},{25,1},{2,26},{10... | collective-permute-start | bytes 884744 | tf_op jit(solution)/shard_map/ppermute | solution.py:88
  171.1 4.3 %copy-start.15 = (bf16[192,1,256]{2,0,1:T(8,128)(2,1)S(1)}, bf16[192,1,256]{2,0,1:T(8,128)(2,1)}, u32[]{:S(2)}) copy-start(bf16[192,1,256]{2,0,1:T(8,128)(2,1)} %get-tuple-element.69) | copy-start | bytes 294916
  171.1 4.3 %copy-start.16 = (bf16[192,1,256]{2,0,1:T(8,128)(2,1)S(1)}, bf16[192,1,256]{2,0,1:T(8,128)(2,1)}, u32[]{:S(2)}) copy-start(bf16[192,1,256]{2,0,1:T(8,128)(2,1)} %get-tuple-element.70) | copy-start | bytes 294916
  172.3 13.6 %collective-permute-start.37 = (bf16[192,1024]{1,0:T(8,128)(2,1)S(1)}, bf16[192,1024]{1,0:T(8,128)(2,1)S(1)}, u32[]{:S(2)}, u32[]{:S(2)}) collective-permute-start(bf16[192,1024]{1,0:T(8,128)(2,1)S(1)} %add_convert_fusion.1), channel_id=1, source_target_pairs={{0,2},{1,3},{2,4},{3,5},{4,6},{5,7},{6,0},{7,1},{8,10},{9,11},{10,... | collective-permute-start | bytes 1179656 | tf_op jit(solution)/shard_map/ppermute | solution.py:72
  (10 other events, 7.2 us)

commit v3 on v2

--- a/solution.py
+++ b/solution.py
@@ -67,9 +67,14 @@
 CORES = 2
 
 
-def ring(value, steps=1):
+def shift(value, steps):
     size = lax.axis_size("tp")
     return lax.ppermute(value, "tp", [(i, (i + steps * CORES) % size) for i in range(size)])
+
+
+def serving_order(chips):
+    relayed = [n for even in range(2, chips, 2) for n in (even, even - 1)]
+    return relayed + [n for n in range(1, chips) if n not in relayed] + [0]
 
 
 def core_swap(value):
@@ -155,7 +160,7 @@
     )(rows, table)
 
 
-def combine(pieces, table):
+def combine(pieces, table, others=()):
     top_count = table.shape[0] // 2
     capacity, width = pieces[0].shape
     row_count = table.shape[1]
@@ -163,6 +168,8 @@
     def kernel(table_ref, *refs):
         out_ref = refs[-1]
         total = jnp.zeros((row_count, width), jnp.float32)
+        for other_ref in refs[len(pieces) : -1]:
+            total = total + other_ref[...].astype(jnp.float32)
         for m in range(len(pieces)):
             hits = slot_hits(table_ref, top_count, m * capacity, capacity)
             weight = jnp.zeros(hits[0].shape, jnp.float32)
@@ -177,17 +184,17 @@
                     (((0,), (0,)), ((), ())),
                     preferred_element_type=jnp.float32,
                 )
-        out_ref[...] = total
+        out_ref[...] = total.astype(jnp.bfloat16)
 
     work = len(pieces) * capacity * row_count * width
     return pl.pallas_call(
         kernel,
-        out_shape=jax.ShapeDtypeStruct((row_count, width), jnp.float32),
+        out_shape=jax.ShapeDtypeStruct((row_count, width), jnp.bfloat16),
         cost_estimate=pl.CostEstimate(
             flops=4 * work, transcendentals=0, bytes_accessed=2 * (len(pieces) * capacity + 2 * row_count) * width
         ),
         name="combine",
-    )(table, *pieces)
+    )(table, *pieces, *others)
 
 
 def ffn(pieces, shards):
@@ -281,17 +288,17 @@
     shard = (w_gate[0], w_up[0], w_down[0])
     shards = [shard, tuple(core_swap(w) for w in shard)]
 
+    order = serving_order(chips)
     table = route_table(routes, route_weight, experts, capacity)
-    blocks = [normed]
-    for _ in range(1, chips):
-        blocks.append(ring(blocks[-1]))
-    tables = [table] + [ring(table, n) for n in range(1, chips)]
-
-    arrived = []
+    blocks, tables = {0: normed}, {0: table}
+    for n in range(1, chips):
+        blocks[n] = shift(normed, n) if n % 2 else shift(blocks[n - 1], 1)
+        tables[n] = shift(table, n)
+
+    arrived = {}
     for n in range(chips):
-        arrived.append(exchange(dispatch(blocks[n], tables[n], experts, capacity)))
-
-    order = list(range(1, chips)) + [0]
+        arrived[n] = exchange(dispatch(blocks[n], tables[n], experts, capacity))
+
     back = {}
     for first in range(0, chips, 2):
         group = order[first : first + 2]
@@ -299,16 +306,17 @@
         for place, n in enumerate(group):
             back[n] = exchange(served[place * experts : (place + 1) * experts])
 
-    total = None
-    for n in order:
-        term = combine(back[n], tables[n])
-        total = term if total is None else term + total.astype(jnp.float32)
-        total = total.astype(jnp.bfloat16)
-        if n:
-            total = ring(total)
+    home, relayed = [], {}
+    for n in order[:-1]:
+        term = combine(back[n], tables[n], relayed.get(n, ()))
+        if n % 2:
+            home.append(shift(term, -n))
+        else:
+            relayed[n - 1] = (shift(term, -1),)
+    expert_out = combine(back[0], tables[0], home)
 
     mixer_out = mixer(mixer_input, mixer_gain, group_weight, mixer_scale)
-    return (mixer_out, total)
+    return (mixer_out, expert_out)
 
 
 def solution(mesh):

time: 189 us -> 185 us (0.979)
  other arithmetic: 10.8 us -> 4.43 us
  starting transfers between devices: 54.3 us -> 56.6 us
    ppermute x9, waiting for transfers between devices: 26.2 us -> 32.1 us  [shift(): lax.ppermute(value, 'tp', [(i, (i + steps * CORES) % size) for i in range...]
    ppermute x24, waiting for transfers between devices: 42.8 us -> 37 us  [exchange(): lax.ppermute(pieces[m], 'ep', [(i, i ^ m) for i in range(count)])]
    ppermute x9, starting transfers between devices: 8.94 us -> 13.7 us  [shift(): lax.ppermute(value, 'tp', [(i, (i + steps * CORES) % size) for i in range...]
    convert_element_type x4 -> x0, other arithmetic: 4.49 us -> none  [on_device(): total = total.astype(jnp.bfloat16)]
    ppermute x24, starting transfers between devices: 42.3 us -> 39.7 us  [exchange(): lax.ppermute(pieces[m], 'ep', [(i, i ^ m) for i in range(count)])]
  transfers between devices with their start and end apart: 38 -> 38, of which waited for: 16 -> 14; matrix products, arithmetic and copies ran while one was open for 4% -> 2% of each run, Pallas kernels for 26% -> 24%
where the time goes in v3:
time: 185 us
  waiting for transfers between devices  69.1 us (37%)
  starting transfers between devices  56.6 us (31%)
  Pallas kernels  48.4 us (26%)
  local copies, waits for them, and re-layouts  4.94 us (3%)
  other arithmetic  4.43 us (2%)
    ppermute x24, starting transfers between devices, exchange(): lax.ppermute(pieces[m], 'ep', [(i, i ^ m) for i in range(count)])  39.7 us
    ppermute x24, waiting for transfers between devices, exchange(): lax.ppermute(pieces[m], 'ep', [(i, i ^ m) for i in range(count)])  37 us
    ppermute x9, waiting for transfers between devices, shift(): lax.ppermute(value, 'tp', [(i, (i + steps * CORES) % size) for i in range...  32.1 us
    pallas_call x2, Pallas kernels, ffn(): pl.pallas_call(kernel, grid=(steps,), in_specs=[whole] * count + [across,...  26.6 us
    ppermute x9, starting transfers between devices, shift(): lax.ppermute(value, 'tp', [(i, (i + steps * CORES) % size) for i in range...  13.7 us
    pallas_call x4, Pallas kernels, combine(): pl.pallas_call(kernel, out_shape=jax.ShapeDtypeStruct((row_count, width),...  12.5 us
    pallas_call x4, Pallas kernels, dispatch(): pl.pallas_call(kernel, out_shape=[shape] * experts, cost_estimate=pl.Cost...  9.32 us
    unnamed x72, local copies, waits for them, and re-layouts  4.86 us
  transfers between devices with their start and end apart: 38, of which 14 were waited for; matrix products, arithmetic and copies ran while one was open for 2% of the time, Pallas kernels for 24%

profile of v3, /device:TPU:0, one launch (start us, length us, event | category | flops | bytes accessed | tf_op | source)
XLA Modules:
  0.0 184.9 jit_solution(16150009290004858863)
XLA Ops:
  0.7 1.2 fusion.3
  1.9 0.8 fusion.5.rows_ref
  2.8 5.1 %collective-permute-start.2 = (bf16[192,1024]{1,0:T(8,128)(2,1)S(1)}, bf16[192,1024]{1,0:T(8,128)(2,1)S(1)}, u32[]{:S(2)}, u32[]{:S(2)}) collective-permute-start(bf16[192,1024]{1,0:T(8,128)(2,1)S(1)} %fusion.5.rows_ref), channel_id=1, source_target_pairs={{0,6},{1,7},{2,0},{3,1},{4,2},{5,3},{6,4},{7,5},{8,14},{9,15},{10,... | collective-permute-start | bytes 1179656 | tf_op jit(solution)/shard_map/ppermute | solution.py:72
  7.9 0.7 copy-done.17
  8.8 0.7 copy-done.18
  9.5 0.6 pad_maximum_fusion.table_ref
  10.1 2.3 %dispatch.5 = (bf16[144,1024]{1,0:T(8,128)(2,1)}, bf16[144,1024]{1,0:T(8,128)(2,1)}, bf16[144,1024]{1,0:T(8,128)(2,1)}, bf16[144,1024]{1,0:T(8,128)(2,1)}) custom-call(bf16[192,1024]{1,0:T(8,128)(2,1)} %copy-done.5, f32[4,192]{1,0:T(4,128)} %pad_maximum_fusion.table_ref), custom_call_target="tpu_custom_call" | custom-call | flops 226492416 | bytes 1572864 | tf_op jit(solution)/shard_map/dispatch/pallas_call | solution.py:153
  12.4 1.5 collective-permute-start.7
  13.9 11.7 %collective-permute-done.17.rows_ref = bf16[192,1024]{1,0:T(8,128)(2,1)S(1)} collective-permute-done((bf16[192,1024]{1,0:T(8,128)(2,1)S(1)}, bf16[192,1024]{1,0:T(8,128)(2,1)S(1)}, u32[]{:S(2)}, u32[]{:S(2)}) %collective-permute-start.17) | collective-permute-done | bytes 393248 | tf_op jit(solution)/shard_map/ppermute | solution.py:72
  25.6 1.6 collective-permute-start.18
  27.2 2.2 %collective-permute-start.3 = (f32[4,192]{1,0:T(4,128)S(1)}, f32[4,192]{1,0:T(4,128)S(1)}, u32[]{:S(2)}, u32[]{:S(2)}) collective-permute-start(f32[4,192]{1,0:T(4,128)S(1)} %copy-done.13), channel_id=1, source_target_pairs={{0,6},{1,7},{2,0},{3,1},{4,2},{5,3},{6,4},{7,5},{8,14},{9,15},{10,... | collective-permute-start | bytes 9224 | tf_op jit(solution)/shard_map/ppermute | solution.py:72
  29.4 5.5 %collective-permute-done.3.table_ref = f32[4,192]{1,0:T(4,128)S(1)} collective-permute-done((f32[4,192]{1,0:T(4,128)S(1)}, f32[4,192]{1,0:T(4,128)S(1)}, u32[]{:S(2)}, u32[]{:S(2)}) %collective-permute-start.3) | collective-permute-done | bytes 3104 | tf_op jit(solution)/shard_map/ppermute | solution.py:72
  34.9 0.6 copy-done.34
  35.5 5.3 %collective-permute-done.16.table_ref = f32[4,192]{1,0:T(4,128)S(1)} collective-permute-done((f32[4,192]{1,0:T(4,128)S(1)}, f32[4,192]{1,0:T(4,128)S(1)}, u32[]{:S(2)}, u32[]{:S(2)}) %collective-permute-start.16) | collective-permute-done | bytes 3104 | tf_op jit(solution)/shard_map/ppermute | solution.py:72
  40.8 0.9 collective-permute-start.19
  41.7 2.3 %dispatch.7 = (bf16[144,1024]{1,0:T(8,128)(2,1)}, bf16[144,1024]{1,0:T(8,128)(2,1)}, bf16[144,1024]{1,0:T(8,128)(2,1)}, bf16[144,1024]{1,0:T(8,128)(2,1)}) custom-call(bf16[192,1024]{1,0:T(8,128)(2,1)} %copy-done.21, f32[4,192]{1,0:T(4,128)} %copy-done.16), custom_call_target="tpu_custom_call" | custom-call | flops 226492416 | bytes 1572864 | tf_op jit(solution)/shard_map/dispatch/pallas_call | solution.py:153
  44.0 1.3 collective-permute-done.19.table_ref
  45.3 0.5 collective-permute-start.12
  45.8 1.5 collective-permute-start.23
  47.5 7.5 %collective-permute-done.23.refs_5_ = bf16[144,1024]{1,0:T(8,128)(2,1)S(1)} collective-permute-done((bf16[144,1024]{1,0:T(8,128)(2,1)}, bf16[144,1024]{1,0:T(8,128)(2,1)S(1)}, u32[]{:S(2)}, u32[]{:S(2)}) %collective-permute-start.23) | collective-permute-done | bytes 294944 | tf_op jit(solution)/shard_map/ppermute | solution.py:93
  55.0 1.5 collective-permute-start.24
  56.6 1.4 collective-permute-start.25
  58.2 2.3 %dispatch.6 = (bf16[144,1024]{1,0:T(8,128)(2,1)}, bf16[144,1024]{1,0:T(8,128)(2,1)}, bf16[144,1024]{1,0:T(8,128)(2,1)}, bf16[144,1024]{1,0:T(8,128)(2,1)}) custom-call(bf16[192,1024]{1,0:T(8,128)(2,1)} %collective-permute-done.18.rows_ref, f32[4,192]{1,0:T(4,128)} %copy-done.35), custom_call_target="tpu_custom_call" | custom-call | flops 226492416 | bytes 1572864 | tf_op jit(solution)/shard_map/dispatch/pallas_call | solution.py:153
  60.5 9.3 %collective-permute-done.24.refs_6_ = bf16[144,1024]{1,0:T(8,128)(2,1)} collective-permute-done((bf16[144,1024]{1,0:T(8,128)(2,1)}, bf16[144,1024]{1,0:T(8,128)(2,1)}, u32[]{:S(2)}, u32[]{:S(2)}) %collective-permute-start.24) | collective-permute-done | bytes 294944 | tf_op jit(solution)/shard_map/ppermute | solution.py:93
  69.8 1.5 collective-permute-start.20
  71.3 1.5 collective-permute-start.21
  73.3 2.4 %dispatch.4 = (bf16[144,1024]{1,0:T(8,128)(2,1)}, bf16[144,1024]{1,0:T(8,128)(2,1)}, bf16[144,1024]{1,0:T(8,128)(2,1)}, bf16[144,1024]{1,0:T(8,128)(2,1)}) custom-call(bf16[192,1024]{1,0:T(8,128)(2,1)} %copy-done.20, f32[4,192]{1,0:T(4,128)} %copy-done.34), custom_call_target="tpu_custom_call" | custom-call | flops 226492416 | bytes 1572864 | tf_op jit(solution)/shard_map/dispatch/pallas_call | solution.py:153
  75.7 1.6 collective-permute-start.8
  77.3 1.4 collective-permute-start.9
  78.7 1.2 collective-permute-done.20.refs_1_
  79.9 1.5 collective-permute-start.4
  81.4 12.7 %collective-permute-done.21.refs_2_ = bf16[144,1024]{1,0:T(8,128)(2,1)} collective-permute-done((bf16[144,1024]{1,0:T(8,128)(2,1)}, bf16[144,1024]{1,0:T(8,128)(2,1)}, u32[]{:S(2)}, u32[]{:S(2)}) %collective-permute-start.21) | collective-permute-done | bytes 294944 | tf_op jit(solution)/shard_map/ppermute | solution.py:93
  94.1 1.5 collective-permute-start.5
  95.6 13.2 %ffn.3 = (bf16[144,1024]{1,0:T(8,128)(2,1)}, bf16[144,1024]{1,0:T(8,128)(2,1)}, bf16[144,1024]{1,0:T(8,128)(2,1)}, bf16[144,1024]{1,0:T(8,128)(2,1)}, bf16[144,1...) custom-call(bf16[144,1024]{1,0:T(8,128)(2,1)} %get-tuple-element.46.refs_0_,, ...), custom_call_target="tpu_custom_call" | custom-call | flops 7247757312 | bytes 11010048 | tf_op jit(solution)/shard_map/ffn/pallas_call | solution.py:250
  108.9 1.3 collective-permute-start
  110.2 1.5 collective-permute-start.1
  111.7 7.7 %collective-permute-start.29 = (bf16[144,1024]{1,0:T(8,128)(2,1)}, bf16[144,1024]{1,0:T(8,128)(2,1)S(1)}, u32[]{:S(2)}, u32[]{:S(2)}) collective-permute-start(bf16[144,1024]{1,0:T(8,128)(2,1)} %get-tuple-element.59), channel_id=1, source_target_pairs={{0,8},{8,0},{16,24},{24,16},{1,9},{9,1},{17,25},{25,17},{2,10},{10... | collective-permute-start | bytes 884744 | tf_op jit(solution)/shard_map/ppermute | solution.py:93
  119.4 1.5 collective-permute-start.30
  120.9 1.0 collective-permute-start.31
  121.9 13.4 %ffn.2 = (bf16[144,1024]{1,0:T(8,128)(2,1)}, bf16[144,1024]{1,0:T(8,128)(2,1)}, bf16[144,1024]{1,0:T(8,128)(2,1)}, bf16[144,1024]{1,0:T(8,128)(2,1)}, bf16[144,1...) custom-call(bf16[144,1024]{1,0:T(8,128)(2,1)} %get-tuple-element.34.refs_0_,, ...), custom_call_target="tpu_custom_call" | custom-call | flops 7247757312 | bytes 11010048 | tf_op jit(solution)/shard_map/ffn/pallas_call | solution.py:250
  135.3 1.0 collective-permute-start.34
  136.4 1.5 collective-permute-start.35
  138.0 1.1 collective-permute-start.36
  139.1 3.0 %combine.4 = bf16[192,1024]{1,0:T(8,128)(2,1)} custom-call(f32[4,192]{1,0:T(4,128)} %copy-done.35, bf16[144,1024]{1,0:T(8,128)(2,1)} %get-tuple-element.58.refs_0_, bf16[144,1024]{1,0:T(8,128)(2,1)} %copy-done.33, bf16[144,1024]{1,0:T(8,128)(2,1)} %collective-permute-done.30.refs_2_, bf16[144,1024]{1,0:T(8,128)(2,1)} %collective-permute-done.31.refs_3_), custom_call_target="tpu_custom_call" | custom-call | flops 452984832 | bytes 1966080 | tf_op jit(solution)/shard_map/combine/pallas_call | solution.py:190
  142.3 1.2 collective-permute-start.26
  143.5 0.7 copy-done.32
  144.2 1.4 collective-permute-start.27
  145.6 0.8 collective-permute-done.35.refs_2_
  146.3 1.9 %collective-permute-start.28 = (bf16[144,1024]{1,0:T(8,128)(2,1)}, bf16[144,1024]{1,0:T(8,128)(2,1)S(1)}, u32[]{:S(2)}, u32[]{:S(2)}) collective-permute-start(bf16[144,1024]{1,0:T(8,128)(2,1)} %get-tuple-element.57), channel_id=1, source_target_pairs={{0,24},{8,16},{16,8},{24,0},{1,25},{9,17},{17,9},{25,1},{2,26},{10... | collective-permute-start | bytes 884744 | tf_op jit(solution)/shard_map/ppermute | solution.py:93
  148.5 1.2 collective-permute-done.36.refs_3_
  149.7 2.1 %collective-permute-start.13 = (bf16[144,1024]{1,0:T(8,128)(2,1)}, bf16[144,1024]{1,0:T(8,128)(2,1)S(1)}, u32[]{:S(2)}, u32[]{:S(2)}) collective-permute-start(bf16[144,1024]{1,0:T(8,128)(2,1)} %get-tuple-element.43), channel_id=1, source_target_pairs={{0,8},{8,0},{16,24},{24,16},{1,9},{9,1},{17,25},{25,17},{2,10},{10... | collective-permute-start | bytes 884744 | tf_op jit(solution)/shard_map/ppermute | solution.py:93
  151.8 3.0 %combine.6 = bf16[192,1024]{1,0:T(8,128)(2,1)} custom-call(f32[4,192]{1,0:T(4,128)} %copy-done.34, bf16[144,1024]{1,0:T(8,128)(2,1)} %get-tuple-element.62.refs_0_, bf16[144,1024]{1,0:T(8,128)(2,1)} %copy-done.32, bf16[144,1024]{1,0:T(8,128)(2,1)} %collective-permute-done.35.refs_2_, bf16[144,1024]{1,0:T(8,128)(2,1)} %collective-permute-done.36.refs_3_), custom_call_target="tpu_custom_call" | custom-call | flops 452984832 | bytes 1966080 | tf_op jit(solution)/shard_map/combine/pallas_call | solution.py:190
  154.9 1.6 collective-permute-start.14
  156.5 3.9 %collective-permute-done.27.refs_2_ = bf16[144,1024]{1,0:T(8,128)(2,1)S(1)} collective-permute-done((bf16[144,1024]{1,0:T(8,128)(2,1)S(1)}, bf16[144,1024]{1,0:T(8,128)(2,1)S(1)}, u32[]{:S(2)}, u32[]{:S(2)}) %collective-permute-start.27) | collective-permute-done | bytes 294944 | tf_op jit(solution)/shard_map/ppermute | solution.py:93
  160.4 2.2 %collective-permute-start.15 = (bf16[144,1024]{1,0:T(8,128)(2,1)}, bf16[144,1024]{1,0:T(8,128)(2,1)S(1)}, u32[]{:S(2)}, u32[]{:S(2)}) collective-permute-start(bf16[144,1024]{1,0:T(8,128)(2,1)} %get-tuple-element.45), channel_id=1, source_target_pairs={{0,24},{8,16},{16,8},{24,0},{1,25},{9,17},{17,9},{25,1},{2,26},{10... | collective-permute-start | bytes 884744 | tf_op jit(solution)/shard_map/ppermute | solution.py:93
  162.8 0.6 copy-done.12
  163.5 3.2 %combine.5 = bf16[192,1024]{1,0:T(8,128)(2,1)} custom-call(f32[4,192]{1,0:T(4,128)} %copy-done.16, bf16[144,1024]{1,0:T(8,128)(2,1)} %get-tuple-element.54.refs_0_, bf16[144,1024]{1,0:T(8,128)(2,1)} %copy-done.10, bf16[144,1024]{1,0:T(8,128)(2,1)} %copy-done.11, bf16[144,1024]{1,0:T(8,128)(2,1)} %copy-done.12, bf16[192,1024]{1,0:T(8,128)(2,1)} %copy-done.6), custom_call_target="tpu_custom_call" | custom-call | flops 452984832 | bytes 1966080 | tf_op jit(solution)/shard_map/combine/pallas_call | solution.py:190
  166.7 3.7 %collective-permute-start.33 = (bf16[192,1024]{1,0:T(8,128)(2,1)}, bf16[192,1024]{1,0:T(8,128)(2,1)S(1)}, u32[]{:S(2)}, u32[]{:S(2)}) collective-permute-start(bf16[192,1024]{1,0:T(8,128)(2,1)} %combine.5), channel_id=1, source_target_pairs={{0,6},{1,7},{2,0},{3,1},{4,2},{5,3},{6,4},{7,5},{8,14},{9,15},{10,... | collective-permute-start | bytes 1179656 | tf_op jit(solution)/shard_map/ppermute | solution.py:72
  170.8 0.6 copy-done.15
  171.3 0.8 multiply_convert_fusion
  172.6 3.0 %collective-permute-done.37.refs_5_ = bf16[192,1024]{1,0:T(8,128)(2,1)S(1)} collective-permute-done((bf16[192,1024]{1,0:T(8,128)(2,1)}, bf16[192,1024]{1,0:T(8,128)(2,1)S(1)}, u32[]{:S(2)}, u32[]{:S(2)}) %collective-permute-start.37) | collective-permute-done | bytes 393248 | tf_op jit(solution)/shard_map/ppermute | solution.py:72
  175.5 5.3 %collective-permute-done.33.refs_4_ = bf16[192,1024]{1,0:T(8,128)(2,1)S(1)} collective-permute-done((bf16[192,1024]{1,0:T(8,128)(2,1)}, bf16[192,1024]{1,0:T(8,128)(2,1)S(1)}, u32[]{:S(2)}, u32[]{:S(2)}) %collective-permute-start.33) | collective-permute-done | bytes 393248 | tf_op jit(solution)/shard_map/ppermute | solution.py:72
  180.9 0.7 copy-done.4
  181.6 3.3 %combine.7 = bf16[192,1024]{1,0:T(8,128)(2,1)} custom-call(f32[4,192]{1,0:T(4,128)} %pad_maximum_fusion.table_ref, bf16[144,1024]{1,0:T(8,128)(2,1)} %get-tuple-element.42.refs_0_, bf16[144,1024]{1,0:T(8,128)(2,1)} %copy-done.7, bf16[144,1024]{1,0:T(8,128)(2,1)} %copy-done.8, bf16[144,1024]{1,0:T(8,128)(2,1)} %copy-done.9, bf16[192,1024]{1,0:T(8,128)(2,1)} %copy-done.4, ...), custom_call_target="tpu_custom_call" | custom-call | flops 452984832 | bytes 1966080 | tf_op jit(solution)/shard_map/combine/pallas_call | solution.py:190
  (114 shorter events, 2.8 us)
Async XLA Ops:
  0.6 169.8 %copy-start = (bf16[4,256,256]{2,1,0:T(8,128)(2,1)S(1)}, bf16[4,256,256]{2,1,0:T(8,128)(2,1)}, u32[]{:S(2)}) copy-start(bf16[4,256,256]{2,1,0:T(8,128)(2,1)} %param.13) | copy-start | bytes 1572868
  0.6 1.3 copy-start.1
  2.8 7.3 %copy-start.5 = (bf16[192,1024]{1,0:T(8,128)(2,1)}, bf16[192,1024]{1,0:T(8,128)(2,1)S(1)}, u32[]{:S(2)}) copy-start(bf16[192,1024]{1,0:T(8,128)(2,1)S(1)} %fusion.5.rows_ref) | copy-start | bytes 1179652
  2.8 43.1 %collective-permute-start.2 = (bf16[192,1024]{1,0:T(8,128)(2,1)S(1)}, bf16[192,1024]{1,0:T(8,128)(2,1)S(1)}, u32[]{:S(2)}, u32[]{:S(2)}) collective-permute-start(bf16[192,1024]{1,0:T(8,128)(2,1)S(1)} %fusion.5.rows_ref), channel_id=1, source_target_pairs={{0,6},{1,7},{2,0},{3,1},{4,2},{5,3},{6,4},{7,5},{8,14},{9,15},{10,... | collective-permute-start | bytes 1179656 | tf_op jit(solution)/shard_map/ppermute | solution.py:72
  7.9 17.7 %collective-permute-start.17 = (bf16[192,1024]{1,0:T(8,128)(2,1)S(1)}, bf16[192,1024]{1,0:T(8,128)(2,1)S(1)}, u32[]{:S(2)}, u32[]{:S(2)}) collective-permute-start(bf16[192,1024]{1,0:T(8,128)(2,1)S(1)} %fusion.5.rows_ref), channel_id=1, source_target_pairs={{0,2},{1,3},{2,4},{3,5},{4,6},{5,7},{6,0},{7,1},{8,10},{9,11},{10,... | collective-permute-start | bytes 1179656 | tf_op jit(solution)/shard_map/ppermute | solution.py:72
  7.9 64.9 %collective-permute-start.10 = (bf16[1024,512]{1,0:T(8,128)(2,1)}, bf16[1024,512]{1,0:T(8,128)(2,1)}, u32[]{:S(2)}, u32[]{:S(2)}) collective-permute-start(bf16[1024,512]{1,0:T(8,128)(2,1)} %bitcast.29), channel_id=1, source_target_pairs={{0,1},{1,0},{2,3},{3,2},{4,5},{5,4},{6,7},{7,6},{8,9},{9,8},{10,11... | collective-permute-start | bytes 3145736 | tf_op jit(solution)/shard_map/ppermute | solution.py:82
  10.1 17.2 %copy-start.13 = (f32[4,192]{1,0:T(4,128)S(1)}, f32[4,192]{1,0:T(4,128)}, u32[]{:S(2)}) copy-start(f32[4,192]{1,0:T(4,128)} %pad_maximum_fusion.table_ref) | copy-start | bytes 9220
  10.1 35.2 %copy-start.19 = (bf16[1,1024,512]{2,1,0:T(8,128)(2,1)S(1)}, bf16[1,1024,512]{2,1,0:T(8,128)(2,1)}, u32[]{:S(2)}) copy-start(bf16[1,1024,512]{2,1,0:T(8,128)(2,1)} %param.20) | copy-start | bytes 3145732
  12.4 32.9 %collective-permute-start.7 = (bf16[144,1024]{1,0:T(8,128)(2,1)}, bf16[144,1024]{1,0:T(8,128)(2,1)}, u32[]{:S(2)}, u32[]{:S(2)}) collective-permute-start(bf16[144,1024]{1,0:T(8,128)(2,1)} %get-tuple-element.39), channel_id=1, source_target_pairs={{0,8},{8,0},{16,24},{24,16},{1,9},{9,1},{17,25},{25,17},{2,10},{10... | collective-permute-start | bytes 884744 | tf_op jit(solution)/shard_map/ppermute | solution.py:93
  25.6 16.1 %copy-start.21 = (bf16[192,1024]{1,0:T(8,128)(2,1)}, bf16[192,1024]{1,0:T(8,128)(2,1)S(1)}, u32[]{:S(2)}) copy-start(bf16[192,1024]{1,0:T(8,128)(2,1)S(1)} %collective-permute-done.17.rows_ref) | copy-start | bytes 1179652
  25.6 30.9 %collective-permute-start.18 = (bf16[192,1024]{1,0:T(8,128)(2,1)S(1)}, bf16[192,1024]{1,0:T(8,128)(2,1)}, u32[]{:S(2)}, u32[]{:S(2)}) collective-permute-start(bf16[192,1024]{1,0:T(8,128)(2,1)S(1)} %collective-permute-done.17.rows_ref), channel_id=1, source_target_pairs={{0,2},{1,3},{2,4},{3,5},{4,6},{5,7},{6,0},{7,1},{8,10},{9,11},{10,... | collective-permute-start | bytes 1179656 | tf_op jit(solution)/shard_map/ppermute | solution.py:72
  27.2 7.7 %collective-permute-start.3 = (f32[4,192]{1,0:T(4,128)S(1)}, f32[4,192]{1,0:T(4,128)S(1)}, u32[]{:S(2)}, u32[]{:S(2)}) collective-permute-start(f32[4,192]{1,0:T(4,128)S(1)} %copy-done.13), channel_id=1, source_target_pairs={{0,6},{1,7},{2,0},{3,1},{4,2},{5,3},{6,4},{7,5},{8,14},{9,15},{10,... | collective-permute-start | bytes 9224 | tf_op jit(solution)/shard_map/ppermute | solution.py:72
  34.9 5.9 %collective-permute-start.16 = (f32[4,192]{1,0:T(4,128)S(1)}, f32[4,192]{1,0:T(4,128)S(1)}, u32[]{:S(2)}, u32[]{:S(2)}) collective-permute-start(f32[4,192]{1,0:T(4,128)S(1)} %copy-done.13), channel_id=1, source_target_pairs={{0,2},{1,3},{2,4},{3,5},{4,6},{5,7},{6,0},{7,1},{8,10},{9,11},{10,... | collective-permute-start | bytes 9224 | tf_op jit(solution)/shard_map/ppermute | solution.py:72
  35.5 11.8 %copy-start.2 = (bf16[192,1024]{1,0:T(8,128)(2,1)S(1)}, bf16[192,1024]{1,0:T(8,128)(2,1)}, u32[]{:S(2)}) copy-start(bf16[192,1024]{1,0:T(8,128)(2,1)} %param.11) | copy-start | bytes 1179652
  40.8 4.5 %collective-permute-start.19 = (f32[4,192]{1,0:T(4,128)S(1)}, f32[4,192]{1,0:T(4,128)S(1)}, u32[]{:S(2)}, u32[]{:S(2)}) collective-permute-start(f32[4,192]{1,0:T(4,128)S(1)} %copy-done.13), channel_id=1, source_target_pairs={{0,4},{1,5},{2,6},{3,7},{4,0},{5,1},{6,2},{7,3},{8,12},{9,13},{10,... | collective-permute-start | bytes 9224 | tf_op jit(solution)/shard_map/ppermute | solution.py:72
  45.3 2.2 %copy-start.35 = (f32[4,192]{1,0:T(4,128)}, f32[4,192]{1,0:T(4,128)S(1)}, u32[]{:S(2)}) copy-start(f32[4,192]{1,0:T(4,128)S(1)} %collective-permute-done.19.table_ref) | copy-start | bytes 9220
  45.3 30.4 %collective-permute-start.11 = (bf16[1024,512]{1,0:T(8,128)(2,1)S(1)}, bf16[1024,512]{1,0:T(8,128)(2,1)}, u32[]{:S(2)}, u32[]{:S(2)}) collective-permute-start(bf16[1024,512]{1,0:T(8,128)(2,1)S(1)} %bitcast.34), channel_id=1, source_target_pairs={{0,1},{1,0},{2,3},{3,2},{4,5},{5,4},{6,7},{7,6},{8,9},{9,8},{10,11... | collective-permute-start | bytes 3145736 | tf_op jit(solution)/shard_map/ppermute | solution.py:82
  45.3 32.0 %collective-permute-start.12 = (bf16[512,1024]{1,0:T(8,128)(2,1)}, bf16[512,1024]{1,0:T(8,128)(2,1)}, u32[]{:S(2)}, u32[]{:S(2)}) collective-permute-start(bf16[512,1024]{1,0:T(8,128)(2,1)} %bitcast.35), channel_id=1, source_target_pairs={{0,1},{1,0},{2,3},{3,2},{4,5},{5,4},{6,7},{7,6},{8,9},{9,8},{10,11... | collective-permute-start | bytes 3145736 | tf_op jit(solution)/shard_map/ppermute | solution.py:82
  45.8 12.3 %copy-start.20 = (bf16[192,1024]{1,0:T(8,128)(2,1)}, bf16[192,1024]{1,0:T(8,128)(2,1)S(1)}, u32[]{:S(2)}) copy-start(bf16[192,1024]{1,0:T(8,128)(2,1)S(1)} %collective-permute-done.2.rows_ref) | copy-start | bytes 1179652
  45.8 9.2 %collective-permute-start.23 = (bf16[144,1024]{1,0:T(8,128)(2,1)}, bf16[144,1024]{1,0:T(8,128)(2,1)S(1)}, u32[]{:S(2)}, u32[]{:S(2)}) collective-permute-start(bf16[144,1024]{1,0:T(8,128)(2,1)} %get-tuple-element.51), channel_id=1, source_target_pairs={{0,8},{8,0},{16,24},{24,16},{1,9},{9,1},{17,25},{25,17},{2,10},{10... | collective-permute-start | bytes 884744 | tf_op jit(solution)/shard_map/ppermute | solution.py:93
  47.5 10.5 %copy-start.14 = (f32[1024]{0:T(1024)S(1)}, f32[1024]{0:T(1024)}, u32[]{:S(2)}) copy-start(f32[1024]{0:T(1024)} %param.12) | copy-start | bytes 12292
  55.0 3.1 %copy-start.25 = (bf16[144,1024]{1,0:T(8,128)(2,1)}, bf16[144,1024]{1,0:T(8,128)(2,1)S(1)}, u32[]{:S(2)}) copy-start(bf16[144,1024]{1,0:T(8,128)(2,1)S(1)} %collective-permute-done.23.refs_5_) | copy-start | bytes 884740
  55.0 14.8 %collective-permute-start.24 = (bf16[144,1024]{1,0:T(8,128)(2,1)}, bf16[144,1024]{1,0:T(8,128)(2,1)}, u32[]{:S(2)}, u32[]{:S(2)}) collective-permute-start(bf16[144,1024]{1,0:T(8,128)(2,1)} %get-tuple-element.52), channel_id=1, source_target_pairs={{0,16},{8,24},{16,0},{24,8},{1,17},{9,25},{17,1},{25,9},{2,18},{10... | collective-permute-start | bytes 884744 | tf_op jit(solution)/shard_map/ppermute | solution.py:93
  56.6 14.7 %collective-permute-start.25 = (bf16[144,1024]{1,0:T(8,128)(2,1)}, bf16[144,1024]{1,0:T(8,128)(2,1)S(1)}, u32[]{:S(2)}, u32[]{:S(2)}) collective-permute-start(bf16[144,1024]{1,0:T(8,128)(2,1)} %get-tuple-element.53), channel_id=1, source_target_pairs={{0,24},{8,16},{16,8},{24,0},{1,25},{9,17},{17,9},{25,1},{2,26},{10... | collective-permute-start | bytes 884744 | tf_op jit(solution)/shard_map/ppermute | solution.py:93
  69.8 10.1 %collective-permute-start.20 = (bf16[144,1024]{1,0:T(8,128)(2,1)}, bf16[144,1024]{1,0:T(8,128)(2,1)S(1)}, u32[]{:S(2)}, u32[]{:S(2)}) collective-permute-start(bf16[144,1024]{1,0:T(8,128)(2,1)} %get-tuple-element.47), channel_id=1, source_target_pairs={{0,8},{8,0},{16,24},{24,16},{1,9},{9,1},{17,25},{25,17},{2,10},{10... | collective-permute-start | bytes 884744 | tf_op jit(solution)/shard_map/ppermute | solution.py:93
  71.3 4.4 %copy-start.28 = (bf16[144,1024]{1,0:T(8,128)(2,1)}, bf16[144,1024]{1,0:T(8,128)(2,1)S(1)}, u32[]{:S(2)}) copy-start(bf16[144,1024]{1,0:T(8,128)(2,1)S(1)} %collective-permute-done.25.refs_7_) | copy-start | bytes 884740
  71.3 22.8 %collective-permute-start.21 = (bf16[144,1024]{1,0:T(8,128)(2,1)}, bf16[144,1024]{1,0:T(8,128)(2,1)}, u32[]{:S(2)}, u32[]{:S(2)}) collective-permute-start(bf16[144,1024]{1,0:T(8,128)(2,1)} %get-tuple-element.48), channel_id=1, source_target_pairs={{0,16},{8,24},{16,0},{24,8},{1,17},{9,25},{17,1},{25,9},{2,18},{10... | collective-permute-start | bytes 884744 | tf_op jit(solution)/shard_map/ppermute | solution.py:93
  72.8 22.8 %collective-permute-start.22 = (bf16[144,1024]{1,0:T(8,128)(2,1)}, bf16[144,1024]{1,0:T(8,128)(2,1)}, u32[]{:S(2)}, u32[]{:S(2)}) collective-permute-start(bf16[144,1024]{1,0:T(8,128)(2,1)} %get-tuple-element.49), channel_id=1, source_target_pairs={{0,24},{8,16},{16,8},{24,0},{1,25},{9,17},{17,9},{25,1},{2,26},{10... | collective-permute-start | bytes 884744 | tf_op jit(solution)/shard_map/ppermute | solution.py:93
  73.3 2.4 %copy-start.23 = (bf16[144,1024]{1,0:T(8,128)(2,1)S(1)}, bf16[144,1024]{1,0:T(8,128)(2,1)}, u32[]{:S(2)}) copy-start(bf16[144,1024]{1,0:T(8,128)(2,1)} %get-tuple-element.40) | copy-start | bytes 884740
  73.3 4.0 %copy-start.22 = (bf16[144,1024]{1,0:T(8,128)(2,1)S(1)}, bf16[144,1024]{1,0:T(8,128)(2,1)}, u32[]{:S(2)}) copy-start(bf16[144,1024]{1,0:T(8,128)(2,1)} %get-tuple-element.41) | copy-start | bytes 884740
  75.7 33.1 %collective-permute-start.8 = (bf16[144,1024]{1,0:T(8,128)(2,1)S(1)}, bf16[144,1024]{1,0:T(8,128)(2,1)S(1)}, u32[]{:S(2)}, u32[]{:S(2)}) collective-permute-start(bf16[144,1024]{1,0:T(8,128)(2,1)S(1)} %copy-done.23), channel_id=1, source_target_pairs={{0,16},{8,24},{16,0},{24,8},{1,17},{9,25},{17,1},{25,9},{2,18},{10... | collective-permute-start | bytes 884744 | tf_op jit(solution)/shard_map/ppermute | solution.py:93
  77.3 32.9 %collective-permute-start.9 = (bf16[144,1024]{1,0:T(8,128)(2,1)S(1)}, bf16[144,1024]{1,0:T(8,128)(2,1)S(1)}, u32[]{:S(2)}, u32[]{:S(2)}) collective-permute-start(bf16[144,1024]{1,0:T(8,128)(2,1)S(1)} %copy-done.22), channel_id=1, source_target_pairs={{0,24},{8,16},{16,8},{24,0},{1,25},{9,17},{17,9},{25,1},{2,26},{10... | collective-permute-start | bytes 884744 | tf_op jit(solution)/shard_map/ppermute | solution.py:93
  79.9 15.7 %copy-start.31 = (bf16[144,1024]{1,0:T(8,128)(2,1)}, bf16[144,1024]{1,0:T(8,128)(2,1)S(1)}, u32[]{:S(2)}) copy-start(bf16[144,1024]{1,0:T(8,128)(2,1)S(1)} %collective-permute-done.20.refs_1_) | copy-start | bytes 884740
  79.9 31.8 %collective-permute-start.4 = (bf16[144,1024]{1,0:T(8,128)(2,1)}, bf16[144,1024]{1,0:T(8,128)(2,1)S(1)}, u32[]{:S(2)}, u32[]{:S(2)}) collective-permute-start(bf16[144,1024]{1,0:T(8,128)(2,1)} %get-tuple-element.35), channel_id=1, source_target_pairs={{0,8},{8,0},{16,24},{24,16},{1,9},{9,1},{17,25},{25,17},{2,10},{10... | collective-permute-start | bytes 884744 | tf_op jit(solution)/shard_map/ppermute | solution.py:93
  94.1 25.3 %collective-permute-start.5 = (bf16[144,1024]{1,0:T(8,128)(2,1)}, bf16[144,1024]{1,0:T(8,128)(2,1)S(1)}, u32[]{:S(2)}, u32[]{:S(2)}) collective-permute-start(bf16[144,1024]{1,0:T(8,128)(2,1)} %get-tuple-element.36), channel_id=1, source_target_pairs={{0,16},{8,24},{16,0},{24,8},{1,17},{9,25},{17,1},{25,9},{2,18},{10... | collective-permute-start | bytes 884744 | tf_op jit(solution)/shard_map/ppermute | solution.py:93
  95.6 25.3 %collective-permute-start.6 = (bf16[144,1024]{1,0:T(8,128)(2,1)}, bf16[144,1024]{1,0:T(8,128)(2,1)}, u32[]{:S(2)}, u32[]{:S(2)}) collective-permute-start(bf16[144,1024]{1,0:T(8,128)(2,1)} %get-tuple-element.37), channel_id=1, source_target_pairs={{0,24},{8,16},{16,8},{24,0},{1,25},{9,17},{17,9},{25,1},{2,26},{10... | collective-permute-start | bytes 884744 | tf_op jit(solution)/shard_map/ppermute | solution.py:93
  108.9 13.0 %copy-start.26 = (bf16[144,1024]{1,0:T(8,128)(2,1)}, bf16[144,1024]{1,0:T(8,128)(2,1)S(1)}, u32[]{:S(2)}) copy-start(bf16[144,1024]{1,0:T(8,128)(2,1)S(1)} %collective-permute-done.8.refs_6_) | copy-start | bytes 884740
  108.9 26.4 %collective-permute-start = (bf16[8,1024]{1,0:T(8,128)(2,1)S(1)}, bf16[8,1024]{1,0:T(8,128)(2,1)S(1)}, u32[]{:S(2)}, u32[]{:S(2)}) collective-permute-start(bf16[8,1024]{1,0:T(8,128)(2,1)S(1)} %get-tuple-element.71), channel_id=1, source_target_pairs={{0,1},{1,2},{2,3},{3,4},{4,5},{5,6},{6,7},{7,8},{8,9},{9,10},{10,1... | collective-permute-start | bytes 49160 | tf_op jit(solution)/shard_map/ppermute | solution.py:18
  110.2 11.7 %copy-start.27 = (bf16[144,1024]{1,0:T(8,128)(2,1)}, bf16[144,1024]{1,0:T(8,128)(2,1)S(1)}, u32[]{:S(2)}) copy-start(bf16[144,1024]{1,0:T(8,128)(2,1)S(1)} %collective-permute-done.9.refs_7_) | copy-start | bytes 884740
  110.2 26.2 %collective-permute-start.1 = (bf16[8,1024]{1,0:T(8,128)(2,1)S(1)}, bf16[8,1024]{1,0:T(8,128)(2,1)S(1)}, u32[]{:S(2)}, u32[]{:S(2)}) collective-permute-start(bf16[8,1024]{1,0:T(8,128)(2,1)S(1)} %get-tuple-element.72), channel_id=1, source_target_pairs={{1,0},{2,1},{3,2},{4,3},{5,4},{6,5},{7,6},{8,7},{9,8},{10,9},{11,1... | collective-permute-start | bytes 49160 | tf_op jit(solution)/shard_map/ppermute | solution.py:19
  111.7 10.2 %copy-start.29 = (bf16[144,1024]{1,0:T(8,128)(2,1)}, bf16[144,1024]{1,0:T(8,128)(2,1)S(1)}, u32[]{:S(2)}) copy-start(bf16[144,1024]{1,0:T(8,128)(2,1)S(1)} %collective-permute-done.4.refs_1_) | copy-start | bytes 884740
  111.7 26.3 %collective-permute-start.29 = (bf16[144,1024]{1,0:T(8,128)(2,1)}, bf16[144,1024]{1,0:T(8,128)(2,1)S(1)}, u32[]{:S(2)}, u32[]{:S(2)}) collective-permute-start(bf16[144,1024]{1,0:T(8,128)(2,1)} %get-tuple-element.59), channel_id=1, source_target_pairs={{0,8},{8,0},{16,24},{24,16},{1,9},{9,1},{17,25},{25,17},{2,10},{10... | collective-permute-start | bytes 884744 | tf_op jit(solution)/shard_map/ppermute | solution.py:93
  119.4 2.5 %copy-start.30 = (bf16[144,1024]{1,0:T(8,128)(2,1)}, bf16[144,1024]{1,0:T(8,128)(2,1)S(1)}, u32[]{:S(2)}) copy-start(bf16[144,1024]{1,0:T(8,128)(2,1)S(1)} %collective-permute-done.5.refs_2_) | copy-start | bytes 884740
  119.4 19.6 %collective-permute-start.30 = (bf16[144,1024]{1,0:T(8,128)(2,1)}, bf16[144,1024]{1,0:T(8,128)(2,1)}, u32[]{:S(2)}, u32[]{:S(2)}) collective-permute-start(bf16[144,1024]{1,0:T(8,128)(2,1)} %get-tuple-element.60), channel_id=1, source_target_pairs={{0,16},{8,24},{16,0},{24,8},{1,17},{9,25},{17,1},{25,9},{2,18},{10... | collective-permute-start | bytes 884744 | tf_op jit(solution)/shard_map/ppermute | solution.py:93
  120.9 18.1 %collective-permute-start.31 = (bf16[144,1024]{1,0:T(8,128)(2,1)}, bf16[144,1024]{1,0:T(8,128)(2,1)}, u32[]{:S(2)}, u32[]{:S(2)}) collective-permute-start(bf16[144,1024]{1,0:T(8,128)(2,1)} %get-tuple-element.61), channel_id=1, source_target_pairs={{0,24},{8,16},{16,8},{24,0},{1,25},{9,17},{17,9},{25,1},{2,26},{10... | collective-permute-start | bytes 884744 | tf_op jit(solution)/shard_map/ppermute | solution.py:93
  135.3 8.2 %collective-permute-start.34 = (bf16[144,1024]{1,0:T(8,128)(2,1)}, bf16[144,1024]{1,0:T(8,128)(2,1)S(1)}, u32[]{:S(2)}, u32[]{:S(2)}) collective-permute-start(bf16[144,1024]{1,0:T(8,128)(2,1)} %get-tuple-element.63), channel_id=1, source_target_pairs={{0,8},{8,0},{16,24},{24,16},{1,9},{9,1},{17,25},{25,17},{2,10},{10... | collective-permute-start | bytes 884744 | tf_op jit(solution)/shard_map/ppermute | solution.py:93
  136.4 10.0 %collective-permute-start.35 = (bf16[144,1024]{1,0:T(8,128)(2,1)}, bf16[144,1024]{1,0:T(8,128)(2,1)}, u32[]{:S(2)}, u32[]{:S(2)}) collective-permute-start(bf16[144,1024]{1,0:T(8,128)(2,1)} %get-tuple-element.64), channel_id=1, source_target_pairs={{0,16},{8,24},{16,0},{24,8},{1,17},{9,25},{17,1},{25,9},{2,18},{10... | collective-permute-start | bytes 884744 | tf_op jit(solution)/shard_map/ppermute | solution.py:93
  138.0 11.7 %collective-permute-start.36 = (bf16[144,1024]{1,0:T(8,128)(2,1)}, bf16[144,1024]{1,0:T(8,128)(2,1)}, u32[]{:S(2)}, u32[]{:S(2)}) collective-permute-start(bf16[144,1024]{1,0:T(8,128)(2,1)} %get-tuple-element.65), channel_id=1, source_target_pairs={{0,24},{8,16},{16,8},{24,0},{1,25},{9,17},{17,9},{25,1},{2,26},{10... | collective-permute-start | bytes 884744 | tf_op jit(solution)/shard_map/ppermute | solution.py:93
  142.1 20.7 %collective-permute-start.32 = (bf16[192,1024]{1,0:T(8,128)(2,1)}, bf16[192,1024]{1,0:T(8,128)(2,1)S(1)}, u32[]{:S(2)}, u32[]{:S(2)}) collective-permute-start(bf16[192,1024]{1,0:T(8,128)(2,1)} %combine.4), channel_id=1, source_target_pairs={{0,6},{1,7},{2,0},{3,1},{4,2},{5,3},{6,4},{7,5},{8,14},{9,15},{10,... | collective-permute-start | bytes 1179656 | tf_op jit(solution)/shard_map/ppermute | solution.py:72
  142.1 2.1 %copy-start.24 = (bf16[144,1024]{1,0:T(8,128)(2,1)S(1)}, bf16[144,1024]{1,0:T(8,128)(2,1)}, u32[]{:S(2)}) copy-start(bf16[144,1024]{1,0:T(8,128)(2,1)} %get-tuple-element.56) | copy-start | bytes 884740
  142.3 12.6 %collective-permute-start.26 = (bf16[144,1024]{1,0:T(8,128)(2,1)}, bf16[144,1024]{1,0:T(8,128)(2,1)S(1)}, u32[]{:S(2)}, u32[]{:S(2)}) collective-permute-start(bf16[144,1024]{1,0:T(8,128)(2,1)} %get-tuple-element.55), channel_id=1, source_target_pairs={{0,8},{8,0},{16,24},{24,16},{1,9},{9,1},{17,25},{25,17},{2,10},{10... | collective-permute-start | bytes 884744 | tf_op jit(solution)/shard_map/ppermute | solution.py:93
  144.2 16.2 %collective-permute-start.27 = (bf16[144,1024]{1,0:T(8,128)(2,1)S(1)}, bf16[144,1024]{1,0:T(8,128)(2,1)S(1)}, u32[]{:S(2)}, u32[]{:S(2)}) collective-permute-start(bf16[144,1024]{1,0:T(8,128)(2,1)S(1)} %copy-done.24), channel_id=1, source_target_pairs={{0,16},{8,24},{16,0},{24,8},{1,17},{9,25},{17,1},{25,9},{2,18},{10... | collective-permute-start | bytes 884744 | tf_op jit(solution)/shard_map/ppermute | solution.py:93
  146.3 16.3 %collective-permute-start.28 = (bf16[144,1024]{1,0:T(8,128)(2,1)}, bf16[144,1024]{1,0:T(8,128)(2,1)S(1)}, u32[]{:S(2)}, u32[]{:S(2)}) collective-permute-start(bf16[144,1024]{1,0:T(8,128)(2,1)} %get-tuple-element.57), channel_id=1, source_target_pairs={{0,24},{8,16},{16,8},{24,0},{1,25},{9,17},{17,9},{25,1},{2,26},{10... | collective-permute-start | bytes 884744 | tf_op jit(solution)/shard_map/ppermute | solution.py:93
  149.7 22.4 %collective-permute-start.13 = (bf16[144,1024]{1,0:T(8,128)(2,1)}, bf16[144,1024]{1,0:T(8,128)(2,1)S(1)}, u32[]{:S(2)}, u32[]{:S(2)}) collective-permute-start(bf16[144,1024]{1,0:T(8,128)(2,1)} %get-tuple-element.43), channel_id=1, source_target_pairs={{0,8},{8,0},{16,24},{24,16},{1,9},{9,1},{17,25},{25,17},{2,10},{10... | collective-permute-start | bytes 884744 | tf_op jit(solution)/shard_map/ppermute | solution.py:93
  154.9 7.9 %copy-start.10 = (bf16[144,1024]{1,0:T(8,128)(2,1)}, bf16[144,1024]{1,0:T(8,128)(2,1)S(1)}, u32[]{:S(2)}) copy-start(bf16[144,1024]{1,0:T(8,128)(2,1)S(1)} %collective-permute-done.26.refs_1_) | copy-start | bytes 884740
  154.9 17.7 %collective-permute-start.14 = (bf16[144,1024]{1,0:T(8,128)(2,1)}, bf16[144,1024]{1,0:T(8,128)(2,1)S(1)}, u32[]{:S(2)}, u32[]{:S(2)}) collective-permute-start(bf16[144,1024]{1,0:T(8,128)(2,1)} %get-tuple-element.44), channel_id=1, source_target_pairs={{0,16},{8,24},{16,0},{24,8},{1,17},{9,25},{17,1},{25,9},{2,18},{10... | collective-permute-start | bytes 884744 | tf_op jit(solution)/shard_map/ppermute | solution.py:93
  160.4 2.4 %copy-start.11 = (bf16[144,1024]{1,0:T(8,128)(2,1)}, bf16[144,1024]{1,0:T(8,128)(2,1)S(1)}, u32[]{:S(2)}) copy-start(bf16[144,1024]{1,0:T(8,128)(2,1)S(1)} %collective-permute-done.27.refs_2_) | copy-start | bytes 884740
  160.4 12.1 %collective-permute-start.15 = (bf16[144,1024]{1,0:T(8,128)(2,1)}, bf16[144,1024]{1,0:T(8,128)(2,1)S(1)}, u32[]{:S(2)}, u32[]{:S(2)}) collective-permute-start(bf16[144,1024]{1,0:T(8,128)(2,1)} %get-tuple-element.45), channel_id=1, source_target_pairs={{0,24},{8,16},{16,8},{24,0},{1,25},{9,17},{17,9},{25,1},{2,26},{10... | collective-permute-start | bytes 884744 | tf_op jit(solution)/shard_map/ppermute | solution.py:93
  162.7 12.9 %collective-permute-start.37 = (bf16[192,1024]{1,0:T(8,128)(2,1)}, bf16[192,1024]{1,0:T(8,128)(2,1)S(1)}, u32[]{:S(2)}, u32[]{:S(2)}) collective-permute-start(bf16[192,1024]{1,0:T(8,128)(2,1)} %combine.6), channel_id=1, source_target_pairs={{0,2},{1,3},{2,4},{3,5},{4,6},{5,7},{6,0},{7,1},{8,10},{9,11},{10,... | collective-permute-start | bytes 1179656 | tf_op jit(solution)/shard_map/ppermute | solution.py:72
  166.7 14.2 %collective-permute-start.33 = (bf16[192,1024]{1,0:T(8,128)(2,1)}, bf16[192,1024]{1,0:T(8,128)(2,1)S(1)}, u32[]{:S(2)}, u32[]{:S(2)}) collective-permute-start(bf16[192,1024]{1,0:T(8,128)(2,1)} %combine.5), channel_id=1, source_target_pairs={{0,6},{1,7},{2,0},{3,1},{4,2},{5,3},{6,4},{7,5},{8,14},{9,15},{10,... | collective-permute-start | bytes 1179656 | tf_op jit(solution)/shard_map/ppermute | solution.py:72
  172.2 8.7 %copy-start.7 = (bf16[144,1024]{1,0:T(8,128)(2,1)}, bf16[144,1024]{1,0:T(8,128)(2,1)S(1)}, u32[]{:S(2)}) copy-start(bf16[144,1024]{1,0:T(8,128)(2,1)S(1)} %collective-permute-done.13.refs_1_) | copy-start | bytes 884740
  172.5 8.3 %copy-start.8 = (bf16[144,1024]{1,0:T(8,128)(2,1)}, bf16[144,1024]{1,0:T(8,128)(2,1)S(1)}, u32[]{:S(2)}) copy-start(bf16[144,1024]{1,0:T(8,128)(2,1)S(1)} %collective-permute-done.14.refs_2_) | copy-start | bytes 884740
  172.6 8.3 %copy-start.9 = (bf16[144,1024]{1,0:T(8,128)(2,1)}, bf16[144,1024]{1,0:T(8,128)(2,1)S(1)}, u32[]{:S(2)}) copy-start(bf16[144,1024]{1,0:T(8,128)(2,1)S(1)} %collective-permute-done.15.refs_3_) | copy-start | bytes 884740
  175.5 5.4 %copy-start.3 = (bf16[192,1024]{1,0:T(8,128)(2,1)}, bf16[192,1024]{1,0:T(8,128)(2,1)S(1)}, u32[]{:S(2)}) copy-start(bf16[192,1024]{1,0:T(8,128)(2,1)S(1)} %collective-permute-done.37.refs_5_) | copy-start | bytes 1179652
  (10 other events, 7.6 us)

commit v4 on v3

--- a/solution.py
+++ b/solution.py
@@ -77,6 +77,11 @@
     return relayed + [n for n in range(1, chips) if n not in relayed] + [0]
 
 
+def serving_groups(order):
+    pairs = [order[n : n + 2] for n in range(2, len(order), 2)]
+    return [[order[1]], [order[0]]] + pairs
+
+
 def core_swap(value):
     size = lax.axis_size("tp")
     return lax.ppermute(value, "tp", [(i, i ^ 1) for i in range(size)])
@@ -160,7 +165,7 @@
     )(rows, table)
 
 
-def combine(pieces, table, others=()):
+def combine(pieces, table, others, kind):
     top_count = table.shape[0] // 2
     capacity, width = pieces[0].shape
     row_count = table.shape[1]
@@ -184,12 +189,12 @@
                     (((0,), (0,)), ((), ())),
                     preferred_element_type=jnp.float32,
                 )
-        out_ref[...] = total.astype(jnp.bfloat16)
+        out_ref[...] = total.astype(kind)
 
     work = len(pieces) * capacity * row_count * width
     return pl.pallas_call(
         kernel,
-        out_shape=jax.ShapeDtypeStruct((row_count, width), jnp.bfloat16),
+        out_shape=jax.ShapeDtypeStruct((row_count, width), kind),
         cost_estimate=pl.CostEstimate(
             flops=4 * work, transcendentals=0, bytes_accessed=2 * (len(pieces) * capacity + 2 * row_count) * width
         ),
@@ -300,20 +305,22 @@
         arrived[n] = exchange(dispatch(blocks[n], tables[n], experts, capacity))
 
     back = {}
-    for first in range(0, chips, 2):
-        group = order[first : first + 2]
+    for group in serving_groups(order):
         served = ffn([piece for n in group for piece in arrived[n]], shards)
         for place, n in enumerate(group):
             back[n] = exchange(served[place * experts : (place + 1) * experts])
 
     home, relayed = [], {}
     for n in order[:-1]:
-        term = combine(back[n], tables[n], relayed.get(n, ()))
+        term = combine(back[n], tables[n], relayed.get(n, ()), jnp.bfloat16)
         if n % 2:
             home.append(shift(term, -n))
         else:
             relayed[n - 1] = (shift(term, -1),)
-    expert_out = combine(back[0], tables[0], home)
+    total = combine(back[0], tables[0], (), jnp.float32)
+    for term in home:
+        total = total + term.astype(jnp.float32)
+    expert_out = total.astype(jnp.bfloat16)
 
     mixer_out = mixer(mixer_input, mixer_gain, group_weight, mixer_scale)
     return (mixer_out, expert_out)

time: 185 us -> 173 us (0.935)
  waiting for transfers between devices: 69.1 us -> 46.7 us
  starting transfers between devices: 56.6 us -> 60.2 us
  Pallas kernels: 48.4 us -> 51.3 us
  other arithmetic: 4.43 us -> 6.58 us
    ppermute x24, waiting for transfers between devices: 37 us -> 24.4 us  [exchange(): lax.ppermute(pieces[m], 'ep', [(i, i ^ m) for i in range(count)])]
    ppermute x9, waiting for transfers between devices: 32.1 us -> 22.3 us  [shift(): lax.ppermute(value, 'tp', [(i, (i + steps * CORES) % size) for i in range...]
    ppermute x9, starting transfers between devices: 13.7 us -> 17 us  [shift(): lax.ppermute(value, 'tp', [(i, (i + steps * CORES) % size) for i in range...]
    pallas_call x2 -> x3, Pallas kernels: 26.6 us -> 29.7 us  [ffn(): pl.pallas_call(kernel, grid=(steps,), in_specs=[whole] * count + [across,...]
    convert_element_type x0 -> x1, other arithmetic: none -> 2.05 us  [on_device(): expert_out = total.astype(jnp.bfloat16)]
    unnamed x72 -> x76, local copies, waits for them, and re-layouts: 4.86 us -> 5.09 us
  transfers between devices with their start and end apart: 38 -> 38, of which waited for: 14 -> 13; matrix products, arithmetic and copies ran while one was open for 2% -> 2% of each run, Pallas kernels for 24% -> 30%
where the time goes in v4:
time: 173 us; the launch traced here: 172 us
  starting transfers between devices  60.2 us (35%)
  Pallas kernels  51.3 us (30%)
  waiting for transfers between devices  46.7 us (27%)
  other arithmetic  6.58 us (4%)
  local copies, waits for them, and re-layouts  5.18 us (3%)
    ppermute x24, starting transfers between devices, exchange(): lax.ppermute(pieces[m], 'ep', [(i, i ^ m) for i in range(count)])  39.9 us
    pallas_call x3, Pallas kernels, ffn(): pl.pallas_call(kernel, grid=(steps,), in_specs=[whole] * count + [across,...  29.7 us
    ppermute x24, waiting for transfers between devices, exchange(): lax.ppermute(pieces[m], 'ep', [(i, i ^ m) for i in range(count)])  24.4 us
    ppermute x9, waiting for transfers between devices, shift(): lax.ppermute(value, 'tp', [(i, (i + steps * CORES) % size) for i in range...  22.3 us
    ppermute x9, starting transfers between devices, shift(): lax.ppermute(value, 'tp', [(i, (i + steps * CORES) % size) for i in range...  17 us
    pallas_call x4, Pallas kernels, combine(): pl.pallas_call(kernel, out_shape=jax.ShapeDtypeStruct((row_count, width),...  12.4 us
    pallas_call x4, Pallas kernels, dispatch(): pl.pallas_call(kernel, out_shape=[shape] * experts, cost_estimate=pl.Cost...  9.19 us
    unnamed x76, local copies, waits for them, and re-layouts  5.09 us
  transfers between devices with their start and end apart: 38, of which 13 were waited for; matrix products, arithmetic and copies ran while one was open for 2% of the time, Pallas kernels for 30%

profile of v4, /device:TPU:0, one launch (start us, length us, event | category | flops | bytes accessed | tf_op | source)
XLA Modules:
  0.0 172.3 jit_solution(8148654401497813981)
XLA Ops:
  0.7 1.2 fusion.3
  1.9 0.9 fusion.5.rows_ref
  2.8 3.1 %collective-permute-start.17 = (bf16[192,1024]{1,0:T(8,128)(2,1)S(1)}, bf16[192,1024]{1,0:T(8,128)(2,1)S(1)}, u32[]{:S(2)}, u32[]{:S(2)}) collective-permute-start(bf16[192,1024]{1,0:T(8,128)(2,1)S(1)} %fusion.5.rows_ref), channel_id=1, source_target_pairs={{0,2},{1,3},{2,4},{3,5},{4,6},{5,7},{6,0},{7,1},{8,10},{9,11},{10,... | collective-permute-start | bytes 1179656 | tf_op jit(solution)/shard_map/ppermute | solution.py:72
  5.9 0.7 copy-done.16
  6.8 0.7 copy-done.17
  7.5 2.7 %collective-permute-start.24 = (f32[4,192]{1,0:T(4,128)S(1)}, f32[4,192]{1,0:T(4,128)S(1)}, u32[]{:S(2)}, u32[]{:S(2)}) collective-permute-start(f32[4,192]{1,0:T(4,128)S(1)} %pad_maximum_fusion.table_ref), channel_id=1, source_target_pairs={{0,4},{1,5},{2,6},{3,7},{4,0},{5,1},{6,2},{7,3},{8,12},{9,13},{10,... | collective-permute-start | bytes 9224 | tf_op jit(solution)/shard_map/ppermute | solution.py:72
  10.4 0.3 collective-permute-start.12
  10.8 3.6 %collective-permute-done.24.table_ref = f32[4,192]{1,0:T(4,128)S(1)} collective-permute-done((f32[4,192]{1,0:T(4,128)S(1)}, f32[4,192]{1,0:T(4,128)S(1)}, u32[]{:S(2)}, u32[]{:S(2)}) %collective-permute-start.24) | collective-permute-done | bytes 3104 | tf_op jit(solution)/shard_map/ppermute | solution.py:72
  14.4 4.5 %collective-permute-start.2 = (bf16[192,1024]{1,0:T(8,128)(2,1)S(1)}, bf16[192,1024]{1,0:T(8,128)(2,1)S(1)}, u32[]{:S(2)}, u32[]{:S(2)}) collective-permute-start(bf16[192,1024]{1,0:T(8,128)(2,1)S(1)} %fusion.5.rows_ref), channel_id=1, source_target_pairs={{0,6},{1,7},{2,0},{3,1},{4,2},{5,3},{6,4},{7,5},{8,14},{9,15},{10,... | collective-permute-start | bytes 1179656 | tf_op jit(solution)/shard_map/ppermute | solution.py:72
  19.0 0.7 copy-done.13
  19.8 15.6 %collective-permute-done.25.rows_ref = bf16[192,1024]{1,0:T(8,128)(2,1)S(1)} collective-permute-done((bf16[192,1024]{1,0:T(8,128)(2,1)S(1)}, bf16[192,1024]{1,0:T(8,128)(2,1)S(1)}, u32[]{:S(2)}, u32[]{:S(2)}) %collective-permute-start.25) | collective-permute-done | bytes 393248 | tf_op jit(solution)/shard_map/ppermute | solution.py:72
  35.5 1.8 %collective-permute-start.3 = (f32[4,192]{1,0:T(4,128)S(1)}, f32[4,192]{1,0:T(4,128)S(1)}, u32[]{:S(2)}, u32[]{:S(2)}) collective-permute-start(f32[4,192]{1,0:T(4,128)S(1)} %pad_maximum_fusion.table_ref), channel_id=1, source_target_pairs={{0,6},{1,7},{2,0},{3,1},{4,2},{5,3},{6,4},{7,5},{8,14},{9,15},{10,... | collective-permute-start | bytes 9224 | tf_op jit(solution)/shard_map/ppermute | solution.py:72
  37.3 2.3 %dispatch.7 = (bf16[144,1024]{1,0:T(8,128)(2,1)}, bf16[144,1024]{1,0:T(8,128)(2,1)}, bf16[144,1024]{1,0:T(8,128)(2,1)}, bf16[144,1024]{1,0:T(8,128)(2,1)}) custom-call(bf16[192,1024]{1,0:T(8,128)(2,1)} %copy-done.20, f32[4,192]{1,0:T(4,128)} %copy-done.37), custom_call_target="tpu_custom_call" | custom-call | flops 226492416 | bytes 1572864 | tf_op jit(solution)/shard_map/dispatch/pallas_call | solution.py:158
  39.6 1.5 collective-permute-start.26
  41.1 1.5 collective-permute-start.27
  42.6 0.5 collective-permute-start.28
  43.1 2.3 %dispatch.5 = (bf16[144,1024]{1,0:T(8,128)(2,1)}, bf16[144,1024]{1,0:T(8,128)(2,1)}, bf16[144,1024]{1,0:T(8,128)(2,1)}, bf16[144,1024]{1,0:T(8,128)(2,1)}) custom-call(bf16[192,1024]{1,0:T(8,128)(2,1)} %copy-done.3, f32[4,192]{1,0:T(4,128)} %copy-done.11), custom_call_target="tpu_custom_call" | custom-call | flops 226492416 | bytes 1572864 | tf_op jit(solution)/shard_map/dispatch/pallas_call | solution.py:158
  45.4 2.3 %dispatch.4 = (bf16[144,1024]{1,0:T(8,128)(2,1)}, bf16[144,1024]{1,0:T(8,128)(2,1)}, bf16[144,1024]{1,0:T(8,128)(2,1)}, bf16[144,1024]{1,0:T(8,128)(2,1)}) custom-call(bf16[192,1024]{1,0:T(8,128)(2,1)} %copy-done.19, f32[4,192]{1,0:T(4,128)} %copy-done.36), custom_call_target="tpu_custom_call" | custom-call | flops 226492416 | bytes 1572864 | tf_op jit(solution)/shard_map/dispatch/pallas_call | solution.py:158
  47.7 1.1 collective-permute-start.16
  48.8 1.5 collective-permute-start.7
  50.3 1.6 collective-permute-start.8
  51.9 2.9 %collective-permute-done.27.refs_2_ = bf16[144,1024]{1,0:T(8,128)(2,1)} collective-permute-done((bf16[144,1024]{1,0:T(8,128)(2,1)}, bf16[144,1024]{1,0:T(8,128)(2,1)}, u32[]{:S(2)}, u32[]{:S(2)}) %collective-permute-start.27) | collective-permute-done | bytes 294944 | tf_op jit(solution)/shard_map/ppermute | solution.py:98
  54.7 1.3 collective-permute-start
  56.0 1.1 collective-permute-done.28.refs_3_
  57.1 1.5 collective-permute-start.1
  58.6 8.3 %ffn.5 = (bf16[144,1024]{1,0:T(8,128)(2,1)}, bf16[144,1024]{1,0:T(8,128)(2,1)}, bf16[144,1024]{1,0:T(8,128)(2,1)}, bf16[144,1024]{1,0:T(8,128)(2,1)}) custom-call(bf16[144,1024]{1,0:T(8,128)(2,1)} %get-tuple-element.54.refs_0_, bf16[144,1024]{1,0:T(8,128)(2,1)} %copy-done.33, bf16[144,1024]{1,0:T(8,128)(2,1)} %collective-permute-done.27.refs_2_, ...), custom_call_target="tpu_custom_call" | custom-call | flops 3623878656 | bytes 8650752 | tf_op jit(solution)/shard_map/ffn/pallas_call | solution.py:255
  66.9 5.7 %collective-permute-start.9 = (bf16[144,1024]{1,0:T(8,128)(2,1)}, bf16[144,1024]{1,0:T(8,128)(2,1)}, u32[]{:S(2)}, u32[]{:S(2)}) collective-permute-start(bf16[144,1024]{1,0:T(8,128)(2,1)} %get-tuple-element.41), channel_id=1, source_target_pairs={{0,24},{8,16},{16,8},{24,0},{1,25},{9,17},{17,9},{25,1},{2,26},{10... | collective-permute-start | bytes 884744 | tf_op jit(solution)/shard_map/ppermute | solution.py:98
  72.6 4.2 %collective-permute-start.4 = (bf16[144,1024]{1,0:T(8,128)(2,1)}, bf16[144,1024]{1,0:T(8,128)(2,1)}, u32[]{:S(2)}, u32[]{:S(2)}) collective-permute-start(bf16[144,1024]{1,0:T(8,128)(2,1)} %get-tuple-element.35), channel_id=1, source_target_pairs={{0,8},{8,0},{16,24},{24,16},{1,9},{9,1},{17,25},{25,17},{2,10},{10... | collective-permute-start | bytes 884744 | tf_op jit(solution)/shard_map/ppermute | solution.py:98
  76.9 1.6 collective-permute-start.6
  78.5 2.0 %collective-permute-start.29 = (bf16[144,1024]{1,0:T(8,128)(2,1)}, bf16[144,1024]{1,0:T(8,128)(2,1)}, u32[]{:S(2)}, u32[]{:S(2)}) collective-permute-start(bf16[144,1024]{1,0:T(8,128)(2,1)} %get-tuple-element.59), channel_id=1, source_target_pairs={{0,8},{8,0},{16,24},{24,16},{1,9},{9,1},{17,25},{25,17},{2,10},{10... | collective-permute-start | bytes 884744 | tf_op jit(solution)/shard_map/ppermute | solution.py:98
  80.8 2.3 %dispatch.6 = (bf16[144,1024]{1,0:T(8,128)(2,1)}, bf16[144,1024]{1,0:T(8,128)(2,1)}, bf16[144,1024]{1,0:T(8,128)(2,1)}, bf16[144,1024]{1,0:T(8,128)(2,1)}) custom-call(bf16[192,1024]{1,0:T(8,128)(2,1)} %copy-done.18, f32[4,192]{1,0:T(4,128)} %copy-done.15), custom_call_target="tpu_custom_call" | custom-call | flops 226492416 | bytes 1572864 | tf_op jit(solution)/shard_map/dispatch/pallas_call | solution.py:158
  83.2 1.9 %collective-permute-start.18 = (bf16[144,1024]{1,0:T(8,128)(2,1)}, bf16[144,1024]{1,0:T(8,128)(2,1)S(1)}, u32[]{:S(2)}, u32[]{:S(2)}) collective-permute-start(bf16[144,1024]{1,0:T(8,128)(2,1)} %get-tuple-element.47), channel_id=1, source_target_pairs={{0,8},{8,0},{16,24},{24,16},{1,9},{9,1},{17,25},{25,17},{2,10},{10... | collective-permute-start | bytes 884744 | tf_op jit(solution)/shard_map/ppermute | solution.py:98
  85.1 6.3 %collective-permute-done.4.refs_1_ = bf16[144,1024]{1,0:T(8,128)(2,1)} collective-permute-done((bf16[144,1024]{1,0:T(8,128)(2,1)}, bf16[144,1024]{1,0:T(8,128)(2,1)}, u32[]{:S(2)}, u32[]{:S(2)}) %collective-permute-start.4) | collective-permute-done | bytes 294944 | tf_op jit(solution)/shard_map/ppermute | solution.py:98
  91.5 1.7 collective-permute-start.20
  93.5 5.7 %collective-permute-start.30 = (bf16[144,1024]{1,0:T(8,128)(2,1)S(1)}, bf16[144,1024]{1,0:T(8,128)(2,1)S(1)}, u32[]{:S(2)}, u32[]{:S(2)}) collective-permute-start(bf16[144,1024]{1,0:T(8,128)(2,1)S(1)} %copy-done.26), channel_id=1, source_target_pairs={{0,16},{8,24},{16,0},{24,8},{1,17},{9,25},{17,1},{25,9},{2,18},{10... | collective-permute-start | bytes 884744 | tf_op jit(solution)/shard_map/ppermute | solution.py:98
  99.2 4.9 %collective-permute-done.29.refs_1_ = bf16[144,1024]{1,0:T(8,128)(2,1)} collective-permute-done((bf16[144,1024]{1,0:T(8,128)(2,1)}, bf16[144,1024]{1,0:T(8,128)(2,1)}, u32[]{:S(2)}, u32[]{:S(2)}) %collective-permute-start.29) | collective-permute-done | bytes 294944 | tf_op jit(solution)/shard_map/ppermute | solution.py:98
  104.0 13.2 %ffn.3 = (bf16[144,1024]{1,0:T(8,128)(2,1)}, bf16[144,1024]{1,0:T(8,128)(2,1)}, bf16[144,1024]{1,0:T(8,128)(2,1)}, bf16[144,1024]{1,0:T(8,128)(2,1)}, bf16[144,1...) custom-call(bf16[144,1024]{1,0:T(8,128)(2,1)} %get-tuple-element.34.refs_0_,, ...), custom_call_target="tpu_custom_call" | custom-call | flops 7247757312 | bytes 11010048 | tf_op jit(solution)/shard_map/ffn/pallas_call | solution.py:255
  117.4 1.3 collective-permute-done.31.refs_3_
  118.7 3.2 %collective-permute-start.35 = (bf16[144,1024]{1,0:T(8,128)(2,1)}, bf16[144,1024]{1,0:T(8,128)(2,1)}, u32[]{:S(2)}, u32[]{:S(2)}) collective-permute-start(bf16[144,1024]{1,0:T(8,128)(2,1)} %get-tuple-element.64), channel_id=1, source_target_pairs={{0,16},{8,24},{16,0},{24,8},{1,17},{9,25},{17,1},{25,9},{2,18},{10... | collective-permute-start | bytes 884744 | tf_op jit(solution)/shard_map/ppermute | solution.py:98
  121.9 3.1 %combine.5 = bf16[192,1024]{1,0:T(8,128)(2,1)} custom-call(f32[4,192]{1,0:T(4,128)} %copy-done.37, bf16[144,1024]{1,0:T(8,128)(2,1)} %get-tuple-element.58.refs_0_, bf16[144,1024]{1,0:T(8,128)(2,1)} %collective-permute-done.29.refs_1_, bf16[144,1024]{1,0:T(8,128)(2,1)} %copy-done.34, bf16[144,1024]{1,0:T(8,128)(2,1)} %copy-done.35), custom_call_target="tpu_custom_call" | custom-call | flops 452984832 | bytes 1966080 | tf_op jit(solution)/shard_map/combine/pallas_call | solution.py:195
  124.9 0.5 collective-permute-start.36
  125.6 0.6 copy-done.30
  126.2 8.2 %ffn.4 = (bf16[144,1024]{1,0:T(8,128)(2,1)}, bf16[144,1024]{1,0:T(8,128)(2,1)}, bf16[144,1024]{1,0:T(8,128)(2,1)}, bf16[144,1024]{1,0:T(8,128)(2,1)}) custom-call(bf16[144,1024]{1,0:T(8,128)(2,1)} %get-tuple-element.46.refs_0_, bf16[144,1024]{1,0:T(8,128)(2,1)} %copy-done.27, bf16[144,1024]{1,0:T(8,128)(2,1)} %collective-permute-done.19.refs_2_, ...), custom_call_target="tpu_custom_call" | custom-call | flops 3623878656 | bytes 8650752 | tf_op jit(solution)/shard_map/ffn/pallas_call | solution.py:255
  134.4 1.8 %collective-permute-start.21 = (bf16[144,1024]{1,0:T(8,128)(2,1)}, bf16[144,1024]{1,0:T(8,128)(2,1)S(1)}, u32[]{:S(2)}, u32[]{:S(2)}) collective-permute-start(bf16[144,1024]{1,0:T(8,128)(2,1)} %get-tuple-element.51), channel_id=1, source_target_pairs={{0,8},{8,0},{16,24},{24,16},{1,9},{9,1},{17,25},{25,17},{2,10},{10... | collective-permute-start | bytes 884744 | tf_op jit(solution)/shard_map/ppermute | solution.py:98
  136.2 1.3 collective-permute-start.22
  137.5 0.5 collective-permute-start.23
  137.9 0.9 fusion.28
  138.8 1.7 %collective-permute-start.13 = (bf16[144,1024]{1,0:T(8,128)(2,1)}, bf16[144,1024]{1,0:T(8,128)(2,1)S(1)}, u32[]{:S(2)}, u32[]{:S(2)}) collective-permute-start(bf16[144,1024]{1,0:T(8,128)(2,1)} %get-tuple-element.43), channel_id=1, source_target_pairs={{0,8},{8,0},{16,24},{24,16},{1,9},{9,1},{17,25},{25,17},{2,10},{10... | collective-permute-start | bytes 884744 | tf_op jit(solution)/shard_map/ppermute | solution.py:98
  140.6 3.0 %combine.7 = bf16[192,1024]{1,0:T(8,128)(2,1)} custom-call(f32[4,192]{1,0:T(4,128)} %copy-done.36, bf16[144,1024]{1,0:T(8,128)(2,1)} %get-tuple-element.62.refs_0_, bf16[144,1024]{1,0:T(8,128)(2,1)} %copy-done.31, bf16[144,1024]{1,0:T(8,128)(2,1)} %collective-permute-done.35.refs_2_, bf16[144,1024]{1,0:T(8,128)(2,1)} %collective-permute-done.36.refs_3_), custom_call_target="tpu_custom_call" | custom-call | flops 452984832 | bytes 1966080 | tf_op jit(solution)/shard_map/combine/pallas_call | solution.py:195
  143.6 0.9 collective-permute-done.21.refs_1_
  144.5 1.0 collective-permute-start.14
  145.5 5.4 %collective-permute-done.22.refs_2_ = bf16[144,1024]{1,0:T(8,128)(2,1)S(1)} collective-permute-done((bf16[144,1024]{1,0:T(8,128)(2,1)}, bf16[144,1024]{1,0:T(8,128)(2,1)S(1)}, u32[]{:S(2)}, u32[]{:S(2)}) %collective-permute-start.22) | collective-permute-done | bytes 294944 | tf_op jit(solution)/shard_map/ppermute | solution.py:98
  151.0 0.4 collective-permute-start.15
  151.4 3.6 %collective-permute-start.37 = (bf16[192,1024]{1,0:T(8,128)(2,1)}, bf16[192,1024]{1,0:T(8,128)(2,1)S(1)}, u32[]{:S(2)}, u32[]{:S(2)}) collective-permute-start(bf16[192,1024]{1,0:T(8,128)(2,1)} %combine.7), channel_id=1, source_target_pairs={{0,2},{1,3},{2,4},{3,5},{4,6},{5,7},{6,0},{7,1},{8,10},{9,11},{10,... | collective-permute-start | bytes 1179656 | tf_op jit(solution)/shard_map/ppermute | solution.py:72
  155.0 0.7 copy-done.4
  155.8 3.2 %combine.6 = bf16[192,1024]{1,0:T(8,128)(2,1)} custom-call(f32[4,192]{1,0:T(4,128)} %copy-done.15, bf16[144,1024]{1,0:T(8,128)(2,1)} %get-tuple-element.50.refs_0_, bf16[144,1024]{1,0:T(8,128)(2,1)} %copy-done.5, bf16[144,1024]{1,0:T(8,128)(2,1)} %copy-done.7, bf16[144,1024]{1,0:T(8,128)(2,1)} %copy-done.8, bf16[192,1024]{1,0:T(8,128)(2,1)} %copy-done.4), custom_call_target="tpu_custom_call" | custom-call | flops 452984832 | bytes 1966080 | tf_op jit(solution)/shard_map/combine/pallas_call | solution.py:195
  159.1 1.2 convolution_bitcast_fusion
  160.4 0.6 copy-done.14
  161.0 0.8 multiply_convert_fusion
  161.9 1.2 collective-permute-done.14.refs_2_
  163.1 0.7 copy-done.9
  163.9 3.2 %combine.4 = f32[192,1024]{1,0:T(8,128)} custom-call(f32[4,192]{1,0:T(4,128)} %copy-done.11, bf16[144,1024]{1,0:T(8,128)(2,1)} %get-tuple-element.42.refs_0_, bf16[144,1024]{1,0:T(8,128)(2,1)} %copy-done.6, bf16[144,1024]{1,0:T(8,128)(2,1)} %copy-done.9, bf16[144,1024]{1,0:T(8,128)(2,1)} %copy-done.10), custom_call_target="tpu_custom_call" | custom-call | flops 452984832 | bytes 1966080 | tf_op jit(solution)/shard_map/combine/pallas_call | solution.py:195
  167.1 3.2 %collective-permute-done.33 = bf16[192,1024]{1,0:T(8,128)(2,1)S(1)} collective-permute-done((bf16[192,1024]{1,0:T(8,128)(2,1)}, bf16[192,1024]{1,0:T(8,128)(2,1)S(1)}, u32[]{:S(2)}, u32[]{:S(2)}) %collective-permute-start.33) | collective-permute-done | bytes 393248 | tf_op jit(solution)/shard_map/ppermute | solution.py:72
  170.3 2.0 %add_convert_fusion = bf16[192,1024]{1,0:T(8,128)(2,1)} fusion(bf16[192,1024]{1,0:T(8,128)(2,1)S(1)} %collective-permute-done.37, f32[192,1024]{1,0:T(8,128)} %combine.4, bf16[192,1024]{1,0:T(8,128)(2,1)S(1)} %collective-permute-done.33), kind=kLoop, calls=%fused_computation.12 | loop fusion | flops 983040 | bytes 1966080 | tf_op jit(solution)/shard_map/convert_element_type | solution.py:323
  (120 shorter events, 2.3 us)
Async XLA Ops:
  0.6 158.5 %copy-start = (bf16[4,256,256]{2,1,0:T(8,128)(2,1)S(1)}, bf16[4,256,256]{2,1,0:T(8,128)(2,1)}, u32[]{:S(2)}) copy-start(bf16[4,256,256]{2,1,0:T(8,128)(2,1)} %param.13) | copy-start | bytes 1572868
  1.9 8.8 %copy-start.2 = (bf16[192,1024]{1,0:T(8,128)(2,1)S(1)}, bf16[192,1024]{1,0:T(8,128)(2,1)}, u32[]{:S(2)}) copy-start(bf16[192,1024]{1,0:T(8,128)(2,1)} %param.11) | copy-start | bytes 1179652
  2.8 17.0 %copy-start.3 = (bf16[192,1024]{1,0:T(8,128)(2,1)}, bf16[192,1024]{1,0:T(8,128)(2,1)S(1)}, u32[]{:S(2)}) copy-start(bf16[192,1024]{1,0:T(8,128)(2,1)S(1)} %fusion.5.rows_ref) | copy-start | bytes 1179652
  2.8 16.1 %collective-permute-start.17 = (bf16[192,1024]{1,0:T(8,128)(2,1)S(1)}, bf16[192,1024]{1,0:T(8,128)(2,1)S(1)}, u32[]{:S(2)}, u32[]{:S(2)}) collective-permute-start(bf16[192,1024]{1,0:T(8,128)(2,1)S(1)} %fusion.5.rows_ref), channel_id=1, source_target_pairs={{0,2},{1,3},{2,4},{3,5},{4,6},{5,7},{6,0},{7,1},{8,10},{9,11},{10,... | collective-permute-start | bytes 1179656 | tf_op jit(solution)/shard_map/ppermute | solution.py:72
  5.9 36.7 %collective-permute-start.10 = (bf16[1024,512]{1,0:T(8,128)(2,1)}, bf16[1024,512]{1,0:T(8,128)(2,1)}, u32[]{:S(2)}, u32[]{:S(2)}) collective-permute-start(bf16[1024,512]{1,0:T(8,128)(2,1)} %bitcast.29), channel_id=1, source_target_pairs={{0,1},{1,0},{2,3},{3,2},{4,5},{5,4},{6,7},{7,6},{8,9},{9,8},{10,11... | collective-permute-start | bytes 3145736 | tf_op jit(solution)/shard_map/ppermute | solution.py:87
  7.5 28.0 %copy-start.11 = (f32[4,192]{1,0:T(4,128)}, f32[4,192]{1,0:T(4,128)S(1)}, u32[]{:S(2)}) copy-start(f32[4,192]{1,0:T(4,128)S(1)} %pad_maximum_fusion.table_ref) | copy-start | bytes 9220
  7.5 6.9 %collective-permute-start.24 = (f32[4,192]{1,0:T(4,128)S(1)}, f32[4,192]{1,0:T(4,128)S(1)}, u32[]{:S(2)}, u32[]{:S(2)}) collective-permute-start(f32[4,192]{1,0:T(4,128)S(1)} %pad_maximum_fusion.table_ref), channel_id=1, source_target_pairs={{0,4},{1,5},{2,6},{3,7},{4,0},{5,1},{6,2},{7,3},{8,12},{9,13},{10,... | collective-permute-start | bytes 9224 | tf_op jit(solution)/shard_map/ppermute | solution.py:72
  10.2 37.6 %collective-permute-start.11 = (bf16[1024,512]{1,0:T(8,128)(2,1)}, bf16[1024,512]{1,0:T(8,128)(2,1)}, u32[]{:S(2)}, u32[]{:S(2)}) collective-permute-start(bf16[1024,512]{1,0:T(8,128)(2,1)} %bitcast.33), channel_id=1, source_target_pairs={{0,1},{1,0},{2,3},{3,2},{4,5},{5,4},{6,7},{7,6},{8,9},{9,8},{10,11... | collective-permute-start | bytes 3145736 | tf_op jit(solution)/shard_map/ppermute | solution.py:87
  10.4 38.4 %collective-permute-start.12 = (bf16[512,1024]{1,0:T(8,128)(2,1)}, bf16[512,1024]{1,0:T(8,128)(2,1)}, u32[]{:S(2)}, u32[]{:S(2)}) collective-permute-start(bf16[512,1024]{1,0:T(8,128)(2,1)} %bitcast.37), channel_id=1, source_target_pairs={{0,1},{1,0},{2,3},{3,2},{4,5},{5,4},{6,7},{7,6},{8,9},{9,8},{10,11... | collective-permute-start | bytes 3145736 | tf_op jit(solution)/shard_map/ppermute | solution.py:87
  14.4 4.6 %copy-start.37 = (f32[4,192]{1,0:T(4,128)}, f32[4,192]{1,0:T(4,128)S(1)}, u32[]{:S(2)}) copy-start(f32[4,192]{1,0:T(4,128)S(1)} %collective-permute-done.24.table_ref) | copy-start | bytes 9220
  14.4 26.7 %collective-permute-start.2 = (bf16[192,1024]{1,0:T(8,128)(2,1)S(1)}, bf16[192,1024]{1,0:T(8,128)(2,1)S(1)}, u32[]{:S(2)}, u32[]{:S(2)}) collective-permute-start(bf16[192,1024]{1,0:T(8,128)(2,1)S(1)} %fusion.5.rows_ref), channel_id=1, source_target_pairs={{0,6},{1,7},{2,0},{3,1},{4,2},{5,3},{6,4},{7,5},{8,14},{9,15},{10,... | collective-permute-start | bytes 1179656 | tf_op jit(solution)/shard_map/ppermute | solution.py:72
  18.9 16.5 %collective-permute-start.25 = (bf16[192,1024]{1,0:T(8,128)(2,1)S(1)}, bf16[192,1024]{1,0:T(8,128)(2,1)S(1)}, u32[]{:S(2)}, u32[]{:S(2)}) collective-permute-start(bf16[192,1024]{1,0:T(8,128)(2,1)S(1)} %collective-permute-done.17.rows_ref), channel_id=1, source_target_pairs={{0,2},{1,3},{2,4},{3,5},{4,6},{5,7},{6,0},{7,1},{8,10},{9,11},{10,... | collective-permute-start | bytes 1179656 | tf_op jit(solution)/shard_map/ppermute | solution.py:72
  35.5 1.8 %copy-start.20 = (bf16[192,1024]{1,0:T(8,128)(2,1)}, bf16[192,1024]{1,0:T(8,128)(2,1)S(1)}, u32[]{:S(2)}) copy-start(bf16[192,1024]{1,0:T(8,128)(2,1)S(1)} %collective-permute-done.25.rows_ref) | copy-start | bytes 1179652
  35.5 4.1 %collective-permute-start.3 = (f32[4,192]{1,0:T(4,128)S(1)}, f32[4,192]{1,0:T(4,128)S(1)}, u32[]{:S(2)}, u32[]{:S(2)}) collective-permute-start(f32[4,192]{1,0:T(4,128)S(1)} %pad_maximum_fusion.table_ref), channel_id=1, source_target_pairs={{0,6},{1,7},{2,0},{3,1},{4,2},{5,3},{6,4},{7,5},{8,14},{9,15},{10,... | collective-permute-start | bytes 9224 | tf_op jit(solution)/shard_map/ppermute | solution.py:72
  39.6 3.5 %copy-start.36 = (f32[4,192]{1,0:T(4,128)}, f32[4,192]{1,0:T(4,128)S(1)}, u32[]{:S(2)}) copy-start(f32[4,192]{1,0:T(4,128)S(1)} %collective-permute-done.3.table_ref) | copy-start | bytes 9220
  39.6 10.7 %collective-permute-start.26 = (bf16[144,1024]{1,0:T(8,128)(2,1)}, bf16[144,1024]{1,0:T(8,128)(2,1)S(1)}, u32[]{:S(2)}, u32[]{:S(2)}) collective-permute-start(bf16[144,1024]{1,0:T(8,128)(2,1)} %get-tuple-element.55), channel_id=1, source_target_pairs={{0,8},{8,0},{16,24},{24,16},{1,9},{9,1},{17,25},{25,17},{2,10},{10... | collective-permute-start | bytes 884744 | tf_op jit(solution)/shard_map/ppermute | solution.py:98
  41.1 4.3 %copy-start.19 = (bf16[192,1024]{1,0:T(8,128)(2,1)}, bf16[192,1024]{1,0:T(8,128)(2,1)S(1)}, u32[]{:S(2)}) copy-start(bf16[192,1024]{1,0:T(8,128)(2,1)S(1)} %collective-permute-done.2.rows_ref) | copy-start | bytes 1179652
  41.1 13.6 %collective-permute-start.27 = (bf16[144,1024]{1,0:T(8,128)(2,1)}, bf16[144,1024]{1,0:T(8,128)(2,1)}, u32[]{:S(2)}, u32[]{:S(2)}) collective-permute-start(bf16[144,1024]{1,0:T(8,128)(2,1)} %get-tuple-element.56), channel_id=1, source_target_pairs={{0,16},{8,24},{16,0},{24,8},{1,17},{9,25},{17,1},{25,9},{2,18},{10... | collective-permute-start | bytes 884744 | tf_op jit(solution)/shard_map/ppermute | solution.py:98
  42.6 14.4 %collective-permute-start.28 = (bf16[144,1024]{1,0:T(8,128)(2,1)}, bf16[144,1024]{1,0:T(8,128)(2,1)}, u32[]{:S(2)}, u32[]{:S(2)}) collective-permute-start(bf16[144,1024]{1,0:T(8,128)(2,1)} %get-tuple-element.57), channel_id=1, source_target_pairs={{0,24},{8,16},{16,8},{24,0},{1,25},{9,17},{17,9},{25,1},{2,26},{10... | collective-permute-start | bytes 884744 | tf_op jit(solution)/shard_map/ppermute | solution.py:98
  45.4 2.3 %copy-start.12 = (f32[4,192]{1,0:T(4,128)S(1)}, f32[4,192]{1,0:T(4,128)}, u32[]{:S(2)}) copy-start(f32[4,192]{1,0:T(4,128)} %copy-done.11) | copy-start | bytes 9220
  45.4 3.4 %copy-start.32 = (bf16[144,1024]{1,0:T(8,128)(2,1)S(1)}, bf16[144,1024]{1,0:T(8,128)(2,1)}, u32[]{:S(2)}) copy-start(bf16[144,1024]{1,0:T(8,128)(2,1)} %get-tuple-element.39) | copy-start | bytes 884740
  45.4 4.9 %copy-start.29 = (bf16[144,1024]{1,0:T(8,128)(2,1)S(1)}, bf16[144,1024]{1,0:T(8,128)(2,1)}, u32[]{:S(2)}) copy-start(bf16[144,1024]{1,0:T(8,128)(2,1)} %get-tuple-element.40) | copy-start | bytes 884740
  47.7 19.1 %collective-permute-start.16 = (f32[4,192]{1,0:T(4,128)S(1)}, f32[4,192]{1,0:T(4,128)S(1)}, u32[]{:S(2)}, u32[]{:S(2)}) collective-permute-start(f32[4,192]{1,0:T(4,128)S(1)} %copy-done.12), channel_id=1, source_target_pairs={{0,2},{1,3},{2,4},{3,5},{4,6},{5,7},{6,0},{7,1},{8,10},{9,11},{10,... | collective-permute-start | bytes 9224 | tf_op jit(solution)/shard_map/ppermute | solution.py:72
  48.8 28.1 %collective-permute-start.7 = (bf16[144,1024]{1,0:T(8,128)(2,1)S(1)}, bf16[144,1024]{1,0:T(8,128)(2,1)S(1)}, u32[]{:S(2)}, u32[]{:S(2)}) collective-permute-start(bf16[144,1024]{1,0:T(8,128)(2,1)S(1)} %copy-done.32), channel_id=1, source_target_pairs={{0,8},{8,0},{16,24},{24,16},{1,9},{9,1},{17,25},{25,17},{2,10},{10... | collective-permute-start | bytes 884744 | tf_op jit(solution)/shard_map/ppermute | solution.py:98
  50.3 8.3 %copy-start.33 = (bf16[144,1024]{1,0:T(8,128)(2,1)}, bf16[144,1024]{1,0:T(8,128)(2,1)S(1)}, u32[]{:S(2)}) copy-start(bf16[144,1024]{1,0:T(8,128)(2,1)S(1)} %collective-permute-done.26.refs_1_) | copy-start | bytes 884740
  50.3 28.2 %collective-permute-start.8 = (bf16[144,1024]{1,0:T(8,128)(2,1)S(1)}, bf16[144,1024]{1,0:T(8,128)(2,1)S(1)}, u32[]{:S(2)}, u32[]{:S(2)}) collective-permute-start(bf16[144,1024]{1,0:T(8,128)(2,1)S(1)} %copy-done.29), channel_id=1, source_target_pairs={{0,16},{8,24},{16,0},{24,8},{1,17},{9,25},{17,1},{25,9},{2,18},{10... | collective-permute-start | bytes 884744 | tf_op jit(solution)/shard_map/ppermute | solution.py:98
  54.7 17.9 %collective-permute-start = (bf16[8,1024]{1,0:T(8,128)(2,1)S(1)}, bf16[8,1024]{1,0:T(8,128)(2,1)S(1)}, u32[]{:S(2)}, u32[]{:S(2)}) collective-permute-start(bf16[8,1024]{1,0:T(8,128)(2,1)S(1)} %get-tuple-element.71), channel_id=1, source_target_pairs={{0,1},{1,2},{2,3},{3,4},{4,5},{5,6},{6,7},{7,8},{8,9},{9,10},{10,1... | collective-permute-start | bytes 49160 | tf_op jit(solution)/shard_map/ppermute | solution.py:18
  57.1 19.8 %collective-permute-start.1 = (bf16[8,1024]{1,0:T(8,128)(2,1)S(1)}, bf16[8,1024]{1,0:T(8,128)(2,1)S(1)}, u32[]{:S(2)}, u32[]{:S(2)}) collective-permute-start(bf16[8,1024]{1,0:T(8,128)(2,1)S(1)} %get-tuple-element.72), channel_id=1, source_target_pairs={{1,0},{2,1},{3,2},{4,3},{5,4},{6,5},{7,6},{8,7},{9,8},{10,9},{11,1... | collective-permute-start | bytes 49160 | tf_op jit(solution)/shard_map/ppermute | solution.py:19
  58.6 18.3 %copy-start.25 = (bf16[144,1024]{1,0:T(8,128)(2,1)S(1)}, bf16[144,1024]{1,0:T(8,128)(2,1)}, u32[]{:S(2)}) copy-start(bf16[144,1024]{1,0:T(8,128)(2,1)} %get-tuple-element.36) | copy-start | bytes 884740
  58.6 18.3 %copy-start.23 = (bf16[144,1024]{1,0:T(8,128)(2,1)S(1)}, bf16[144,1024]{1,0:T(8,128)(2,1)}, u32[]{:S(2)}) copy-start(bf16[144,1024]{1,0:T(8,128)(2,1)} %get-tuple-element.37) | copy-start | bytes 884740
  66.9 11.6 %copy-start.15 = (f32[4,192]{1,0:T(4,128)}, f32[4,192]{1,0:T(4,128)S(1)}, u32[]{:S(2)}) copy-start(f32[4,192]{1,0:T(4,128)S(1)} %collective-permute-done.16.table_ref) | copy-start | bytes 9220
  66.9 16.3 %collective-permute-start.9 = (bf16[144,1024]{1,0:T(8,128)(2,1)}, bf16[144,1024]{1,0:T(8,128)(2,1)}, u32[]{:S(2)}, u32[]{:S(2)}) collective-permute-start(bf16[144,1024]{1,0:T(8,128)(2,1)} %get-tuple-element.41), channel_id=1, source_target_pairs={{0,24},{8,16},{16,8},{24,0},{1,25},{9,17},{17,9},{25,1},{2,26},{10... | collective-permute-start | bytes 884744 | tf_op jit(solution)/shard_map/ppermute | solution.py:98
  72.6 18.8 %collective-permute-start.4 = (bf16[144,1024]{1,0:T(8,128)(2,1)}, bf16[144,1024]{1,0:T(8,128)(2,1)}, u32[]{:S(2)}, u32[]{:S(2)}) collective-permute-start(bf16[144,1024]{1,0:T(8,128)(2,1)} %get-tuple-element.35), channel_id=1, source_target_pairs={{0,8},{8,0},{16,24},{24,16},{1,9},{9,1},{17,25},{25,17},{2,10},{10... | collective-permute-start | bytes 884744 | tf_op jit(solution)/shard_map/ppermute | solution.py:98
  76.9 14.7 %collective-permute-start.5 = (bf16[144,1024]{1,0:T(8,128)(2,1)S(1)}, bf16[144,1024]{1,0:T(8,128)(2,1)}, u32[]{:S(2)}, u32[]{:S(2)}) collective-permute-start(bf16[144,1024]{1,0:T(8,128)(2,1)S(1)} %copy-done.25), channel_id=1, source_target_pairs={{0,16},{8,24},{16,0},{24,8},{1,17},{9,25},{17,1},{25,9},{2,18},{10... | collective-permute-start | bytes 884744 | tf_op jit(solution)/shard_map/ppermute | solution.py:98
  76.9 3.7 %copy-start.21 = (bf16[144,1024]{1,0:T(8,128)(2,1)}, bf16[144,1024]{1,0:T(8,128)(2,1)S(1)}, u32[]{:S(2)}) copy-start(bf16[144,1024]{1,0:T(8,128)(2,1)S(1)} %collective-permute-done.7.refs_5_) | copy-start | bytes 884740
  76.9 16.6 %collective-permute-start.6 = (bf16[144,1024]{1,0:T(8,128)(2,1)S(1)}, bf16[144,1024]{1,0:T(8,128)(2,1)}, u32[]{:S(2)}, u32[]{:S(2)}) collective-permute-start(bf16[144,1024]{1,0:T(8,128)(2,1)S(1)} %copy-done.23), channel_id=1, source_target_pairs={{0,24},{8,16},{16,8},{24,0},{1,25},{9,17},{17,9},{25,1},{2,26},{10... | collective-permute-start | bytes 884744 | tf_op jit(solution)/shard_map/ppermute | solution.py:98
  78.5 2.1 %copy-start.22 = (bf16[144,1024]{1,0:T(8,128)(2,1)}, bf16[144,1024]{1,0:T(8,128)(2,1)S(1)}, u32[]{:S(2)}) copy-start(bf16[144,1024]{1,0:T(8,128)(2,1)S(1)} %collective-permute-done.8.refs_6_) | copy-start | bytes 884740
  78.5 25.5 %collective-permute-start.29 = (bf16[144,1024]{1,0:T(8,128)(2,1)}, bf16[144,1024]{1,0:T(8,128)(2,1)}, u32[]{:S(2)}, u32[]{:S(2)}) collective-permute-start(bf16[144,1024]{1,0:T(8,128)(2,1)} %get-tuple-element.59), channel_id=1, source_target_pairs={{0,8},{8,0},{16,24},{24,16},{1,9},{9,1},{17,25},{25,17},{2,10},{10... | collective-permute-start | bytes 884744 | tf_op jit(solution)/shard_map/ppermute | solution.py:98
  80.8 12.6 %copy-start.26 = (bf16[144,1024]{1,0:T(8,128)(2,1)S(1)}, bf16[144,1024]{1,0:T(8,128)(2,1)}, u32[]{:S(2)}) copy-start(bf16[144,1024]{1,0:T(8,128)(2,1)} %get-tuple-element.60) | copy-start | bytes 884740
  80.8 23.2 %copy-start.24 = (bf16[144,1024]{1,0:T(8,128)(2,1)S(1)}, bf16[144,1024]{1,0:T(8,128)(2,1)}, u32[]{:S(2)}) copy-start(bf16[144,1024]{1,0:T(8,128)(2,1)} %get-tuple-element.61) | copy-start | bytes 884740
  83.2 41.7 %collective-permute-start.18 = (bf16[144,1024]{1,0:T(8,128)(2,1)}, bf16[144,1024]{1,0:T(8,128)(2,1)S(1)}, u32[]{:S(2)}, u32[]{:S(2)}) collective-permute-start(bf16[144,1024]{1,0:T(8,128)(2,1)} %get-tuple-element.47), channel_id=1, source_target_pairs={{0,8},{8,0},{16,24},{24,16},{1,9},{9,1},{17,25},{25,17},{2,10},{10... | collective-permute-start | bytes 884744 | tf_op jit(solution)/shard_map/ppermute | solution.py:98
  91.4 34.1 %collective-permute-start.19 = (bf16[144,1024]{1,0:T(8,128)(2,1)}, bf16[144,1024]{1,0:T(8,128)(2,1)}, u32[]{:S(2)}, u32[]{:S(2)}) collective-permute-start(bf16[144,1024]{1,0:T(8,128)(2,1)} %get-tuple-element.48), channel_id=1, source_target_pairs={{0,16},{8,24},{16,0},{24,8},{1,17},{9,25},{17,1},{25,9},{2,18},{10... | collective-permute-start | bytes 884744 | tf_op jit(solution)/shard_map/ppermute | solution.py:98
  91.5 33.9 %collective-permute-start.20 = (bf16[144,1024]{1,0:T(8,128)(2,1)}, bf16[144,1024]{1,0:T(8,128)(2,1)S(1)}, u32[]{:S(2)}, u32[]{:S(2)}) collective-permute-start(bf16[144,1024]{1,0:T(8,128)(2,1)} %get-tuple-element.49), channel_id=1, source_target_pairs={{0,24},{8,16},{16,8},{24,0},{1,25},{9,17},{17,9},{25,1},{2,26},{10... | collective-permute-start | bytes 884744 | tf_op jit(solution)/shard_map/ppermute | solution.py:98
  93.5 23.8 %collective-permute-start.30 = (bf16[144,1024]{1,0:T(8,128)(2,1)S(1)}, bf16[144,1024]{1,0:T(8,128)(2,1)S(1)}, u32[]{:S(2)}, u32[]{:S(2)}) collective-permute-start(bf16[144,1024]{1,0:T(8,128)(2,1)S(1)} %copy-done.26), channel_id=1, source_target_pairs={{0,16},{8,24},{16,0},{24,8},{1,17},{9,25},{17,1},{25,9},{2,18},{10... | collective-permute-start | bytes 884744 | tf_op jit(solution)/shard_map/ppermute | solution.py:98
  104.0 14.7 %collective-permute-start.31 = (bf16[144,1024]{1,0:T(8,128)(2,1)S(1)}, bf16[144,1024]{1,0:T(8,128)(2,1)S(1)}, u32[]{:S(2)}, u32[]{:S(2)}) collective-permute-start(bf16[144,1024]{1,0:T(8,128)(2,1)S(1)} %copy-done.24), channel_id=1, source_target_pairs={{0,24},{8,16},{16,8},{24,0},{1,25},{9,17},{17,9},{25,1},{2,26},{10... | collective-permute-start | bytes 884744 | tf_op jit(solution)/shard_map/ppermute | solution.py:98
  117.3 4.6 %copy-start.34 = (bf16[144,1024]{1,0:T(8,128)(2,1)}, bf16[144,1024]{1,0:T(8,128)(2,1)S(1)}, u32[]{:S(2)}) copy-start(bf16[144,1024]{1,0:T(8,128)(2,1)S(1)} %collective-permute-done.30.refs_2_) | copy-start | bytes 884740
  117.3 18.8 %collective-permute-start.34 = (bf16[144,1024]{1,0:T(8,128)(2,1)}, bf16[144,1024]{1,0:T(8,128)(2,1)S(1)}, u32[]{:S(2)}, u32[]{:S(2)}) collective-permute-start(bf16[144,1024]{1,0:T(8,128)(2,1)} %get-tuple-element.63), channel_id=1, source_target_pairs={{0,8},{8,0},{16,24},{24,16},{1,9},{9,1},{17,25},{25,17},{2,10},{10... | collective-permute-start | bytes 884744 | tf_op jit(solution)/shard_map/ppermute | solution.py:98
  118.7 3.2 %copy-start.35 = (bf16[144,1024]{1,0:T(8,128)(2,1)}, bf16[144,1024]{1,0:T(8,128)(2,1)S(1)}, u32[]{:S(2)}) copy-start(bf16[144,1024]{1,0:T(8,128)(2,1)S(1)} %collective-permute-done.31.refs_3_) | copy-start | bytes 884740
  118.7 18.8 %collective-permute-start.35 = (bf16[144,1024]{1,0:T(8,128)(2,1)}, bf16[144,1024]{1,0:T(8,128)(2,1)}, u32[]{:S(2)}, u32[]{:S(2)}) collective-permute-start(bf16[144,1024]{1,0:T(8,128)(2,1)} %get-tuple-element.64), channel_id=1, source_target_pairs={{0,16},{8,24},{16,0},{24,8},{1,17},{9,25},{17,1},{25,9},{2,18},{10... | collective-permute-start | bytes 884744 | tf_op jit(solution)/shard_map/ppermute | solution.py:98
  121.9 3.1 %copy-start.28 = (bf16[144,1024]{1,0:T(8,128)(2,1)S(1)}, bf16[144,1024]{1,0:T(8,128)(2,1)}, u32[]{:S(2)}) copy-start(bf16[144,1024]{1,0:T(8,128)(2,1)} %get-tuple-element.65) | copy-start | bytes 884740
  124.9 13.9 %collective-permute-start.36 = (bf16[144,1024]{1,0:T(8,128)(2,1)S(1)}, bf16[144,1024]{1,0:T(8,128)(2,1)}, u32[]{:S(2)}, u32[]{:S(2)}) collective-permute-start(bf16[144,1024]{1,0:T(8,128)(2,1)S(1)} %copy-done.28), channel_id=1, source_target_pairs={{0,24},{8,16},{16,8},{24,0},{1,25},{9,17},{17,9},{25,1},{2,26},{10... | collective-permute-start | bytes 884744 | tf_op jit(solution)/shard_map/ppermute | solution.py:98
  125.5 29.6 %collective-permute-start.32 = (bf16[192,1024]{1,0:T(8,128)(2,1)}, bf16[192,1024]{1,0:T(8,128)(2,1)S(1)}, u32[]{:S(2)}, u32[]{:S(2)}) collective-permute-start(bf16[192,1024]{1,0:T(8,128)(2,1)} %combine.5), channel_id=1, source_target_pairs={{0,6},{1,7},{2,0},{3,1},{4,2},{5,3},{6,4},{7,5},{8,14},{9,15},{10,... | collective-permute-start | bytes 1179656 | tf_op jit(solution)/shard_map/ppermute | solution.py:72
  134.4 10.1 %collective-permute-start.21 = (bf16[144,1024]{1,0:T(8,128)(2,1)}, bf16[144,1024]{1,0:T(8,128)(2,1)S(1)}, u32[]{:S(2)}, u32[]{:S(2)}) collective-permute-start(bf16[144,1024]{1,0:T(8,128)(2,1)} %get-tuple-element.51), channel_id=1, source_target_pairs={{0,8},{8,0},{16,24},{24,16},{1,9},{9,1},{17,25},{25,17},{2,10},{10... | collective-permute-start | bytes 884744 | tf_op jit(solution)/shard_map/ppermute | solution.py:98
  136.2 1.3 copy-start.31
  136.2 14.8 %collective-permute-start.22 = (bf16[144,1024]{1,0:T(8,128)(2,1)}, bf16[144,1024]{1,0:T(8,128)(2,1)S(1)}, u32[]{:S(2)}, u32[]{:S(2)}) collective-permute-start(bf16[144,1024]{1,0:T(8,128)(2,1)} %get-tuple-element.52), channel_id=1, source_target_pairs={{0,16},{8,24},{16,0},{24,8},{1,17},{9,25},{17,1},{25,9},{2,18},{10... | collective-permute-start | bytes 884744 | tf_op jit(solution)/shard_map/ppermute | solution.py:98
  137.5 13.9 %collective-permute-start.23 = (bf16[144,1024]{1,0:T(8,128)(2,1)}, bf16[144,1024]{1,0:T(8,128)(2,1)S(1)}, u32[]{:S(2)}, u32[]{:S(2)}) collective-permute-start(bf16[144,1024]{1,0:T(8,128)(2,1)} %get-tuple-element.53), channel_id=1, source_target_pairs={{0,24},{8,16},{16,8},{24,0},{1,25},{9,17},{17,9},{25,1},{2,26},{10... | collective-permute-start | bytes 884744 | tf_op jit(solution)/shard_map/ppermute | solution.py:98
  138.8 23.0 %collective-permute-start.13 = (bf16[144,1024]{1,0:T(8,128)(2,1)}, bf16[144,1024]{1,0:T(8,128)(2,1)S(1)}, u32[]{:S(2)}, u32[]{:S(2)}) collective-permute-start(bf16[144,1024]{1,0:T(8,128)(2,1)} %get-tuple-element.43), channel_id=1, source_target_pairs={{0,8},{8,0},{16,24},{24,16},{1,9},{9,1},{17,25},{25,17},{2,10},{10... | collective-permute-start | bytes 884744 | tf_op jit(solution)/shard_map/ppermute | solution.py:98
  144.5 10.5 %copy-start.5 = (bf16[144,1024]{1,0:T(8,128)(2,1)}, bf16[144,1024]{1,0:T(8,128)(2,1)S(1)}, u32[]{:S(2)}) copy-start(bf16[144,1024]{1,0:T(8,128)(2,1)S(1)} %collective-permute-done.21.refs_1_) | copy-start | bytes 884740
  144.5 18.6 %collective-permute-start.14 = (bf16[144,1024]{1,0:T(8,128)(2,1)}, bf16[144,1024]{1,0:T(8,128)(2,1)S(1)}, u32[]{:S(2)}, u32[]{:S(2)}) collective-permute-start(bf16[144,1024]{1,0:T(8,128)(2,1)} %get-tuple-element.44), channel_id=1, source_target_pairs={{0,16},{8,24},{16,0},{24,8},{1,17},{9,25},{17,1},{25,9},{2,18},{10... | collective-permute-start | bytes 884744 | tf_op jit(solution)/shard_map/ppermute | solution.py:98
  150.9 4.1 %copy-start.7 = (bf16[144,1024]{1,0:T(8,128)(2,1)}, bf16[144,1024]{1,0:T(8,128)(2,1)S(1)}, u32[]{:S(2)}) copy-start(bf16[144,1024]{1,0:T(8,128)(2,1)S(1)} %collective-permute-done.22.refs_2_) | copy-start | bytes 884740
  151.0 12.2 %collective-permute-start.15 = (bf16[144,1024]{1,0:T(8,128)(2,1)}, bf16[144,1024]{1,0:T(8,128)(2,1)S(1)}, u32[]{:S(2)}, u32[]{:S(2)}) collective-permute-start(bf16[144,1024]{1,0:T(8,128)(2,1)} %get-tuple-element.45), channel_id=1, source_target_pairs={{0,24},{8,16},{16,8},{24,0},{1,25},{9,17},{17,9},{25,1},{2,26},{10... | collective-permute-start | bytes 884744 | tf_op jit(solution)/shard_map/ppermute | solution.py:98
  151.4 3.7 %copy-start.8 = (bf16[144,1024]{1,0:T(8,128)(2,1)}, bf16[144,1024]{1,0:T(8,128)(2,1)S(1)}, u32[]{:S(2)}) copy-start(bf16[144,1024]{1,0:T(8,128)(2,1)S(1)} %collective-permute-done.23.refs_3_) | copy-start | bytes 884740
  151.4 15.7 %collective-permute-start.37 = (bf16[192,1024]{1,0:T(8,128)(2,1)}, bf16[192,1024]{1,0:T(8,128)(2,1)S(1)}, u32[]{:S(2)}, u32[]{:S(2)}) collective-permute-start(bf16[192,1024]{1,0:T(8,128)(2,1)} %combine.7), channel_id=1, source_target_pairs={{0,2},{1,3},{2,4},{3,5},{4,6},{5,7},{6,0},{7,1},{8,10},{9,11},{10,... | collective-permute-start | bytes 1179656 | tf_op jit(solution)/shard_map/ppermute | solution.py:72
  158.9 11.3 %collective-permute-start.33 = (bf16[192,1024]{1,0:T(8,128)(2,1)}, bf16[192,1024]{1,0:T(8,128)(2,1)S(1)}, u32[]{:S(2)}, u32[]{:S(2)}) collective-permute-start(bf16[192,1024]{1,0:T(8,128)(2,1)} %combine.6), channel_id=1, source_target_pairs={{0,6},{1,7},{2,0},{3,1},{4,2},{5,3},{6,4},{7,5},{8,14},{9,15},{10,... | collective-permute-start | bytes 1179656 | tf_op jit(solution)/shard_map/ppermute | solution.py:72
  (12 other events, 10.0 us)
